TPU v7x, 128 devices: a whole 4x4x4 slice. The times are simulated.
128 devices in a mesh: sp: 32 (over z, y, core), tp: 4 (over x).
Axes of the slice: x: 4, y: 4, z: 4, core: 2. Of those that a mesh axis runs over, the one named last changes fastest.
Arguments:
- layer_input: bfloat16 [16384, 2048], P('sp'), may hold values from -6 to 6
- out_cot: bfloat16 [16384, 2048], P('sp'), may hold values from -6 to 6
- expert_ids: int32 [16384, 2], P('sp'), may hold values from 0 to 31, all different within a row; in each aligned block of 512 rows (0 to 511, 512 to 1023, ...) at most 40 rows name the same one
- route_weight: float32 [16384, 2], P('sp'), may hold values from 0.1 to 1
- w_gate: bfloat16 [32, 2048, 1024], P('sp', None, 'tp'), may hold values from -0.125 to 0.125
- w_up: bfloat16 [32, 2048, 1024], P('sp', None, 'tp'), may hold values from -0.125 to 0.125
- w_down: bfloat16 [32, 1024, 2048], P('sp', 'tp'), may hold values from -0.1875 to 0.1875
- out_proj: bfloat16 [2048, 1024], P(None, 'tp'), may hold values from -0.1875 to 0.1875
- rec_input: bfloat16 [16384, 1024], P('sp', 'tp'), may hold values from -6 to 6
- gate_input: bfloat16 [16384, 1024], P('sp', 'tp'), may hold values from -6 to 6
- prev_state: float32 [16384, 1024], P('sp', 'tp'), may hold values from -6 to 6
- decay_param: float32 [1024], replicated, may hold values from 4 to 20
- extra_decay: float32 [8, 16384], P('tp', 'sp'), may hold values from -3 to 0, as said below
- gate_a_w: bfloat16 [8, 128, 128], replicated, may hold values from -0.5 to 0.5
- gate_i_w: bfloat16 [8, 128, 128], replicated, may hold values from -0.5 to 0.5
Outputs:
- grad_gate: float32 [32, 2048, 1024], P('sp', None, 'tp')
- grad_up: float32 [32, 2048, 1024], P('sp', None, 'tp')
- grad_down: float32 [32, 1024, 2048], P('sp', 'tp')
- grad_out_proj: float32 [2048, 1024], P('sp', 'tp')
- rec_input_grad: bfloat16 [16384, 1024], P('sp', 'tp')
- gate_input_grad: bfloat16 [16384, 1024], P('sp', 'tp')
Inputs may be any that keep to these rules, and one draw needn't show every extreme that they name: `expert_ids`: each row names 2 different experts; among the slots of the tokens of one sp index (aligned blocks of 512 rows) no expert is named more than 40 times, and in every draw some expert is named exactly 40 times in some block. `extra_decay`: every entry is at most -0.05 / 16384.
All inputs are finite; a program needn't handle non-finite values.
Results may differ from a plain program's by a relative error of at most 0.017.
Values may be sent and summed in bfloat16 or wider, within the bound.
No kernel may reach another device: no remote copies, remote signals or barrier semaphores. Data moves between devices by JAX's collectives and lax.ppermute only.
A program may use at most 128 MiB of HBM per device.

v0:
```python
import functools
import jax
import jax.numpy as jnp
from jax import lax
from jax.experimental import pallas as pl
from jax.experimental.pallas import tpu as pltpu
from jax.sharding import Mesh, PartitionSpec as P


F32 = jnp.float32
BF16 = jnp.bfloat16
gelu_scale = 0.7978845608028654
gelu_cubic = 0.044715
decay_factor = 8.0
ring_steps = (0, 3, 1, 2)


def params(limit_mib=48, **extra):
    return pltpu.CompilerParams(vmem_limit_bytes=limit_mib * 1024 * 1024, **extra)


def cost(flops, moved):
    return pl.CostEstimate(flops=flops, bytes_accessed=moved, transcendentals=0)


def whole(shape):
    return pl.BlockSpec(shape, lambda *_: (0,) * len(shape), pipeline_mode=pl.Buffered(1))


SMEM = pl.BlockSpec(memory_space=pltpu.SMEM)


def made(shape, dtype):
    return pltpu.HBM(shape, dtype)


def kept(arrays):
    return [pltpu.with_memory_space_constraint(a, pltpu.HBM) for a in arrays]


def dot(a, b, dims=((1,), (0,))):
    return lax.dot_general(a, b, (dims, ((), ())), preferred_element_type=F32)


def sigmoid(v):
    return 1.0 / (1.0 + jnp.exp(-v))


def minus_expm1(v):
    series = 1.0 + v / 8.0
    for order in range(7, 1, -1):
        series = 1.0 + v / order * series
    return jnp.where(v > -0.5, -v * series, 1.0 - jnp.exp(v))


def early_kernel(
    where_ref, ids, rec, gate_in, prev, rates, extra, map_a, map_i,
    out_rec, out_act, out_b, out_ca, out_ci, out_cs, out_decay, out_seg, out_exp, out_block, out_sel,
    *, capacity, experts,
):
    tokens, channels = rec.shape
    heads = channels // 128
    first = where_ref[0] * heads
    for h in range(heads):
        cols = slice(h * 128, (h + 1) * 128)
        values_bf = rec[:, cols]
        x = values_bf.astype(F32)
        ra = sigmoid(dot(values_bf, map_a[first + h]))
        ig = sigmoid(dot(values_bf, map_i[first + h]))
        rate = rates[pl.ds(first + h, 1), :]
        log_decay = -rate * ra + extra[:, h : h + 1]
        decay = jnp.exp(log_decay)
        scale = jnp.sqrt(minus_expm1(2.0 * log_decay))
        before = prev[:, cols]
        state = decay * before + scale * ig * x
        g = gate_in[:, cols].astype(F32)
        bend = jnp.tanh(gelu_scale * (g + gelu_cubic * g * g * g))
        act = 0.5 * g * (1.0 + bend)
        slope = 0.5 * (1.0 + bend) + 0.5 * g * (1.0 - bend * bend) * gelu_scale * (
            1.0 + 3.0 * gelu_cubic * g * g
        )
        out_rec[:, cols] = (state * act).astype(BF16)
        out_act[:, cols] = act
        out_b[:, cols] = state * slope
        out_ca[:, cols] = (decay * before - decay * decay / scale * ig * x) * -rate * ra * (1.0 - ra)
        out_ci[:, cols] = scale * x * ig * (1.0 - ig)
        out_cs[:, cols] = scale * ig
        out_decay[h] = decay
    length = tokens // 8
    for h in range(heads):
        cols = slice(h * 128, (h + 1) * 128)
        product = jnp.ones((8, 128), F32)
        for i in range(length - 1, -1, -1):
            out_seg[h, pl.ds(i, 8, stride=length), :] = product
            product = product * out_decay[h, pl.ds(i, 8, stride=length), :]
        carry = jnp.ones((1, 128), F32)
        for k in range(7, -1, -1):
            rows = slice(k * length, (k + 1) * length)
            out_exp[rows, cols] = out_seg[h, rows, :] * carry
            carry = carry * product[k : k + 1, :]
        out_block[:, cols] = jnp.broadcast_to(carry, (8, 128))
    lane = lax.broadcasted_iota(jnp.int32, (tokens, 128), 1)
    first_id = ids[:, 0:1]
    second_id = ids[:, 1:2]
    one = (lane == first_id).astype(F32)
    two = (lane == second_id).astype(F32)
    lower = lax.broadcasted_iota(jnp.int32, (tokens, tokens), 0) > lax.broadcasted_iota(
        jnp.int32, (tokens, tokens), 1
    )
    rank = dot(lower.astype(F32).astype(BF16), (one + two).astype(BF16))
    place_one = first_id * capacity + jnp.sum(rank * one, axis=1, keepdims=True).astype(jnp.int32)
    place_two = second_id * capacity + jnp.sum(rank * two, axis=1, keepdims=True).astype(jnp.int32)
    slots = experts * capacity
    for at in range(0, slots, 256):
        slot = lax.broadcasted_iota(jnp.int32, (tokens, 256), 1) + at
        hit = (slot == place_one) | (slot == place_two)
        out_sel[:, at : at + 256] = jnp.where(hit, 1.0, 0.0).astype(BF16)


def early(position, ids, rec, gate_in, prev, rates, extra, map_a, map_i, capacity, experts):
    tokens, channels = rec.shape
    wide = made((tokens, channels), F32)
    heads = made((channels // 128, tokens, 128), F32)
    outs = (
        made((tokens, channels), BF16),
        wide, wide, wide, wide, wide, heads, heads, wide,
        made((8, channels), F32),
        made((tokens, experts * capacity), BF16),
    )
    args = (position, ids, rec, gate_in, prev, rates, extra, map_a, map_i)
    return pl.pallas_call(
        functools.partial(early_kernel, capacity=capacity, experts=experts),
        out_shape=outs,
        in_specs=[SMEM] + [whole(a.shape) for a in args[1:]],
        out_specs=[whole(o.shape) for o in outs],
        compiler_params=params(14),
        cost_estimate=cost(3 * 10**9, 8 * 2**20),
        name="early",
    )(args[0], *kept(args[1:]))


def build_kernel(where_ref, ids, weight, *refs, capacity, group, weighted):
    sources, out, rank_ref, weight_ref = refs[:-3], refs[-3], refs[-2], refs[-1]
    experts, tokens = rank_ref.shape

    @pl.when(pl.program_id(0) == 0)
    def _():
        name = lax.broadcasted_iota(jnp.int32, (experts, tokens), 0)
        one = jnp.where(name == ids[0:1, :], 1.0, 0.0)
        two = jnp.where(name == ids[1:2, :], 1.0, 0.0)
        both = one + two
        upper = lax.broadcasted_iota(jnp.int32, (tokens, tokens), 0) < lax.broadcasted_iota(
            jnp.int32, (tokens, tokens), 1
        )
        rank = dot(both.astype(BF16), upper.astype(F32).astype(BF16))
        rank_ref[...] = jnp.where(both > 0.0, rank, -1.0)
        weight_ref[...] = one * weight[0:1, :] + two * weight[1:2, :]

    first = pl.program_id(0) * group
    place = lax.broadcasted_iota(jnp.int32, (capacity, tokens), 0).astype(F32)
    picks, weights = [], []
    for e in range(group):
        hit = place == rank_ref[pl.ds(first + e, 1), :]
        picks.append(jnp.where(hit, 1.0, 0.0))
        weights.append(
            jnp.sum(jnp.where(hit, weight_ref[pl.ds(first + e, 1), :], 0.0), axis=1, keepdims=True)
        )
    pick = jnp.concatenate(picks, axis=0).astype(BF16)
    by = jnp.concatenate(weights, axis=0)
    at = 0
    for source, scaled in zip(sources, weighted):
        rows = dot(pick, source[...])
        if scaled:
            rows = rows * by
        out[:, at : at + source.shape[1]] = rows.astype(BF16)
        at += source.shape[1]


def build(position, ids, weight, parts, capacity, experts, group=4):
    tokens = ids.shape[1]
    total = sum(width for _, width, _, _ in parts)
    specs = [pl.BlockSpec(ids.shape, lambda i, where: (0, 0))] * 2
    for _, width, column, _ in parts:
        specs.append(pl.BlockSpec((tokens, width), functools.partial(column_block, column)))
    return pl.pallas_call(
        functools.partial(
            build_kernel, capacity=capacity, group=group, weighted=tuple(p[3] for p in parts)
        ),
        out_shape=made((experts * capacity, total), BF16),
        grid_spec=pltpu.PrefetchScalarGridSpec(
            num_scalar_prefetch=1,
            grid=(experts // group,),
            in_specs=specs,
            out_specs=pl.BlockSpec((group * capacity, total), lambda i, where: (i, 0)),
            scratch_shapes=[pltpu.VMEM((experts, tokens), F32), pltpu.VMEM((experts, tokens), F32)],
        ),
        compiler_params=params(14),
        cost_estimate=cost(1400000 * total, 5000 * total),
    )(position, *kept([ids, weight, *(p[0] for p in parts)]))


def column_block(column, i, where):
    return (0, where[0] if column is None else column)


def weights_kernel(where_ref, w_gate, w_up, *refs):
    pieces, out_gate, out_up = refs[:-2], refs[-2], refs[-1]
    at = where_ref[0]
    for n, step in enumerate(ring_steps):
        group = lax.rem(at + step, 4)
        top, bottom = pieces[2 * n], pieces[2 * n + 1]
        half = top.shape[0]
        for weights, out in ((w_gate, out_gate), (w_up, out_up)):
            out[group] = (
                dot(weights[:half, :], top[...], ((0,), (0,)))
                + dot(weights[half:, :], bottom[...], ((0,), (0,)))
            ).astype(BF16)


def folded_weights(position, w_gate, w_up, pieces):
    hidden, width = w_gate.shape[1], pieces[0].shape[1]
    args = (position, w_gate, w_up, *pieces)
    out = made((4, hidden, width), BF16)
    return pl.pallas_call(
        weights_kernel,
        out_shape=(out, out),
        in_specs=[SMEM] + [whole(a.shape) for a in args[1:]],
        out_specs=[whole(out.shape)] * 2,
        compiler_params=params(16),
        cost_estimate=cost(4 * 10**9, 7 * 2**20),
        name="folded",
    )(position, *kept([w_gate, w_up]), *pieces)


def expert_kernel(where_ref, got_rows, got_cot, *refs, row_part, cot_part):
    pieces = refs[:8]
    w_gate, w_up, w_down, fold_gate, fold_up, out_hidden, out_gate, out_up, out_mix = refs[8:]
    at = where_ref[0]
    upper = pl.program_id(0) < pl.num_programs(0) // 2
    rows, cots = got_rows[...], got_cot[...]
    gate_pre = dot(rows, w_gate[4 * row_part :, :])
    up_pre = dot(rows, w_up[4 * row_part :, :])
    hidden_cot = dot(cots, w_down[:, 4 * cot_part :], ((1,), (1,)))
    for n, step in enumerate(ring_steps):
        group = lax.rem(at + step, 4)
        piece = jnp.where(upper, pieces[2 * n][...], pieces[2 * n + 1][...])
        lines = pl.ds(pl.multiple_of(group * row_part, row_part), row_part)
        columns = pl.ds(pl.multiple_of(group * cot_part, 128), cot_part)
        gate_pre = gate_pre + dot(piece[:, :row_part], w_gate[lines, :])
        up_pre = up_pre + dot(piece[:, :row_part], w_up[lines, :])
        hidden_cot = hidden_cot + dot(piece[:, row_part:], w_down[:, columns], ((1,), (1,)))
    sigma = sigmoid(gate_pre)
    swish = gate_pre * sigma
    out_hidden[...] = (swish * up_pre).astype(BF16)
    gate_cot = (hidden_cot * up_pre * sigma * (1.0 + gate_pre * (1.0 - sigma))).astype(BF16)
    up_cot = (hidden_cot * swish).astype(BF16)
    out_gate[...] = gate_cot
    out_up[...] = up_cot
    for c in range(4):
        out_mix[c] = (dot(gate_cot, fold_gate[c]) + dot(up_cot, fold_up[c])).astype(BF16)


def expert(position, got, pieces, w_gate, w_up, w_down, fold_gate, fold_up, row_part, cot_part, steps=4):
    rows = got.shape[0]
    width, hidden = w_gate.shape
    block = rows // steps
    part = fold_gate.shape[2]
    half = steps // 2
    row_rest, cot_rest = width - 4 * row_part, width - 4 * cot_part
    narrow = made((rows, hidden), BF16)
    mine = pl.BlockSpec((block, hidden), lambda i: (i, 0))
    top = pl.BlockSpec((block, row_part + cot_part), lambda i: (jnp.minimum(i, half - 1), 0))
    bottom = pl.BlockSpec((block, row_part + cot_part), lambda i: (jnp.maximum(i - half, 0), 0))
    return pl.pallas_call(
        functools.partial(expert_kernel, row_part=row_part, cot_part=cot_part),
        out_shape=(narrow, narrow, narrow, made((4, rows, part), BF16)),
        grid=(steps,),
        in_specs=[
            SMEM,
            pl.BlockSpec((block, row_rest), lambda i: (i, 0)),
            pl.BlockSpec((block, cot_rest), lambda i: (i, row_rest // cot_rest)),
            *([top, bottom] * 4),
            *(whole(a.shape) for a in (w_gate, w_up, w_down, fold_gate, fold_up)),
        ],
        out_specs=[mine, mine, mine, pl.BlockSpec((4, block, part), lambda i: (0, i, 0))],
        compiler_params=params(30),
        cost_estimate=cost(7 * 10**9, 18 * 2**20),
        name="expert",
    )(position, *kept([got, got]), *pieces, *kept([w_gate, w_up, w_down, fold_gate, fold_up]))


def grads_kernel(where_ref, got_rows, got_cot, *refs, row_part, cot_part):
    pieces = refs[:8]
    hidden, gate_cot, up_cot, out_gate, out_up, out_down = refs[8:]
    at = where_ref[0]
    first = ((0,), (0,))
    rows = got_rows[...]
    out_gate[0, 4 * row_part :, :] = dot(rows, gate_cot[...], first)
    out_up[0, 4 * row_part :, :] = dot(rows, up_cot[...], first)
    out_down[0, :, 4 * cot_part :] = dot(hidden[...], got_cot[...], first)
    for n, step in enumerate(ring_steps):
        group = lax.rem(at + step, 4)
        top, bottom = pieces[2 * n], pieces[2 * n + 1]
        half = top.shape[0]
        lines = pl.ds(pl.multiple_of(group * row_part, row_part), row_part)
        columns = pl.ds(pl.multiple_of(group * cot_part, 128), cot_part)
        for cot, out in ((gate_cot, out_gate), (up_cot, out_up)):
            out[0, lines, :] = dot(top[:, :row_part], cot[:half, :], first) + dot(
                bottom[:, :row_part], cot[half:, :], first
            )
        out_down[0, :, columns] = dot(hidden[:half, :], top[:, row_part:], first) + dot(
            hidden[half:, :], bottom[:, row_part:], first
        )


def grads(position, got, pieces, hidden, gate_cot, up_cot, width, row_part, cot_part):
    rows, units = hidden.shape
    row_rest, cot_rest = width - 4 * row_part, width - 4 * cot_part
    outs = (
        made((1, width, units), F32),
        made((1, width, units), F32),
        made((1, units, width), F32),
    )
    tail = (*pieces, hidden, gate_cot, up_cot)
    return pl.pallas_call(
        functools.partial(grads_kernel, row_part=row_part, cot_part=cot_part),
        out_shape=outs,
        grid=(1,),
        in_specs=[
            SMEM,
            pl.BlockSpec((rows, row_rest), lambda i: (0, 0), pipeline_mode=pl.Buffered(1)),
            pl.BlockSpec(
                (rows, cot_rest), lambda i: (0, row_rest // cot_rest), pipeline_mode=pl.Buffered(1)
            ),
            *(whole(a.shape) for a in tail),
        ],
        out_specs=[whole(o.shape) for o in outs],
        compiler_params=params(30),
        cost_estimate=cost(4 * 10**9, 17 * 2**20),
        name="grads",
    )(position, *kept([got, got]), *pieces, *kept(tail[len(pieces) :]))


def proj_kernel(where_ref, gate_cot, up_cot, w_gate, w_up, local, *refs):
    pieces, out = refs[:-1], refs[-1]
    at = where_ref[0]
    core = where_ref[1]
    first = ((0,), (0,))
    for n, step in enumerate(ring_steps):
        group = lax.rem(at + step, 4)
        top, bottom = pieces[2 * n], pieces[2 * n + 1]
        half = top.shape[0]
        push_gate, push_up = (
            (dot(cot[:half, :], top[...], first) + dot(cot[half:, :], bottom[...], first)).astype(BF16)
            for cot in (gate_cot, up_cot)
        )
        term = dot(w_gate[...], push_gate) + dot(w_up[...], push_up)
        if step == 0:
            term = term + local[...]
        term = term.astype(BF16)
        lines = out.shape[3]
        for s in range(2 * out.shape[2]):
            slot = lax.rem(s % 2 + core, 2)
            out[slot, group, s // 2] = term[s * lines : (s + 1) * lines, :]


def proj(position, gate_cot, up_cot, w_gate, w_up, local, pieces, lines):
    width, part = w_gate.shape[0], pieces[0].shape[1]
    args = (position, gate_cot, up_cot, w_gate, w_up, local, *pieces)
    out = made((2, 4, width // lines // 2, lines, part), BF16)
    return pl.pallas_call(
        proj_kernel,
        out_shape=out,
        in_specs=[SMEM] + [whole(a.shape) for a in args[1:]],
        out_specs=whole(out.shape),
        compiler_params=params(22),
        cost_estimate=cost(4 * 10**9, 14 * 2**20),
        name="proj",
    )(position, *kept(args[1:6]), *pieces)


def scan_kernel(back, sel, base, act, b, decay, seg, block, out_grad, out_local, out_pair, drive, part):
    tokens, channels = base.shape
    length = tokens // 8
    mix = base[...]
    total = back[0].astype(F32) + back[1].astype(F32) + back[2].astype(F32) + back[3].astype(F32)
    mix = mix + dot(sel[...], total.astype(BF16))
    out_grad[...] = (mix * b[...]).astype(BF16)
    push = mix * act[...]
    for h in range(channels // 128):
        cols = slice(h * 128, (h + 1) * 128)
        drive[h] = push[:, cols]
        value = drive[h, pl.ds(length - 1, 8, stride=length), :]
        part[h, pl.ds(length - 1, 8, stride=length), :] = value
        for i in range(length - 2, -1, -1):
            value = (
                drive[h, pl.ds(i, 8, stride=length), :]
                + decay[h, pl.ds(i + 1, 8, stride=length), :] * value
            )
            part[h, pl.ds(i, 8, stride=length), :] = value
        lead = decay[h, pl.ds(0, 8, stride=length), :]
        inner = seg[h, pl.ds(0, 8, stride=length), :]
        carry = jnp.zeros((1, 128), F32)
        for k in range(7, -1, -1):
            rows = slice(k * length, (k + 1) * length)
            out_local[rows, cols] = part[h, rows, :] + seg[h, rows, :] * carry
            one = slice(k, k + 1)
            carry = lead[one, :] * (value[one, :] + inner[one, :] * carry)
        out_pair[:, cols] = jnp.concatenate([carry, block[0:1, cols]], axis=0)


def scanned(back, sel, base, act, b, decay, seg, block):
    tokens, channels = base.shape
    args = (back, sel, base, act, b, decay, seg, block)
    outs = (
        made((tokens, channels), BF16),
        made((tokens, channels), F32),
        made((2, channels), F32),
    )
    return pl.pallas_call(
        scan_kernel,
        out_shape=outs,
        in_specs=[whole(a.shape) for a in args],
        out_specs=[whole(o.shape) for o in outs],
        scratch_shapes=[pltpu.VMEM(decay.shape, F32), pltpu.VMEM(decay.shape, F32)],
        compiler_params=params(14),
        cost_estimate=cost(4 * 10**8, 8 * 2**20),
        name="scanned",
    )(back, *kept(args[1:]))


def final_kernel(where_ref, carry, local, exp, ca, ci, cs, map_a, map_i, out):
    channels = local.shape[1]
    heads = channels // 128
    first = where_ref[0] * heads
    for h in range(heads):
        cols = slice(h * 128, (h + 1) * 128)
        cot = local[:, cols] + exp[:, cols] * carry[0:1, cols]
        a_cot = (cot * ca[:, cols]).astype(BF16)
        i_cot = (cot * ci[:, cols]).astype(BF16)
        total = (
            cot * cs[:, cols]
            + dot(a_cot, map_a[first + h], ((1,), (1,)))
            + dot(i_cot, map_i[first + h], ((1,), (1,)))
        )
        out[:, cols] = total.astype(BF16)


def final(position, carry, local, exp, ca, ci, cs, map_a, map_i):
    args = (position, carry, local, exp, ca, ci, cs, map_a, map_i)
    return pl.pallas_call(
        final_kernel,
        out_shape=made(local.shape, BF16),
        in_specs=[SMEM] + [whole(a.shape) for a in args[1:]],
        out_specs=whole(local.shape),
        compiler_params=params(8),
        cost_estimate=cost(10**8, 4 * 2**20),
        name="final",
    )(position, carry, *kept(args[2:]))


def shifted(piece, by):
    return lax.ppermute(piece, "tp", [(i, (i + by) % 4) for i in range(4)])


def ring_gather(top, bottom):
    left_top, right_bottom = shifted(top, 1), shifted(bottom, -1)
    left_bottom, right_top = shifted(bottom, 1), shifted(top, -1)
    far_top, far_bottom = shifted(left_top, 1), shifted(right_bottom, -1)
    return top, bottom, left_top, left_bottom, right_top, right_bottom, far_top, far_bottom


def later(pair, by, length):
    return lax.ppermute(pair, ("sq", "core"), [(i, i - by) for i in range(by, length)])


def joined(near, far):
    return jnp.stack([near[0] + near[1] * far[0], near[1] * far[1]])


def carried(pair, length):
    one, two, three, four = (later(pair, by, length) for by in (1, 2, 3, 4))
    pair = joined(joined(one, two), joined(three, four))
    one, two, three = (later(pair, by, length) for by in (4, 8, 12))
    pair = joined(joined(pair, one), joined(two, three))
    return joined(pair, later(pair, 16, length))


def per_device(
    layer_input, out_cot, expert_ids, route_weight, w_gate, w_up, w_down, out_proj,
    rec_input, gate_input, prev_state, decay_param, extra_decay, gate_a_w, gate_i_w,
):
    sources = lax.axis_size("sq") * lax.axis_size("core")
    tp = lax.axis_index("tp")
    core = lax.axis_index("core")
    sp_axes = ("sq", "core")
    position = jnp.stack([tp, core]).astype(jnp.int32)
    w_gate, w_up, w_down = w_gate[0], w_up[0], w_down[0]
    tokens, width = layer_input.shape
    capacity = 5 * tokens * expert_ids.shape[1] // (4 * sources)
    slots = sources * capacity
    row_part, cot_part = width // 8, 3 * width // 16
    row_rest, cot_rest = width - 4 * row_part, width - 4 * cot_part
    ids, weight = expert_ids.T, route_weight.T

    def exchanged(rows):
        return lax.all_to_all(
            rows.reshape(sources, capacity, -1), sp_axes, 0, 0, tiled=True
        ).reshape(rows.shape)

    spread = build(
        position, ids, weight,
        [(layer_input, row_part, None, False), (out_cot, cot_part, None, True)],
        capacity, sources,
    )
    spread = exchanged(spread)
    half = out_proj.shape[0] // 2
    projections = ring_gather(out_proj[:half], out_proj[half:])
    fold_gate, fold_up = folded_weights(position, w_gate, w_up, projections)
    rates = (decay_factor * jax.nn.softplus(-decay_param)).reshape(-1, gate_a_w.shape[1])
    rec_output, act, b, ca, ci, cs, decay, seg, exp, block, sel = early(
        position, expert_ids, rec_input, gate_input, prev_state, rates, extra_decay.T,
        gate_a_w, gate_i_w, capacity, sources,
    )
    direct = build(
        position, ids, weight,
        [
            (layer_input, row_rest, 4 * row_part // row_rest, False),
            (out_cot, cot_rest, 4 * cot_part // cot_rest, True),
            (rec_output, rec_output.shape[1], 0, False),
        ],
        capacity, sources,
    )
    got = exchanged(direct)
    pieces = ring_gather(spread[: slots // 2], spread[slots // 2 :])
    base = jnp.dot(out_cot, out_proj, preferred_element_type=F32)
    local_proj = lax.dot_general(
        out_cot, rec_output, (((0,), (0,)), ((), ())), preferred_element_type=F32
    )
    hidden, gate_cot, up_cot, mix = expert(
        position, got, pieces, w_gate, w_up, w_down, fold_gate, fold_up, row_part, cot_part
    )
    back = lax.all_to_all(
        mix.reshape(4 * sources, capacity, -1), ("tp", *sp_axes), 0, 0, tiled=True
    ).reshape(mix.shape)
    grad_gate, grad_up, grad_down = grads(
        position, got, pieces, hidden, gate_cot, up_cot, width, row_part, cot_part
    )
    start = row_rest + cot_rest
    recs = ring_gather(got[: slots // 2, start:], got[slots // 2 :, start:])
    lines = width // sources
    parts = proj(position, gate_cot, up_cot, w_gate, w_up, local_proj, recs, lines)
    other = lax.ppermute(parts[1], "core", [(0, 1), (1, 0)])
    chip = (parts[0].astype(F32) + other.astype(F32)).astype(BF16)
    arrived = lax.all_to_all(
        chip.reshape(4 * chip.shape[1], lines, -1), ("tp", "sq"), 0, 0, tiled=True
    )
    grad_out_proj = arrived.astype(F32).sum(axis=0)
    gate_input_grad, local, pair = scanned(back, sel, base, act, b, decay, seg, block)
    carry = carried(pair, sources)
    rec_input_grad = final(position, carry, local, exp, ca, ci, cs, gate_a_w, gate_i_w)
    return (grad_gate, grad_up, grad_down, grad_out_proj, rec_input_grad, gate_input_grad)


def solution(mesh):
    sp, tp = mesh.devices.shape
    inner = Mesh(mesh.devices.reshape(sp // 2, 2, tp), ("sq", "core", "tp"))
    sp = ("sq", "core")
    in_specs = (
        P(sp, None),
        P(sp, None),
        P(sp, None),
        P(sp, None),
        P(sp, None, "tp"),
        P(sp, None, "tp"),
        P(sp, "tp", None),
        P(None, "tp"),
        P(sp, "tp"),
        P(sp, "tp"),
        P(sp, "tp"),
        P(),
        P("tp", sp),
        P(),
        P(),
    )
    out_specs = (
        P(sp, None, "tp"),
        P(sp, None, "tp"),
        P(sp, "tp", None),
        P(sp, "tp"),
        P(sp, "tp"),
        P(sp, "tp"),
    )
    return jax.shard_map(
        per_device, mesh=inner, in_specs=in_specs, out_specs=out_specs, check_vma=False
    )
```

profile of v0, /device:TPU:1, one launch (start us, length us, event | category | flops | bytes accessed | tf_op | source)
XLA Modules:
  0.0 272.6 jit_solution(3082798533846405972)
XLA Ops:
  0.7 6.4 %shard_map.191 = bf16[1280,640]{1,0:T(8,128)(2,1)} custom-call(s32[2]{0:T(128)S(1)} %pad_add_fusion.where_ref, s32[2,512]{1,0:T(2,128)} %bitcast.45, f32[2,512]{1,0:T(2,128)} %bitcast.47, bf16[512,2048]{1,0:T(8,128)(2,1)} %refs_0_.3, bf16[512,2048]{1,0:T(8,128)(2,1)} %refs_1_.3), custom_call_target="tpu_custom_call" | custom-call | flops 896000000 | bytes 3200000 | tf_op jit(solution)/shard_map/pallas_call | solution.py:185
  7.1 9.7 %all-to-all-start.1 = ((bf16[32,40,640]{2,1,0:T(8,128)(2,1)}), bf16[32,40,640]{2,1,0:T(8,128)(2,1)S(1)}, u32[]{:S(2)}, u32[]{:S(2)}) async-start(bf16[32,40,640]{2,1,0:T(8,128)(2,1)} %bitcast.41), calls=%async_computation.1 | async-start | bytes 3276800 | tf_op jit(solution)/shard_map/all_to_all | solution.py:507
  16.8 0.9 copy.22.ids
  17.7 0.9 copy.21
  19.2 6.4 %early.1 = (bf16[512,256]{1,0:T(8,128)(2,1)}, f32[512,256]{1,0:T(8,128)}, f32[512,256]{1,0:T(8,128)}, f32[512,256]{1,0:T(8,128)}, f32[512,256]{1,0:T(8,128)}, /*...) custom-call(s32[2]{0:T(128)S(1)} %pad_add_fusion.where_ref, ...), custom_call_target="tpu_custom_call" | custom-call | flops 3000000000 | bytes 8388608 | tf_op jit(solution)/shard_map/early/pallas_call | solution.py:131
  25.6 7.9 %shard_map.190 = bf16[1280,1792]{1,0:T(8,128)(2,1)} custom-call(s32[2]{0:T(128)S(1)} %pad_add_fusion.where_ref, s32[2,512]{1,0:T(2,128)} %bitcast.46, f32[2,512]{1,0:T(2,128)} %bitcast.48, bf16[512,2048]{1,0:T(8,128)(2,1)} %refs_0_.3, bf16[512,2048]{1,0:T(8,128)(2,1)} %refs_1_.3, bf16[512,256]{1,0:T(8,128)(2,1)} %get-tuple-element.29.refs_2_), custom_call_target="tpu_custom_call" | custom-call | flops 2508800000 | bytes 8960000 | tf_op jit(solution)/shard_map/pallas_call | solution.py:185
  33.5 6.9 %all-to-all-done.1 = bf16[32,40,640]{2,1,0:T(8,128)(2,1)S(1)} async-done(((bf16[32,40,640]{2,1,0:T(8,128)(2,1)}), bf16[32,40,640]{2,1,0:T(8,128)(2,1)S(1)}, u32[]{:S(2)}, u32[]{:S(2)}) %all-to-all-start.1) | async-done | bytes 1638432 | tf_op jit(solution)/shard_map/all_to_all | solution.py:507
  40.4 5.8 %all-to-all-start = ((bf16[32,40,1792]{2,1,0:T(8,128)(2,1)}), bf16[32,40,1792]{2,1,0:T(8,128)(2,1)}, u32[]{:S(2)}, u32[]{:S(2)}) async-start(bf16[32,40,1792]{2,1,0:T(8,128)(2,1)} %bitcast.42), calls=%async_computation | async-start | bytes 9175040 | tf_op jit(solution)/shard_map/all_to_all | solution.py:507
  46.2 1.3 fusion.16
  47.5 1.3 collective-permute-start.6
  48.8 1.5 collective-permute-start.9
  50.5 2.7 collective-permute-start.3
  53.2 8.8 %collective-permute-done.6.refs_2_ = bf16[1024,256]{1,0:T(8,128)(2,1)S(1)} collective-permute-done((bf16[1024,256]{1,0:T(8,128)(2,1)S(1)}, bf16[1024,256]{1,0:T(8,128)(2,1)S(1)}, u32[]{:S(2)}, u32[]{:S(2)}) %collective-permute-start.6) | collective-permute-done | bytes 524320 | tf_op jit(solution)/shard_map/ppermute | solution.py:463
  61.9 1.3 collective-permute-start.8
  64.2 26.5 %collective-permute-done.7.refs_3_ = bf16[1024,256]{1,0:T(8,128)(2,1)S(1)} collective-permute-done((bf16[1024,256]{1,0:T(8,128)(2,1)S(1)}, bf16[1024,256]{1,0:T(8,128)(2,1)S(1)}, u32[]{:S(2)}, u32[]{:S(2)}) %collective-permute-start.7) | collective-permute-done | bytes 524320 | tf_op jit(solution)/shard_map/ppermute | solution.py:463
  91.6 0.8 copy-done.14
  92.4 2.7 collective-permute-start.11
  95.0 6.9 %collective-permute-done.10.refs_6_ = bf16[1024,256]{1,0:T(8,128)(2,1)S(1)} collective-permute-done((bf16[1024,256]{1,0:T(8,128)(2,1)S(1)}, bf16[1024,256]{1,0:T(8,128)(2,1)S(1)}, u32[]{:S(2)}, u32[]{:S(2)}) %collective-permute-start.10) | collective-permute-done | bytes 524320 | tf_op jit(solution)/shard_map/ppermute | solution.py:463
  102.0 0.8 copy-done.16
  102.8 1.3 collective-permute-start.2
  104.3 2.5 collective-permute-start.5
  106.8 2.3 convolution_bitcast_fusion.local
  109.1 2.0 fusion.14
  111.1 8.5 %collective-permute-done.1.refs_3_ = bf16[640,640]{1,0:T(8,128)(2,1)} collective-permute-done((bf16[640,640]{1,0:T(8,128)(2,1)S(1)}, bf16[640,640]{1,0:T(8,128)(2,1)}, u32[]{:S(2)}, u32[]{:S(2)}) %collective-permute-start.1) | collective-permute-done | bytes 819232 | tf_op jit(solution)/shard_map/ppermute | solution.py:463
  119.5 1.3 collective-permute-start.15
  120.8 1.0 copy-done.7
  121.8 1.0 copy-done.9
  122.9 1.0 copy-done.11
  123.9 1.0 copy-done.13
  125.0 1.0 copy-done.15
  126.0 1.0 copy-done.17
  127.1 5.2 %folded.1 = (bf16[4,256,256]{2,1,0:T(8,128)(2,1)}, bf16[4,256,256]{2,1,0:T(8,128)(2,1)}) custom-call(s32[2]{0:T(128)S(1)} %pad_add_fusion.where_ref, bf16[2048,256]{1,0:T(8,128)(2,1)} %bitcast.50, bf16[2048,256]{1,0:T(8,128)(2,1)} %bitcast.53, bf16[1024,256]{1,0:T(8,128)(2,1)S(1)} %copy-done.9, bf16[1024,256]{1,0:T(8,128)(2,1)S(1)} %copy-done.7, ...), custom_call_target="tpu_custom_call" | custom-call | flops 4000000000 | bytes 7340032 | tf_op jit(solution)/shard_map/folded/pallas_call | solution.py:224
  132.5 4.6 %collective-permute-done.4.refs_6_ = bf16[640,640]{1,0:T(8,128)(2,1)} collective-permute-done((bf16[640,640]{1,0:T(8,128)(2,1)S(1)}, bf16[640,640]{1,0:T(8,128)(2,1)}, u32[]{:S(2)}, u32[]{:S(2)}) %collective-permute-start.4) | collective-permute-done | bytes 819232 | tf_op jit(solution)/shard_map/ppermute | solution.py:463
  137.1 1.3 collective-permute-start.14
  138.4 5.8 %collective-permute-done.12.refs_2_ = bf16[640,256]{1,0:T(8,128)(2,1)} collective-permute-done((bf16[640,256]{1,0:T(8,128)(2,1)}, bf16[640,256]{1,0:T(8,128)(2,1)}, u32[]{:S(2)}, u32[]{:S(2)}) %collective-permute-start.12) | collective-permute-done | bytes 327712 | tf_op jit(solution)/shard_map/ppermute | solution.py:463
  144.1 3.1 %collective-permute-done.15.refs_5_ = bf16[640,256]{1,0:T(8,128)(2,1)} collective-permute-done((bf16[640,256]{1,0:T(8,128)(2,1)}, bf16[640,256]{1,0:T(8,128)(2,1)}, u32[]{:S(2)}, u32[]{:S(2)}) %collective-permute-start.15) | collective-permute-done | bytes 327712 | tf_op jit(solution)/shard_map/ppermute | solution.py:463
  147.3 3.0 %collective-permute-start.17 = (bf16[640,256]{1,0:T(8,128)(2,1)}, bf16[640,256]{1,0:T(8,128)(2,1)}, u32[]{:S(2)}, u32[]{:S(2)}) collective-permute-start(bf16[640,256]{1,0:T(8,128)(2,1)} %collective-permute-done.15.refs_5_), channel_id=1, source_target_pairs={{0,3},{1,0},{2,1},{3,2},{4,7},{5,4},{6,5},{7,6},{8,11},{9,8},{10,9... | collective-permute-start | bytes 983048 | tf_op jit(solution)/shard_map/ppermute | solution.py:463
  150.3 13.8 %expert.1 = (bf16[1280,256]{1,0:T(8,128)(2,1)}, bf16[1280,256]{1,0:T(8,128)(2,1)}, bf16[1280,256]{1,0:T(8,128)(2,1)}, bf16[4,1280,256]{2,1,0:T(8,128)(2,1)}) custom-call(s32[2]{0:T(128)S(1)} %pad_add_fusion.where_ref, bf16[1280,1792]{1,0:T(8,128)(2,1)} %bitcast.7.got_rows.got_cot, bf16[1280,1792]{1,0:T(8,128)(2,1)} %bitcast.7.got_rows.got_cot, ...), custom_call_target="tpu_custom_call" | custom-call | flops 7000000000 | bytes 18874368 | tf_op jit(solution)/shard_map/expert/pallas_call | solution.py:274
  164.1 12.1 %all-to-all-start.3 = ((bf16[128,40,256]{2,1,0:T(8,128)(2,1)}), bf16[128,40,256]{2,1,0:T(8,128)(2,1)S(1)}, u32[]{:S(2)}, u32[]{:S(2)}) async-start(bf16[128,40,256]{2,1,0:T(8,128)(2,1)} %bitcast.43), calls=%async_computation.3 | async-start | bytes 5242880 | tf_op jit(solution)/shard_map/all_to_all | solution.py:543
  176.2 9.6 %proj.1 = bf16[2,4,16,64,256]{4,3,2,1,0:T(8,128)(2,1)} custom-call(s32[2]{0:T(128)S(1)} %pad_add_fusion.where_ref, bf16[1280,256]{1,0:T(8,128)(2,1)} %get-tuple-element.33.refs_9_.gate_cot, bf16[1280,256]{1,0:T(8,128)(2,1)} %get-tuple-element.34.refs_10_.up_cot, bf16[2048,256]{1,0:T(8,128)(2,1)} %bitcast.52, bf16[2048,256]{1,0:T(8,128)(2,1)} %bitcast.55, ...), custom_call_target="tpu_custom_call" | custom-call | flops 4000000000 | bytes 14680064 | tf_op jit(solution)/shard_map/proj/pallas_call | solution.py:371
  185.8 1.9 slice_bitcast_fusion
  187.7 1.1 collective-permute-start.18
  188.9 3.8 %collective-permute-done.18 = bf16[4,16,64,256]{3,2,1,0:T(8,128)(2,1)S(1)} collective-permute-done((bf16[4,16,64,256]{3,2,1,0:T(8,128)(2,1)S(1)}, bf16[4,16,64,256]{3,2,1,0:T(8,128)(2,1)S(1)}, u32[]{:S(2)}, u32[]{:S(2)}) %collective-permute-start.18) | collective-permute-done | bytes 2097184 | tf_op jit(solution)/shard_map/ppermute | solution.py:553
  192.6 2.2 fusion
  194.8 17.2 %all-to-all-done.3 = bf16[128,40,256]{2,1,0:T(8,128)(2,1)S(1)} async-done(((bf16[128,40,256]{2,1,0:T(8,128)(2,1)}), bf16[128,40,256]{2,1,0:T(8,128)(2,1)S(1)}, u32[]{:S(2)}, u32[]{:S(2)}) %all-to-all-start.3) | async-done | bytes 2621472 | tf_op jit(solution)/shard_map/all_to_all | solution.py:543
  212.1 5.8 %all-to-all-start.2 = ((bf16[64,64,256]{2,1,0:T(8,128)(2,1)}), bf16[64,64,256]{2,1,0:T(8,128)(2,1)}, u32[]{:S(2)}, u32[]{:S(2)}) async-start(bf16[64,64,256]{2,1,0:T(8,128)(2,1)} %bitcast.40), calls=%async_computation.2 | async-start | bytes 4194304 | tf_op jit(solution)/shard_map/all_to_all | solution.py:555
  217.9 3.4 %fusion.17.base = f32[512,256]{1,0:T(8,128)} fusion(bf16[512,2048]{1,0:T(8,128)(2,1)} %refs_1_.3, bf16[2048,256]{1,0:T(8,128)(2,1)} %param.22), kind=kOutput, calls=%fused_computation.37 | convolution fusion | flops 536870912 | bytes 3670016 | tf_op jit(solution)/shard_map/dot_general | solution.py:536
  221.2 4.6 %scanned.1 = (bf16[512,256]{1,0:T(8,128)(2,1)}, f32[512,256]{1,0:T(8,128)}, f32[2,256]{1,0:T(2,128)}) custom-call(bf16[4,1280,256]{2,1,0:T(8,128)(2,1)S(1)} %bitcast.31, bf16[512,1280]{1,0:T(8,128)(2,1)} %get-tuple-element.39.sel, f32[512,256]{1,0:T(8,128)} %fusion.17.base, f32[512,256]{1,0:T(8,128)} %get-tuple-element.40.act, ...), custom_call_target="tpu_custom_call" | custom-call | flops 400000000 | bytes 8388608 | tf_op jit(solution)/shard_map/scanned/pallas_call | solution.py:420
  225.9 3.1 %collective-permute-start.19 = (f32[2,256]{1,0:T(2,128)}, f32[2,256]{1,0:T(2,128)S(1)}, u32[]{:S(2)}, u32[]{:S(2)}) collective-permute-start(f32[2,256]{1,0:T(2,128)} %get-tuple-element.45), channel_id=1, source_target_pairs={{4,0},{8,4},{12,8},{16,12},{20,16},{24,20},{28,24},{32,28},{36,32}... | collective-permute-start | bytes 6152 | tf_op jit(solution)/shard_map/ppermute | solution.py:474
  228.9 1.3 collective-permute-start.20
  230.2 1.3 collective-permute-start.21
  231.5 1.3 collective-permute-start.22
  232.8 4.3 %collective-permute-done.19 = f32[2,256]{1,0:T(2,128)S(1)} collective-permute-done((f32[2,256]{1,0:T(2,128)}, f32[2,256]{1,0:T(2,128)S(1)}, u32[]{:S(2)}, u32[]{:S(2)}) %collective-permute-start.19) | collective-permute-done | bytes 2080 | tf_op jit(solution)/shard_map/ppermute | solution.py:474
  237.2 4.3 %collective-permute-done.21 = f32[2,256]{1,0:T(2,128)S(1)} collective-permute-done((f32[2,256]{1,0:T(2,128)}, f32[2,256]{1,0:T(2,128)S(1)}, u32[]{:S(2)}, u32[]{:S(2)}) %collective-permute-start.21) | collective-permute-done | bytes 2080 | tf_op jit(solution)/shard_map/ppermute | solution.py:474
  241.5 1.3 collective-permute-start.23
  242.8 1.3 collective-permute-start.24
  244.1 1.3 collective-permute-start.25
  245.4 2.3 collective-permute-done.23
  247.8 2.4 collective-permute-done.24
  250.2 4.7 %collective-permute-done.25 = f32[2,256]{1,0:T(2,128)S(1)} collective-permute-done((f32[2,256]{1,0:T(2,128)S(1)}, f32[2,256]{1,0:T(2,128)S(1)}, u32[]{:S(2)}, u32[]{:S(2)}) %collective-permute-start.25) | collective-permute-done | bytes 2080 | tf_op jit(solution)/shard_map/ppermute | solution.py:474
  254.9 1.3 collective-permute-start.26
  256.2 10.9 %grads.1 = (f32[1,2048,256]{2,1,0:T(8,128)}, f32[1,2048,256]{2,1,0:T(8,128)}, f32[1,256,2048]{2,1,0:T(8,128)}) custom-call(s32[2]{0:T(128)S(1)} %pad_add_fusion.where_ref, bf16[1280,1792]{1,0:T(8,128)(2,1)} %bitcast.7.got_rows.got_cot, bf16[1280,1792]{1,0:T(8,128)(2,1)} %bitcast.7.got_rows.got_cot, bf16[640,640]{1,0:T(8,128)(2,1)S(1)} %bitcast.39, ...), custom_call_target="tpu_custom_call" | custom-call | flops 4000000000 | bytes 17825792 | tf_op jit(solution)/shard_map/grads/pallas_call | solution.py:325
  267.2 2.9 %final.1 = bf16[512,256]{1,0:T(8,128)(2,1)} custom-call(s32[2]{0:T(128)S(1)} %pad_add_fusion.where_ref, f32[2,256]{1,0:T(2,128)S(1)} %pad_maximum_fusion.2.carry, f32[512,256]{1,0:T(8,128)} %get-tuple-element.46.local, f32[512,256]{1,0:T(8,128)} %get-tuple-element.47.exp, f32[512,256]{1,0:T(8,128)} %get-tuple-element.48.ca, ...), custom_call_target="tpu_custom_call" | custom-call | flops 100000000 | bytes 4194304 | tf_op jit(solution)/shard_map/final/pallas_call | solution.py:451
  270.1 2.5 convert_reduce_fusion
  (73 shorter events, 3.3 us)
Async XLA Ops:
  7.1 9.7 %copy-start.21 = (s32[512,2]{0,1:T(2,128)S(1)}, s32[512,2]{0,1:T(2,128)}, u32[]{:S(2)}) copy-start(s32[512,2]{0,1:T(2,128)} %param.17) | copy-start | bytes 12292
  7.1 10.6 %copy-start.22 = (f32[2,512]{1,0:T(2,128)S(1)}, f32[2,512]{1,0:T(2,128)}, u32[]{:S(2)}) copy-start(f32[2,512]{1,0:T(2,128)} %param.27) | copy-start | bytes 12292
  7.1 11.5 %copy-start.23 = (f32[1024]{0:T(1024)S(1)}, f32[1024]{0:T(1024)}, u32[]{:S(2)}) copy-start(f32[1024]{0:T(1024)} %param.26) | copy-start | bytes 12292
  7.1 33.3 %all-to-all-start.1 = ((bf16[32,40,640]{2,1,0:T(8,128)(2,1)}), bf16[32,40,640]{2,1,0:T(8,128)(2,1)S(1)}, u32[]{:S(2)}, u32[]{:S(2)}) async-start(bf16[32,40,640]{2,1,0:T(8,128)(2,1)} %bitcast.41), calls=%async_computation.1 | async-start | bytes 3276800 | tf_op jit(solution)/shard_map/all_to_all | solution.py:507
  40.4 68.7 %all-to-all-start = ((bf16[32,40,1792]{2,1,0:T(8,128)(2,1)}), bf16[32,40,1792]{2,1,0:T(8,128)(2,1)}, u32[]{:S(2)}, u32[]{:S(2)}) async-start(bf16[32,40,1792]{2,1,0:T(8,128)(2,1)} %bitcast.42), calls=%async_computation | async-start | bytes 9175040 | tf_op jit(solution)/shard_map/all_to_all | solution.py:507
  47.5 56.8 %copy-start.6 = (bf16[1024,256]{1,0:T(8,128)(2,1)}, bf16[1024,256]{1,0:T(8,128)(2,1)S(1)}, u32[]{:S(2)}) copy-start(bf16[1024,256]{1,0:T(8,128)(2,1)S(1)} %get-tuple-element.56.refs_1_) | copy-start | bytes 1572868
  47.5 59.4 %copy-start.8 = (bf16[1024,256]{1,0:T(8,128)(2,1)}, bf16[1024,256]{1,0:T(8,128)(2,1)S(1)}, u32[]{:S(2)}) copy-start(bf16[1024,256]{1,0:T(8,128)(2,1)S(1)} %get-tuple-element.57.refs_0_) | copy-start | bytes 1572868
  47.5 59.4 %copy-start.18 = (bf16[512,2048]{1,0:T(8,128)(2,1)S(1)}, bf16[512,2048]{1,0:T(8,128)(2,1)}, u32[]{:S(2)}) copy-start(bf16[512,2048]{1,0:T(8,128)(2,1)} %refs_1_.3) | copy-start | bytes 6291460
  47.5 59.4 %copy-start.20 = (bf16[512,256]{1,0:T(8,128)(2,1)S(1)}, bf16[512,256]{1,0:T(8,128)(2,1)}, u32[]{:S(2)}) copy-start(bf16[512,256]{1,0:T(8,128)(2,1)} %get-tuple-element.29.refs_2_) | copy-start | bytes 786436
  47.5 14.5 %collective-permute-start.6 = (bf16[1024,256]{1,0:T(8,128)(2,1)S(1)}, bf16[1024,256]{1,0:T(8,128)(2,1)S(1)}, u32[]{:S(2)}, u32[]{:S(2)}) collective-permute-start(bf16[1024,256]{1,0:T(8,128)(2,1)S(1)} %get-tuple-element.57.refs_0_), channel_id=1, source_target_pairs={{0,1},{1,2},{2,3},{3,0},{4,5},{5,6},{6,7},{7,4},{8,9},{9,10},{10,1... | collective-permute-start | bytes 1572872 | tf_op jit(solution)/shard_map/ppermute | solution.py:463
  48.8 14.4 %collective-permute-start.9 = (bf16[1024,256]{1,0:T(8,128)(2,1)S(1)}, bf16[1024,256]{1,0:T(8,128)(2,1)}, u32[]{:S(2)}, u32[]{:S(2)}) collective-permute-start(bf16[1024,256]{1,0:T(8,128)(2,1)S(1)} %get-tuple-element.56.refs_1_), channel_id=1, source_target_pairs={{0,3},{1,0},{2,1},{3,2},{4,7},{5,4},{6,5},{7,6},{8,11},{9,8},{10,9... | collective-permute-start | bytes 1572872 | tf_op jit(solution)/shard_map/ppermute | solution.py:463
  50.4 99.9 %copy-start = (bf16[16,40,640]{2,1,0:T(8,128)(2,1)}, bf16[16,40,640]{2,1,0:T(8,128)(2,1)S(1)}, u32[]{:S(2)}) copy-start(bf16[16,40,640]{2,1,0:T(8,128)(2,1)S(1)} %get-tuple-element.55) | copy-start | bytes 2457604
  50.4 53.7 %collective-permute-start = (bf16[640,640]{1,0:T(8,128)(2,1)S(1)}, bf16[640,640]{1,0:T(8,128)(2,1)S(1)}, u32[]{:S(2)}, u32[]{:S(2)}) collective-permute-start(bf16[640,640]{1,0:T(8,128)(2,1)S(1)} %bitcast.36), channel_id=1, source_target_pairs={{0,1},{1,2},{2,3},{3,0},{4,5},{5,6},{6,7},{7,4},{8,9},{9,10},{10,1... | collective-permute-start | bytes 2457608 | tf_op jit(solution)/shard_map/ppermute | solution.py:463
  50.5 53.8 %collective-permute-start.3 = (bf16[640,640]{1,0:T(8,128)(2,1)S(1)}, bf16[640,640]{1,0:T(8,128)(2,1)S(1)}, u32[]{:S(2)}, u32[]{:S(2)}) collective-permute-start(bf16[640,640]{1,0:T(8,128)(2,1)S(1)} %bitcast.32), channel_id=1, source_target_pairs={{0,3},{1,0},{2,1},{3,2},{4,7},{5,4},{6,5},{7,6},{8,11},{9,8},{10,9... | collective-permute-start | bytes 2457608 | tf_op jit(solution)/shard_map/ppermute | solution.py:463
  53.1 37.6 %collective-permute-start.7 = (bf16[1024,256]{1,0:T(8,128)(2,1)S(1)}, bf16[1024,256]{1,0:T(8,128)(2,1)S(1)}, u32[]{:S(2)}, u32[]{:S(2)}) collective-permute-start(bf16[1024,256]{1,0:T(8,128)(2,1)S(1)} %get-tuple-element.56.refs_1_), channel_id=1, source_target_pairs={{0,1},{1,2},{2,3},{3,0},{4,5},{5,6},{6,7},{7,4},{8,9},{9,10},{10,1... | collective-permute-start | bytes 1572872 | tf_op jit(solution)/shard_map/ppermute | solution.py:463
  61.9 29.6 %collective-permute-start.8 = (bf16[1024,256]{1,0:T(8,128)(2,1)S(1)}, bf16[1024,256]{1,0:T(8,128)(2,1)S(1)}, u32[]{:S(2)}, u32[]{:S(2)}) collective-permute-start(bf16[1024,256]{1,0:T(8,128)(2,1)S(1)} %get-tuple-element.57.refs_0_), channel_id=1, source_target_pairs={{0,3},{1,0},{2,1},{3,2},{4,7},{5,4},{6,5},{7,6},{8,11},{9,8},{10,9... | collective-permute-start | bytes 1572872 | tf_op jit(solution)/shard_map/ppermute | solution.py:463
  63.2 38.8 %collective-permute-start.10 = (bf16[1024,256]{1,0:T(8,128)(2,1)S(1)}, bf16[1024,256]{1,0:T(8,128)(2,1)S(1)}, u32[]{:S(2)}, u32[]{:S(2)}) collective-permute-start(bf16[1024,256]{1,0:T(8,128)(2,1)S(1)} %collective-permute-done.6.refs_2_), channel_id=1, source_target_pairs={{0,1},{1,2},{2,3},{3,0},{4,5},{5,6},{6,7},{7,4},{8,9},{9,10},{10,1... | collective-permute-start | bytes 1572872 | tf_op jit(solution)/shard_map/ppermute | solution.py:463
  63.4 0.8 copy-start.10
  90.7 0.8 copy-start.12
  91.5 28.0 %collective-permute-start.1 = (bf16[640,640]{1,0:T(8,128)(2,1)S(1)}, bf16[640,640]{1,0:T(8,128)(2,1)}, u32[]{:S(2)}, u32[]{:S(2)}) collective-permute-start(bf16[640,640]{1,0:T(8,128)(2,1)S(1)} %bitcast.33), channel_id=1, source_target_pairs={{0,1},{1,2},{2,3},{3,0},{4,5},{5,6},{6,7},{7,4},{8,9},{9,10},{10,1... | collective-permute-start | bytes 2457608 | tf_op jit(solution)/shard_map/ppermute | solution.py:463
  91.6 0.8 copy-start.14
  92.4 18.7 %collective-permute-start.11 = (bf16[1024,256]{1,0:T(8,128)(2,1)}, bf16[1024,256]{1,0:T(8,128)(2,1)}, u32[]{:S(2)}, u32[]{:S(2)}) collective-permute-start(bf16[1024,256]{1,0:T(8,128)(2,1)} %collective-permute-done.9.refs_5_), channel_id=1, source_target_pairs={{0,3},{1,0},{2,1},{3,2},{4,7},{5,4},{6,5},{7,6},{8,11},{9,8},{10,9... | collective-permute-start | bytes 1572872 | tf_op jit(solution)/shard_map/ppermute | solution.py:463
  102.0 0.8 copy-start.16
  102.8 29.5 %collective-permute-start.2 = (bf16[640,640]{1,0:T(8,128)(2,1)S(1)}, bf16[640,640]{1,0:T(8,128)(2,1)}, u32[]{:S(2)}, u32[]{:S(2)}) collective-permute-start(bf16[640,640]{1,0:T(8,128)(2,1)S(1)} %bitcast.37), channel_id=1, source_target_pairs={{0,3},{1,0},{2,1},{3,2},{4,7},{5,4},{6,5},{7,6},{8,11},{9,8},{10,9... | collective-permute-start | bytes 2457608 | tf_op jit(solution)/shard_map/ppermute | solution.py:463
  104.1 46.2 %copy-start.2 = (bf16[640,640]{1,0:T(8,128)(2,1)}, bf16[640,640]{1,0:T(8,128)(2,1)S(1)}, u32[]{:S(2)}) copy-start(bf16[640,640]{1,0:T(8,128)(2,1)S(1)} %collective-permute-done.refs_2_) | copy-start | bytes 2457604
  104.1 33.0 %collective-permute-start.4 = (bf16[640,640]{1,0:T(8,128)(2,1)S(1)}, bf16[640,640]{1,0:T(8,128)(2,1)}, u32[]{:S(2)}, u32[]{:S(2)}) collective-permute-start(bf16[640,640]{1,0:T(8,128)(2,1)S(1)} %collective-permute-done.refs_2_), channel_id=1, source_target_pairs={{0,1},{1,2},{2,3},{3,0},{4,5},{5,6},{6,7},{7,4},{8,9},{9,10},{10,1... | collective-permute-start | bytes 2457608 | tf_op jit(solution)/shard_map/ppermute | solution.py:463
  104.3 46.0 %copy-start.4 = (bf16[640,640]{1,0:T(8,128)(2,1)}, bf16[640,640]{1,0:T(8,128)(2,1)S(1)}, u32[]{:S(2)}) copy-start(bf16[640,640]{1,0:T(8,128)(2,1)S(1)} %collective-permute-done.3.refs_5_) | copy-start | bytes 2457604
  104.3 45.9 %collective-permute-start.5 = (bf16[640,640]{1,0:T(8,128)(2,1)S(1)}, bf16[640,640]{1,0:T(8,128)(2,1)}, u32[]{:S(2)}, u32[]{:S(2)}) collective-permute-start(bf16[640,640]{1,0:T(8,128)(2,1)S(1)} %collective-permute-done.3.refs_5_), channel_id=1, source_target_pairs={{0,3},{1,0},{2,1},{3,2},{4,7},{5,4},{6,5},{7,6},{8,11},{9,8},{10,9... | collective-permute-start | bytes 2457608 | tf_op jit(solution)/shard_map/ppermute | solution.py:463
  111.1 33.0 %collective-permute-start.12 = (bf16[640,256]{1,0:T(8,128)(2,1)}, bf16[640,256]{1,0:T(8,128)(2,1)}, u32[]{:S(2)}, u32[]{:S(2)}) collective-permute-start(bf16[640,256]{1,0:T(8,128)(2,1)} %get-tuple-element.53.refs_0_), channel_id=1, source_target_pairs={{0,1},{1,2},{2,3},{3,0},{4,5},{5,6},{6,7},{7,4},{8,9},{9,10},{10,1... | collective-permute-start | bytes 983048 | tf_op jit(solution)/shard_map/ppermute | solution.py:463
  119.5 27.7 %collective-permute-start.15 = (bf16[640,256]{1,0:T(8,128)(2,1)}, bf16[640,256]{1,0:T(8,128)(2,1)}, u32[]{:S(2)}, u32[]{:S(2)}) collective-permute-start(bf16[640,256]{1,0:T(8,128)(2,1)} %get-tuple-element.52.refs_1_), channel_id=1, source_target_pairs={{0,3},{1,0},{2,1},{3,2},{4,7},{5,4},{6,5},{7,6},{8,11},{9,8},{10,9... | collective-permute-start | bytes 983048 | tf_op jit(solution)/shard_map/ppermute | solution.py:463
  120.8 1.0 copy-start.7
  121.8 1.0 copy-start.9
  122.9 1.0 copy-start.11
  123.9 1.0 copy-start.13
  125.0 1.0 copy-start.15
  126.0 1.0 copy-start.17
  132.3 43.9 %collective-permute-start.13 = (bf16[640,256]{1,0:T(8,128)(2,1)}, bf16[640,256]{1,0:T(8,128)(2,1)}, u32[]{:S(2)}, u32[]{:S(2)}) collective-permute-start(bf16[640,256]{1,0:T(8,128)(2,1)} %get-tuple-element.52.refs_1_), channel_id=1, source_target_pairs={{0,1},{1,2},{2,3},{3,0},{4,5},{5,6},{6,7},{7,4},{8,9},{9,10},{10,1... | collective-permute-start | bytes 983048 | tf_op jit(solution)/shard_map/ppermute | solution.py:463
  137.1 39.1 %collective-permute-start.14 = (bf16[640,256]{1,0:T(8,128)(2,1)}, bf16[640,256]{1,0:T(8,128)(2,1)}, u32[]{:S(2)}, u32[]{:S(2)}) collective-permute-start(bf16[640,256]{1,0:T(8,128)(2,1)} %get-tuple-element.53.refs_0_), channel_id=1, source_target_pairs={{0,3},{1,0},{2,1},{3,2},{4,7},{5,4},{6,5},{7,6},{8,11},{9,8},{10,9... | collective-permute-start | bytes 983048 | tf_op jit(solution)/shard_map/ppermute | solution.py:463
  144.1 32.1 %collective-permute-start.16 = (bf16[640,256]{1,0:T(8,128)(2,1)}, bf16[640,256]{1,0:T(8,128)(2,1)}, u32[]{:S(2)}, u32[]{:S(2)}) collective-permute-start(bf16[640,256]{1,0:T(8,128)(2,1)} %collective-permute-done.12.refs_2_), channel_id=1, source_target_pairs={{0,1},{1,2},{2,3},{3,0},{4,5},{5,6},{6,7},{7,4},{8,9},{9,10},{10,1... | collective-permute-start | bytes 983048 | tf_op jit(solution)/shard_map/ppermute | solution.py:463
  147.3 28.9 %collective-permute-start.17 = (bf16[640,256]{1,0:T(8,128)(2,1)}, bf16[640,256]{1,0:T(8,128)(2,1)}, u32[]{:S(2)}, u32[]{:S(2)}) collective-permute-start(bf16[640,256]{1,0:T(8,128)(2,1)} %collective-permute-done.15.refs_5_), channel_id=1, source_target_pairs={{0,3},{1,0},{2,1},{3,2},{4,7},{5,4},{6,5},{7,6},{8,11},{9,8},{10,9... | collective-permute-start | bytes 983048 | tf_op jit(solution)/shard_map/ppermute | solution.py:463
  164.1 48.0 %all-to-all-start.3 = ((bf16[128,40,256]{2,1,0:T(8,128)(2,1)}), bf16[128,40,256]{2,1,0:T(8,128)(2,1)S(1)}, u32[]{:S(2)}, u32[]{:S(2)}) async-start(bf16[128,40,256]{2,1,0:T(8,128)(2,1)} %bitcast.43), calls=%async_computation.3 | async-start | bytes 5242880 | tf_op jit(solution)/shard_map/all_to_all | solution.py:543
  185.8 6.8 %copy-start.19 = (bf16[2,4,16,64,256]{4,3,2,1,0:T(8,128)(2,1)S(1)}, bf16[2,4,16,64,256]{4,3,2,1,0:T(8,128)(2,1)}, u32[]{:S(2)}) copy-start(bf16[2,4,16,64,256]{4,3,2,1,0:T(8,128)(2,1)} %proj.1) | copy-start | bytes 12582916
  187.7 4.9 %collective-permute-start.18 = (bf16[4,16,64,256]{3,2,1,0:T(8,128)(2,1)S(1)}, bf16[4,16,64,256]{3,2,1,0:T(8,128)(2,1)S(1)}, u32[]{:S(2)}, u32[]{:S(2)}) collective-permute-start(bf16[4,16,64,256]{3,2,1,0:T(8,128)(2,1)S(1)} %slice_bitcast_fusion), channel_id=1, source_target_pairs={{0,4},{4,0},{1,5},{5,1},{2,6},{6,2},{3,7},{7,3},{8,12},{12,8},{9,1... | collective-permute-start | bytes 6291464 | tf_op jit(solution)/shard_map/ppermute | solution.py:553
  212.1 58.0 %all-to-all-start.2 = ((bf16[64,64,256]{2,1,0:T(8,128)(2,1)}), bf16[64,64,256]{2,1,0:T(8,128)(2,1)}, u32[]{:S(2)}, u32[]{:S(2)}) async-start(bf16[64,64,256]{2,1,0:T(8,128)(2,1)} %bitcast.40), calls=%async_computation.2 | async-start | bytes 4194304 | tf_op jit(solution)/shard_map/all_to_all | solution.py:555
  221.2 35.0 %copy-start.1 = (bf16[16,40,640]{2,1,0:T(8,128)(2,1)S(1)}, bf16[16,40,640]{2,1,0:T(8,128)(2,1)}, u32[]{:S(2)}) copy-start(bf16[16,40,640]{2,1,0:T(8,128)(2,1)} %copy-done) | copy-start | bytes 2457604
  221.2 35.0 %copy-start.3 = (bf16[640,640]{1,0:T(8,128)(2,1)S(1)}, bf16[640,640]{1,0:T(8,128)(2,1)}, u32[]{:S(2)}) copy-start(bf16[640,640]{1,0:T(8,128)(2,1)} %copy-done.2) | copy-start | bytes 2457604
  221.2 35.0 %copy-start.5 = (bf16[640,640]{1,0:T(8,128)(2,1)S(1)}, bf16[640,640]{1,0:T(8,128)(2,1)}, u32[]{:S(2)}) copy-start(bf16[640,640]{1,0:T(8,128)(2,1)} %copy-done.4) | copy-start | bytes 2457604
  225.9 11.3 %collective-permute-start.19 = (f32[2,256]{1,0:T(2,128)}, f32[2,256]{1,0:T(2,128)S(1)}, u32[]{:S(2)}, u32[]{:S(2)}) collective-permute-start(f32[2,256]{1,0:T(2,128)} %get-tuple-element.45), channel_id=1, source_target_pairs={{4,0},{8,4},{12,8},{16,12},{20,16},{24,20},{28,24},{32,28},{36,32}... | collective-permute-start | bytes 6152 | tf_op jit(solution)/shard_map/ppermute | solution.py:474
  228.9 8.2 %collective-permute-start.20 = (f32[2,256]{1,0:T(2,128)}, f32[2,256]{1,0:T(2,128)S(1)}, u32[]{:S(2)}, u32[]{:S(2)}) collective-permute-start(f32[2,256]{1,0:T(2,128)} %get-tuple-element.45), channel_id=1, source_target_pairs={{8,0},{12,4},{16,8},{20,12},{24,16},{28,20},{32,24},{36,28},{40,32... | collective-permute-start | bytes 6152 | tf_op jit(solution)/shard_map/ppermute | solution.py:474
  230.2 11.3 %collective-permute-start.21 = (f32[2,256]{1,0:T(2,128)}, f32[2,256]{1,0:T(2,128)S(1)}, u32[]{:S(2)}, u32[]{:S(2)}) collective-permute-start(f32[2,256]{1,0:T(2,128)} %get-tuple-element.45), channel_id=1, source_target_pairs={{12,0},{16,4},{20,8},{24,12},{28,16},{32,20},{36,24},{40,28},{44,3... | collective-permute-start | bytes 6152 | tf_op jit(solution)/shard_map/ppermute | solution.py:474
  231.5 10.0 %collective-permute-start.22 = (f32[2,256]{1,0:T(2,128)}, f32[2,256]{1,0:T(2,128)S(1)}, u32[]{:S(2)}, u32[]{:S(2)}) collective-permute-start(f32[2,256]{1,0:T(2,128)} %get-tuple-element.45), channel_id=1, source_target_pairs={{16,0},{20,4},{24,8},{28,12},{32,16},{36,20},{40,24},{44,28},{48,3... | collective-permute-start | bytes 6152 | tf_op jit(solution)/shard_map/ppermute | solution.py:474
  241.5 6.2 %collective-permute-start.23 = (f32[2,256]{1,0:T(2,128)S(1)}, f32[2,256]{1,0:T(2,128)S(1)}, u32[]{:S(2)}, u32[]{:S(2)}) collective-permute-start(f32[2,256]{1,0:T(2,128)S(1)} %pad_maximum_fusion), channel_id=1, source_target_pairs={{16,0},{20,4},{24,8},{28,12},{32,16},{36,20},{40,24},{44,28},{48,3... | collective-permute-start | bytes 6152 | tf_op jit(solution)/shard_map/ppermute | solution.py:474
  242.8 7.3 %collective-permute-start.24 = (f32[2,256]{1,0:T(2,128)S(1)}, f32[2,256]{1,0:T(2,128)S(1)}, u32[]{:S(2)}, u32[]{:S(2)}) collective-permute-start(f32[2,256]{1,0:T(2,128)S(1)} %pad_maximum_fusion), channel_id=1, source_target_pairs={{32,0},{36,4},{40,8},{44,12},{48,16},{52,20},{56,24},{60,28},{64,3... | collective-permute-start | bytes 6152 | tf_op jit(solution)/shard_map/ppermute | solution.py:474
  244.1 10.7 %collective-permute-start.25 = (f32[2,256]{1,0:T(2,128)S(1)}, f32[2,256]{1,0:T(2,128)S(1)}, u32[]{:S(2)}, u32[]{:S(2)}) collective-permute-start(f32[2,256]{1,0:T(2,128)S(1)} %pad_maximum_fusion), channel_id=1, source_target_pairs={{48,0},{52,4},{56,8},{60,12},{64,16},{68,20},{72,24},{76,28},{80,3... | collective-permute-start | bytes 6152 | tf_op jit(solution)/shard_map/ppermute | solution.py:474
  254.9 12.3 %collective-permute-start.26 = (f32[2,256]{1,0:T(2,128)S(1)}, f32[2,256]{1,0:T(2,128)S(1)}, u32[]{:S(2)}, u32[]{:S(2)}) collective-permute-start(f32[2,256]{1,0:T(2,128)S(1)} %pad_maximum_fusion.1), channel_id=1, source_target_pairs={{64,0},{68,4},{72,8},{76,12},{80,16},{84,20},{88,24},{92,28},{96,3... | collective-permute-start | bytes 6152 | tf_op jit(solution)/shard_map/ppermute | solution.py:474
where the time goes:
time: 277 us; the launch traced here: 273 us
  waiting for transfers between devices  110 us (40%)
  Pallas kernels  67.8 us (24%)
  starting transfers between devices  66 us (24%)
  local copies, waits for them, and re-layouts  16.5 us (6%)
  matrix products  5.61 us (2%)
  other arithmetic  5.46 us (2%)
    ppermute x18, waiting for transfers between devices, shifted(): return lax.ppermute(piece, 'tp', [(i, (i + by) % 4) for i in range(4)])  64.2 us
    ppermute x18, starting transfers between devices, shifted(): return lax.ppermute(piece, 'tp', [(i, (i + by) % 4) for i in range(4)])  19.4 us
    ppermute x8, waiting for transfers between devices, later(): lax.ppermute(pair, ('sq', 'core'), [(i, i - by) for i in range(by, length)])  18.1 us
    all_to_all x1, waiting for transfers between devices, per_device(): lax.all_to_all(mix.reshape(4 * sources, capacity, -1), ('tp', *sp_axes),...  17.2 us
    all_to_all x2, starting transfers between devices, exchanged(): lax.all_to_all(rows.reshape(sources, capacity, -1), sp_axes, 0, 0, tiled=...  15.5 us
    pallas_call x2, Pallas kernels, build(): pl.pallas_call(functools.partial(build_kernel, capacity=capacity, group=g...  14.2 us
    pallas_call x1, Pallas kernels, expert(): pl.pallas_call(functools.partial(expert_kernel, row_part=row_part, cot_pa...  13.8 us
    ppermute x8, starting transfers between devices, later(): lax.ppermute(pair, ('sq', 'core'), [(i, i - by) for i in range(by, length)])  12.1 us
  transfers between devices with their start and end apart: 31, of which 15 were waited for; matrix products, arithmetic and copies ran while one was open for 6% of the time, Pallas kernels for 23%

commit v1 on v0

--- a/solution.py
+++ b/solution.py
@@ -176,7 +176,7 @@
         at += source.shape[1]
 
 
-def build(position, ids, weight, parts, capacity, experts, group=4):
+def build(position, ids, weight, parts, capacity, experts, group=8):
     tokens = ids.shape[1]
     total = sum(width for _, width, _, _ in parts)
     specs = [pl.BlockSpec(ids.shape, lambda i, where: (0, 0))] * 2
@@ -203,52 +203,69 @@
     return (0, where[0] if column is None else column)
 
 
-def weights_kernel(where_ref, w_gate, w_up, *refs):
-    pieces, out_gate, out_up = refs[:-2], refs[-2], refs[-1]
+def weights_kernel(
+    where_ref, w_gate, w_up, w_down, own, left, right, far_top, far_bottom,
+    out_gate_up, out_down, out_gate, out_up, *, row_part, cot_part,
+):
     at = where_ref[0]
+    width, units = w_gate.shape
+    half = width // 2
+    first = ((0,), (0,))
+    for weights, out in ((w_gate, out_gate), (w_up, out_up)):
+        for step, piece in ((0, own), (3, left), (1, right)):
+            out[lax.rem(at + step, 4)] = dot(weights[...], piece[...], first).astype(BF16)
+        out[lax.rem(at + 2, 4)] = (
+            dot(weights[:half, :], far_top[...], first)
+            + dot(weights[half:, :], far_bottom[...], first)
+        ).astype(BF16)
+    rest = width - 4 * row_part
+    out_gate_up[:rest, :units] = w_gate[4 * row_part :, :]
+    out_gate_up[:rest, units:] = w_up[4 * row_part :, :]
+    cot_rest = width - 4 * cot_part
+    out_down[:cot_rest, :] = w_down[:, 4 * cot_part :].T
     for n, step in enumerate(ring_steps):
         group = lax.rem(at + step, 4)
-        top, bottom = pieces[2 * n], pieces[2 * n + 1]
-        half = top.shape[0]
-        for weights, out in ((w_gate, out_gate), (w_up, out_up)):
-            out[group] = (
-                dot(weights[:half, :], top[...], ((0,), (0,)))
-                + dot(weights[half:, :], bottom[...], ((0,), (0,)))
-            ).astype(BF16)
-
-
-def folded_weights(position, w_gate, w_up, pieces):
-    hidden, width = w_gate.shape[1], pieces[0].shape[1]
-    args = (position, w_gate, w_up, *pieces)
-    out = made((4, hidden, width), BF16)
-    return pl.pallas_call(
-        weights_kernel,
-        out_shape=(out, out),
+        lines = pl.ds(pl.multiple_of(group * row_part, row_part), row_part)
+        columns = pl.ds(pl.multiple_of(group * cot_part, 128), cot_part)
+        to = slice(rest + n * row_part, rest + (n + 1) * row_part)
+        out_gate_up[to, :units] = w_gate[lines, :]
+        out_gate_up[to, units:] = w_up[lines, :]
+        to = slice(cot_rest + n * cot_part, cot_rest + (n + 1) * cot_part)
+        out_down[to, :] = w_down[:, columns].T
+
+
+def folded_weights(position, w_gate, w_up, w_down, pieces, row_part, cot_part):
+    width, units = w_gate.shape
+    args = (position, w_gate, w_up, w_down, *pieces)
+    fold = made((4, units, pieces[0].shape[1]), BF16)
+    outs = (
+        made((width, 2 * units), BF16),
+        made((width, units), BF16),
+        fold,
+        fold,
+    )
+    return pl.pallas_call(
+        functools.partial(weights_kernel, row_part=row_part, cot_part=cot_part),
+        out_shape=outs,
         in_specs=[SMEM] + [whole(a.shape) for a in args[1:]],
-        out_specs=[whole(out.shape)] * 2,
-        compiler_params=params(16),
+        out_specs=[whole(o.shape) for o in outs],
+        compiler_params=params(24),
         cost_estimate=cost(4 * 10**9, 7 * 2**20),
         name="folded",
-    )(position, *kept([w_gate, w_up]), *pieces)
-
-
-def expert_kernel(where_ref, got_rows, got_cot, *refs, row_part, cot_part):
+    )(position, *kept([w_gate, w_up, w_down]), *pieces)
+
+
+def expert_kernel(got_rows, got_cot, *refs, row_part):
     pieces = refs[:8]
-    w_gate, w_up, w_down, fold_gate, fold_up, out_hidden, out_gate, out_up, out_mix = refs[8:]
-    at = where_ref[0]
+    gate_up, down, fold_gate, fold_up, out_hidden, out_gate, out_up, out_mix = refs[8:]
+    units = down.shape[1]
     upper = pl.program_id(0) < pl.num_programs(0) // 2
-    rows, cots = got_rows[...], got_cot[...]
-    gate_pre = dot(rows, w_gate[4 * row_part :, :])
-    up_pre = dot(rows, w_up[4 * row_part :, :])
-    hidden_cot = dot(cots, w_down[:, 4 * cot_part :], ((1,), (1,)))
-    for n, step in enumerate(ring_steps):
-        group = lax.rem(at + step, 4)
-        piece = jnp.where(upper, pieces[2 * n][...], pieces[2 * n + 1][...])
-        lines = pl.ds(pl.multiple_of(group * row_part, row_part), row_part)
-        columns = pl.ds(pl.multiple_of(group * cot_part, 128), cot_part)
-        gate_pre = gate_pre + dot(piece[:, :row_part], w_gate[lines, :])
-        up_pre = up_pre + dot(piece[:, :row_part], w_up[lines, :])
-        hidden_cot = hidden_cot + dot(piece[:, row_part:], w_down[:, columns], ((1,), (1,)))
+    parts = [jnp.where(upper, pieces[2 * n][...], pieces[2 * n + 1][...]) for n in range(4)]
+    rows = jnp.concatenate([got_rows[...], *(p[:, :row_part] for p in parts)], axis=1)
+    cots = jnp.concatenate([got_cot[...], *(p[:, row_part:] for p in parts)], axis=1)
+    both = dot(rows, gate_up[...])
+    gate_pre, up_pre = both[:, :units], both[:, units:]
+    hidden_cot = dot(cots, down[...])
     sigma = sigmoid(gate_pre)
     swish = gate_pre * sigma
     out_hidden[...] = (swish * up_pre).astype(BF16)
@@ -260,9 +277,9 @@
         out_mix[c] = (dot(gate_cot, fold_gate[c]) + dot(up_cot, fold_up[c])).astype(BF16)
 
 
-def expert(position, got, pieces, w_gate, w_up, w_down, fold_gate, fold_up, row_part, cot_part, steps=4):
+def expert(got, pieces, gate_up, down, fold_gate, fold_up, row_part, cot_part, steps=4):
     rows = got.shape[0]
-    width, hidden = w_gate.shape
+    width, hidden = down.shape
     block = rows // steps
     part = fold_gate.shape[2]
     half = steps // 2
@@ -272,21 +289,20 @@
     top = pl.BlockSpec((block, row_part + cot_part), lambda i: (jnp.minimum(i, half - 1), 0))
     bottom = pl.BlockSpec((block, row_part + cot_part), lambda i: (jnp.maximum(i - half, 0), 0))
     return pl.pallas_call(
-        functools.partial(expert_kernel, row_part=row_part, cot_part=cot_part),
+        functools.partial(expert_kernel, row_part=row_part),
         out_shape=(narrow, narrow, narrow, made((4, rows, part), BF16)),
         grid=(steps,),
         in_specs=[
-            SMEM,
             pl.BlockSpec((block, row_rest), lambda i: (i, 0)),
             pl.BlockSpec((block, cot_rest), lambda i: (i, row_rest // cot_rest)),
             *([top, bottom] * 4),
-            *(whole(a.shape) for a in (w_gate, w_up, w_down, fold_gate, fold_up)),
+            *(whole(a.shape) for a in (gate_up, down, fold_gate, fold_up)),
         ],
         out_specs=[mine, mine, mine, pl.BlockSpec((4, block, part), lambda i: (0, i, 0))],
-        compiler_params=params(30),
+        compiler_params=params(26),
         cost_estimate=cost(7 * 10**9, 18 * 2**20),
         name="expert",
-    )(position, *kept([got, got]), *pieces, *kept([w_gate, w_up, w_down, fold_gate, fold_up]))
+    )(*kept([got, got]), *pieces, *kept([gate_up, down, fold_gate, fold_up]))
 
 
 def grads_kernel(where_ref, got_rows, got_cot, *refs, row_part, cot_part):
@@ -470,6 +486,13 @@
     return top, bottom, left_top, left_bottom, right_top, right_bottom, far_top, far_bottom
 
 
+def whole_ring_gather(own):
+    half = own.shape[0] // 2
+    left, right = shifted(own, 1), shifted(own, -1)
+    far_top, far_bottom = shifted(left[:half], 1), shifted(right[half:], -1)
+    return own, left, right, far_top, far_bottom
+
+
 def later(pair, by, length):
     return lax.ppermute(pair, ("sq", "core"), [(i, i - by) for i in range(by, length)])
 
@@ -514,9 +537,10 @@
         capacity, sources,
     )
     spread = exchanged(spread)
-    half = out_proj.shape[0] // 2
-    projections = ring_gather(out_proj[:half], out_proj[half:])
-    fold_gate, fold_up = folded_weights(position, w_gate, w_up, projections)
+    projections = whole_ring_gather(out_proj)
+    gate_up, down, fold_gate, fold_up = folded_weights(
+        position, w_gate, w_up, w_down, projections, row_part, cot_part
+    )
     rates = (decay_factor * jax.nn.softplus(-decay_param)).reshape(-1, gate_a_w.shape[1])
     rec_output, act, b, ca, ci, cs, decay, seg, exp, block, sel = early(
         position, expert_ids, rec_input, gate_input, prev_state, rates, extra_decay.T,
@@ -538,7 +562,7 @@
         out_cot, rec_output, (((0,), (0,)), ((), ())), preferred_element_type=F32
     )
     hidden, gate_cot, up_cot, mix = expert(
-        position, got, pieces, w_gate, w_up, w_down, fold_gate, fold_up, row_part, cot_part
+        got, pieces, gate_up, down, fold_gate, fold_up, row_part, cot_part
     )
     back = lax.all_to_all(
         mix.reshape(4 * sources, capacity, -1), ("tp", *sp_axes), 0, 0, tiled=True

time: 277 us -> 271 us (0.978)
  local copies, waits for them, and re-layouts: 16.5 us -> 11.9 us
    unnamed x50 -> x38, local copies, waits for them, and re-layouts: 11.3 us -> 7.03 us
    ppermute x18 -> x16, starting transfers between devices: 19.4 us -> 17.9 us  [shifted(): return lax.ppermute(piece, 'tp', [(i, (i + by) % 4) for i in range(4)])]
    ppermute x18 -> x16, waiting for transfers between devices: 64.2 us -> 65 us  [shifted(): return lax.ppermute(piece, 'tp', [(i, (i + by) % 4) for i in range(4)])]
  transfers between devices with their start and end apart: 31 -> 29, of which waited for: 15 -> 14; matrix products, arithmetic and copies ran while one was open for 6% -> 6% of each run, Pallas kernels for 23% -> 23%
where the time goes in v1:
time: 271 us; the launch traced here: 267 us
  waiting for transfers between devices  112 us (41%)
  Pallas kernels  66.3 us (24%)
  starting transfers between devices  64.7 us (24%)
  local copies, waits for them, and re-layouts  11.9 us (4%)
  matrix products  5.61 us (2%)
  other arithmetic  5.46 us (2%)
    ppermute x16, waiting for transfers between devices, shifted(): return lax.ppermute(piece, 'tp', [(i, (i + by) % 4) for i in range(4)])  65 us
    ppermute x8, waiting for transfers between devices, later(): lax.ppermute(pair, ('sq', 'core'), [(i, i - by) for i in range(by, length)])  18.1 us
    ppermute x16, starting transfers between devices, shifted(): return lax.ppermute(piece, 'tp', [(i, (i + by) % 4) for i in range(4)])  17.9 us
    all_to_all x1, waiting for transfers between devices, per_device(): lax.all_to_all(mix.reshape(4 * sources, capacity, -1), ('tp', *sp_axes),...  17.2 us
    all_to_all x2, starting transfers between devices, exchanged(): lax.all_to_all(rows.reshape(sources, capacity, -1), sp_axes, 0, 0, tiled=...  15.5 us
    pallas_call x1, Pallas kernels, expert(): pl.pallas_call(functools.partial(expert_kernel, row_part=row_part), out_s...  13.4 us
    all_to_all x1, starting transfers between devices, per_device(): lax.all_to_all(mix.reshape(4 * sources, capacity, -1), ('tp', *sp_axes),...  12.2 us
    ppermute x8, starting transfers between devices, later(): lax.ppermute(pair, ('sq', 'core'), [(i, i - by) for i in range(by, length)])  12.1 us
  transfers between devices with their start and end apart: 29, of which 14 were waited for; matrix products, arithmetic and copies ran while one was open for 6% of the time, Pallas kernels for 23%

profile of v1, /device:TPU:1, one launch (start us, length us, event | category | flops | bytes accessed | tf_op | source)
XLA Modules:
  0.0 267.0 jit_solution(15259401915205619392)
XLA Ops:
  0.7 4.7 %shard_map.191 = bf16[1280,640]{1,0:T(8,128)(2,1)} custom-call(s32[2]{0:T(128)S(1)} %pad_add_fusion.where_ref, s32[2,512]{1,0:T(2,128)} %bitcast.45, f32[2,512]{1,0:T(2,128)} %bitcast.47, bf16[512,2048]{1,0:T(8,128)(2,1)} %refs_0_.3, bf16[512,2048]{1,0:T(8,128)(2,1)} %refs_1_.3), custom_call_target="tpu_custom_call" | custom-call | flops 896000000 | bytes 3200000 | tf_op jit(solution)/shard_map/pallas_call | solution.py:185
  5.4 9.7 %all-to-all-start.1 = ((bf16[32,40,640]{2,1,0:T(8,128)(2,1)}), bf16[32,40,640]{2,1,0:T(8,128)(2,1)S(1)}, u32[]{:S(2)}, u32[]{:S(2)}) async-start(bf16[32,40,640]{2,1,0:T(8,128)(2,1)} %bitcast.41), calls=%async_computation.1 | async-start | bytes 3276800 | tf_op jit(solution)/shard_map/all_to_all | solution.py:530
  15.2 0.9 copy.22.ids
  16.0 0.9 copy.21
  16.9 0.6 fusion.2.rates
  17.5 6.4 %early.1 = (bf16[512,256]{1,0:T(8,128)(2,1)}, f32[512,256]{1,0:T(8,128)}, f32[512,256]{1,0:T(8,128)}, f32[512,256]{1,0:T(8,128)}, f32[512,256]{1,0:T(8,128)}, /*...) custom-call(s32[2]{0:T(128)S(1)} %pad_add_fusion.where_ref, ...), custom_call_target="tpu_custom_call" | custom-call | flops 3000000000 | bytes 8388608 | tf_op jit(solution)/shard_map/early/pallas_call | solution.py:131
  23.9 6.8 %shard_map.190 = bf16[1280,1792]{1,0:T(8,128)(2,1)} custom-call(s32[2]{0:T(128)S(1)} %pad_add_fusion.where_ref, s32[2,512]{1,0:T(2,128)} %bitcast.46, f32[2,512]{1,0:T(2,128)} %bitcast.48, bf16[512,2048]{1,0:T(8,128)(2,1)} %refs_0_.3, bf16[512,2048]{1,0:T(8,128)(2,1)} %refs_1_.3, bf16[512,256]{1,0:T(8,128)(2,1)} %get-tuple-element.31.refs_2_), custom_call_target="tpu_custom_call" | custom-call | flops 2508800000 | bytes 8960000 | tf_op jit(solution)/shard_map/pallas_call | solution.py:185
  30.7 8.0 %all-to-all-done.1 = bf16[32,40,640]{2,1,0:T(8,128)(2,1)S(1)} async-done(((bf16[32,40,640]{2,1,0:T(8,128)(2,1)}), bf16[32,40,640]{2,1,0:T(8,128)(2,1)S(1)}, u32[]{:S(2)}, u32[]{:S(2)}) %all-to-all-start.1) | async-done | bytes 1638432 | tf_op jit(solution)/shard_map/all_to_all | solution.py:530
  38.8 5.8 %all-to-all-start = ((bf16[32,40,1792]{2,1,0:T(8,128)(2,1)}), bf16[32,40,1792]{2,1,0:T(8,128)(2,1)}, u32[]{:S(2)}, u32[]{:S(2)}) async-start(bf16[32,40,1792]{2,1,0:T(8,128)(2,1)} %bitcast.42), calls=%async_computation | async-start | bytes 9175040 | tf_op jit(solution)/shard_map/all_to_all | solution.py:530
  44.6 1.3 collective-permute-start.6
  45.9 1.5 collective-permute-start.7
  47.3 0.1 fusion.15
  47.6 2.7 collective-permute-start.3
  50.2 20.2 %collective-permute-done.6.left = bf16[2048,256]{1,0:T(8,128)(2,1)S(1)} collective-permute-done((bf16[2048,256]{1,0:T(8,128)(2,1)}, bf16[2048,256]{1,0:T(8,128)(2,1)S(1)}, u32[]{:S(2)}, u32[]{:S(2)}) %collective-permute-start.6) | collective-permute-done | bytes 1048608 | tf_op jit(solution)/shard_map/ppermute | solution.py:479
  70.6 1.2 collective-permute-start.1
  71.8 0.9 slice.110
  72.7 1.0 copy-done.8
  73.6 1.5 collective-permute-start.9
  75.2 24.0 %collective-permute-done.8.far_top = bf16[1024,256]{1,0:T(8,128)(2,1)S(1)} collective-permute-done((bf16[1024,256]{1,0:T(8,128)(2,1)S(1)}, bf16[1024,256]{1,0:T(8,128)(2,1)S(1)}, u32[]{:S(2)}, u32[]{:S(2)}) %collective-permute-start.8) | collective-permute-done | bytes 524320 | tf_op jit(solution)/shard_map/ppermute | solution.py:479
  99.2 0.8 copy-done.10
  100.0 1.4 collective-permute-start.2
  101.3 0.1 collective-permute-start.4
  101.4 2.7 collective-permute-start.5
  104.1 2.2 convolution_bitcast_fusion.local
  106.3 2.0 fusion.14
  108.3 8.5 %collective-permute-done.1.refs_3_ = bf16[640,640]{1,0:T(8,128)(2,1)} collective-permute-done((bf16[640,640]{1,0:T(8,128)(2,1)S(1)}, bf16[640,640]{1,0:T(8,128)(2,1)}, u32[]{:S(2)}, u32[]{:S(2)}) %collective-permute-start.1) | collective-permute-done | bytes 819232 | tf_op jit(solution)/shard_map/ppermute | solution.py:479
  116.8 1.3 collective-permute-start.13
  118.1 1.2 copy-done.7
  119.3 1.2 copy-done.9
  120.6 1.0 copy-done.11
  121.6 6.9 %folded.1 = (bf16[2048,512]{1,0:T(8,128)(2,1)}, bf16[2048,256]{1,0:T(8,128)(2,1)}, bf16[4,256,256]{2,1,0:T(8,128)(2,1)}, bf16[4,256,256]{2,1,0:T(8,128)(2,1)}) custom-call(s32[2]{0:T(128)S(1)} %pad_add_fusion.where_ref, bf16[2048,256]{1,0:T(8,128)(2,1)} %bitcast.50, bf16[2048,256]{1,0:T(8,128)(2,1)} %bitcast.52, bf16[256,2048]{1,0:T(8,128)(2,1)} %bitcast.49, ...), custom_call_target="tpu_custom_call" | custom-call | flops 4000000000 | bytes 7340032 | tf_op jit(solution)/shard_map/folded/pallas_call | solution.py:247
  128.5 0.3 collective-permute-start.11
  128.8 5.6 %collective-permute-done.4.refs_6_ = bf16[640,640]{1,0:T(8,128)(2,1)} collective-permute-done((bf16[640,640]{1,0:T(8,128)(2,1)S(1)}, bf16[640,640]{1,0:T(8,128)(2,1)}, u32[]{:S(2)}, u32[]{:S(2)}) %collective-permute-start.4) | collective-permute-done | bytes 819232 | tf_op jit(solution)/shard_map/ppermute | solution.py:479
  134.4 1.3 collective-permute-start.12
  135.7 5.7 %collective-permute-done.10.refs_2_ = bf16[640,256]{1,0:T(8,128)(2,1)} collective-permute-done((bf16[640,256]{1,0:T(8,128)(2,1)}, bf16[640,256]{1,0:T(8,128)(2,1)}, u32[]{:S(2)}, u32[]{:S(2)}) %collective-permute-start.10) | collective-permute-done | bytes 327712 | tf_op jit(solution)/shard_map/ppermute | solution.py:479
  141.4 0.9 collective-permute-done.13.refs_5_
  142.3 2.7 %collective-permute-start.15 = (bf16[640,256]{1,0:T(8,128)(2,1)}, bf16[640,256]{1,0:T(8,128)(2,1)}, u32[]{:S(2)}, u32[]{:S(2)}) collective-permute-start(bf16[640,256]{1,0:T(8,128)(2,1)} %collective-permute-done.13.refs_5_), channel_id=1, source_target_pairs={{0,3},{1,0},{2,1},{3,2},{4,7},{5,4},{6,5},{7,6},{8,11},{9,8},{10,9... | collective-permute-start | bytes 983048 | tf_op jit(solution)/shard_map/ppermute | solution.py:479
  145.0 13.4 %expert.1 = (bf16[1280,256]{1,0:T(8,128)(2,1)}, bf16[1280,256]{1,0:T(8,128)(2,1)}, bf16[1280,256]{1,0:T(8,128)(2,1)}, bf16[4,1280,256]{2,1,0:T(8,128)(2,1)}) custom-call(bf16[1280,1792]{1,0:T(8,128)(2,1)} %bitcast.7.got_rows.got_cot, bf16[1280,1792]{1,0:T(8,128)(2,1)} %bitcast.7.got_rows.got_cot, bf16[640,640]{1,0:T(8,128)(2,1)S(1)} %bitcast.38, ...), custom_call_target="tpu_custom_call" | custom-call | flops 7000000000 | bytes 18874368 | tf_op jit(solution)/shard_map/expert/pallas_call | solution.py:291
  158.4 12.2 %all-to-all-start.3 = ((bf16[128,40,256]{2,1,0:T(8,128)(2,1)}), bf16[128,40,256]{2,1,0:T(8,128)(2,1)S(1)}, u32[]{:S(2)}, u32[]{:S(2)}) async-start(bf16[128,40,256]{2,1,0:T(8,128)(2,1)} %bitcast.43), calls=%async_computation.3 | async-start | bytes 5242880 | tf_op jit(solution)/shard_map/all_to_all | solution.py:567
  170.6 9.6 %proj.1 = bf16[2,4,16,64,256]{4,3,2,1,0:T(8,128)(2,1)} custom-call(s32[2]{0:T(128)S(1)} %pad_add_fusion.where_ref, bf16[1280,256]{1,0:T(8,128)(2,1)} %get-tuple-element.37.refs_9_.gate_cot, bf16[1280,256]{1,0:T(8,128)(2,1)} %get-tuple-element.38.refs_10_.up_cot, bf16[2048,256]{1,0:T(8,128)(2,1)} %bitcast.51, bf16[2048,256]{1,0:T(8,128)(2,1)} %bitcast.53, ...), custom_call_target="tpu_custom_call" | custom-call | flops 4000000000 | bytes 14680064 | tf_op jit(solution)/shard_map/proj/pallas_call | solution.py:387
  180.3 1.9 slice_bitcast_fusion
  182.1 1.1 collective-permute-start.16
  183.3 3.8 %collective-permute-done.16 = bf16[4,16,64,256]{3,2,1,0:T(8,128)(2,1)S(1)} collective-permute-done((bf16[4,16,64,256]{3,2,1,0:T(8,128)(2,1)S(1)}, bf16[4,16,64,256]{3,2,1,0:T(8,128)(2,1)S(1)}, u32[]{:S(2)}, u32[]{:S(2)}) %collective-permute-start.16) | collective-permute-done | bytes 2097184 | tf_op jit(solution)/shard_map/ppermute | solution.py:577
  187.1 2.2 fusion
  189.3 17.2 %all-to-all-done.3 = bf16[128,40,256]{2,1,0:T(8,128)(2,1)S(1)} async-done(((bf16[128,40,256]{2,1,0:T(8,128)(2,1)}), bf16[128,40,256]{2,1,0:T(8,128)(2,1)S(1)}, u32[]{:S(2)}, u32[]{:S(2)}) %all-to-all-start.3) | async-done | bytes 2621472 | tf_op jit(solution)/shard_map/all_to_all | solution.py:567
  206.5 5.8 %all-to-all-start.2 = ((bf16[64,64,256]{2,1,0:T(8,128)(2,1)}), bf16[64,64,256]{2,1,0:T(8,128)(2,1)}, u32[]{:S(2)}, u32[]{:S(2)}) async-start(bf16[64,64,256]{2,1,0:T(8,128)(2,1)} %bitcast.40), calls=%async_computation.2 | async-start | bytes 4194304 | tf_op jit(solution)/shard_map/all_to_all | solution.py:579
  212.3 3.4 %fusion.16.base = f32[512,256]{1,0:T(8,128)} fusion(bf16[512,2048]{1,0:T(8,128)(2,1)} %refs_1_.3, bf16[2048,256]{1,0:T(8,128)(2,1)} %own.1), kind=kOutput, calls=%fused_computation.36 | convolution fusion | flops 536870912 | bytes 3670016 | tf_op jit(solution)/shard_map/dot_general | solution.py:560
  215.7 4.6 %scanned.1 = (bf16[512,256]{1,0:T(8,128)(2,1)}, f32[512,256]{1,0:T(8,128)}, f32[2,256]{1,0:T(2,128)}) custom-call(bf16[4,1280,256]{2,1,0:T(8,128)(2,1)S(1)} %bitcast.31, bf16[512,1280]{1,0:T(8,128)(2,1)} %get-tuple-element.43.sel, f32[512,256]{1,0:T(8,128)} %fusion.16.base, f32[512,256]{1,0:T(8,128)} %get-tuple-element.44.act, ...), custom_call_target="tpu_custom_call" | custom-call | flops 400000000 | bytes 8388608 | tf_op jit(solution)/shard_map/scanned/pallas_call | solution.py:436
  220.3 3.1 %collective-permute-start.17 = (f32[2,256]{1,0:T(2,128)}, f32[2,256]{1,0:T(2,128)S(1)}, u32[]{:S(2)}, u32[]{:S(2)}) collective-permute-start(f32[2,256]{1,0:T(2,128)} %get-tuple-element.49), channel_id=1, source_target_pairs={{4,0},{8,4},{12,8},{16,12},{20,16},{24,20},{28,24},{32,28},{36,32}... | collective-permute-start | bytes 6152 | tf_op jit(solution)/shard_map/ppermute | solution.py:497
  223.4 1.3 collective-permute-start.18
  224.7 1.3 collective-permute-start.19
  226.0 1.3 collective-permute-start.20
  227.3 4.3 %collective-permute-done.17 = f32[2,256]{1,0:T(2,128)S(1)} collective-permute-done((f32[2,256]{1,0:T(2,128)}, f32[2,256]{1,0:T(2,128)S(1)}, u32[]{:S(2)}, u32[]{:S(2)}) %collective-permute-start.17) | collective-permute-done | bytes 2080 | tf_op jit(solution)/shard_map/ppermute | solution.py:497
  231.6 4.3 %collective-permute-done.19 = f32[2,256]{1,0:T(2,128)S(1)} collective-permute-done((f32[2,256]{1,0:T(2,128)}, f32[2,256]{1,0:T(2,128)S(1)}, u32[]{:S(2)}, u32[]{:S(2)}) %collective-permute-start.19) | collective-permute-done | bytes 2080 | tf_op jit(solution)/shard_map/ppermute | solution.py:497
  236.0 1.3 collective-permute-start.21
  237.3 1.3 collective-permute-start.22
  238.6 1.3 collective-permute-start.23
  239.9 2.3 collective-permute-done.21
  242.2 2.4 collective-permute-done.22
  244.6 4.7 %collective-permute-done.23 = f32[2,256]{1,0:T(2,128)S(1)} collective-permute-done((f32[2,256]{1,0:T(2,128)S(1)}, f32[2,256]{1,0:T(2,128)S(1)}, u32[]{:S(2)}, u32[]{:S(2)}) %collective-permute-start.23) | collective-permute-done | bytes 2080 | tf_op jit(solution)/shard_map/ppermute | solution.py:497
  249.3 1.3 collective-permute-start.24
  250.7 10.9 %grads.1 = (f32[1,2048,256]{2,1,0:T(8,128)}, f32[1,2048,256]{2,1,0:T(8,128)}, f32[1,256,2048]{2,1,0:T(8,128)}) custom-call(s32[2]{0:T(128)S(1)} %pad_add_fusion.where_ref, bf16[1280,1792]{1,0:T(8,128)(2,1)} %bitcast.7.got_rows.got_cot, bf16[1280,1792]{1,0:T(8,128)(2,1)} %bitcast.7.got_rows.got_cot, bf16[640,640]{1,0:T(8,128)(2,1)S(1)} %bitcast.39, ...), custom_call_target="tpu_custom_call" | custom-call | flops 4000000000 | bytes 17825792 | tf_op jit(solution)/shard_map/grads/pallas_call | solution.py:341
  261.6 2.9 %final.1 = bf16[512,256]{1,0:T(8,128)(2,1)} custom-call(s32[2]{0:T(128)S(1)} %pad_add_fusion.where_ref, f32[2,256]{1,0:T(2,128)S(1)} %pad_maximum_fusion.2.carry, f32[512,256]{1,0:T(8,128)} %get-tuple-element.50.local, f32[512,256]{1,0:T(8,128)} %get-tuple-element.51.exp, f32[512,256]{1,0:T(8,128)} %get-tuple-element.52.ca, ...), custom_call_target="tpu_custom_call" | custom-call | flops 100000000 | bytes 4194304 | tf_op jit(solution)/shard_map/final/pallas_call | solution.py:467
  264.5 2.5 convert_reduce_fusion
  (58 shorter events, 0.4 us)
Async XLA Ops:
  5.4 9.8 %copy-start.15 = (s32[512,2]{0,1:T(2,128)S(1)}, s32[512,2]{0,1:T(2,128)}, u32[]{:S(2)}) copy-start(s32[512,2]{0,1:T(2,128)} %param.17) | copy-start | bytes 12292
  5.4 10.6 %copy-start.16 = (f32[2,512]{1,0:T(2,128)S(1)}, f32[2,512]{1,0:T(2,128)}, u32[]{:S(2)}) copy-start(f32[2,512]{1,0:T(2,128)} %param.27) | copy-start | bytes 12292
  5.4 11.5 %copy-start.17 = (f32[1024]{0:T(1024)S(1)}, f32[1024]{0:T(1024)}, u32[]{:S(2)}) copy-start(f32[1024]{0:T(1024)} %param.26) | copy-start | bytes 12292
  5.4 33.3 %all-to-all-start.1 = ((bf16[32,40,640]{2,1,0:T(8,128)(2,1)}), bf16[32,40,640]{2,1,0:T(8,128)(2,1)S(1)}, u32[]{:S(2)}, u32[]{:S(2)}) async-start(bf16[32,40,640]{2,1,0:T(8,128)(2,1)} %bitcast.41), calls=%async_computation.1 | async-start | bytes 3276800 | tf_op jit(solution)/shard_map/all_to_all | solution.py:530
  38.8 67.6 %all-to-all-start = ((bf16[32,40,1792]{2,1,0:T(8,128)(2,1)}), bf16[32,40,1792]{2,1,0:T(8,128)(2,1)}, u32[]{:S(2)}, u32[]{:S(2)}) async-start(bf16[32,40,1792]{2,1,0:T(8,128)(2,1)} %bitcast.42), calls=%async_computation | async-start | bytes 9175040 | tf_op jit(solution)/shard_map/all_to_all | solution.py:530
  44.6 59.5 %copy-start.12 = (bf16[512,2048]{1,0:T(8,128)(2,1)S(1)}, bf16[512,2048]{1,0:T(8,128)(2,1)}, u32[]{:S(2)}) copy-start(bf16[512,2048]{1,0:T(8,128)(2,1)} %refs_1_.3) | copy-start | bytes 6291460
  44.6 59.5 %copy-start.14 = (bf16[512,256]{1,0:T(8,128)(2,1)S(1)}, bf16[512,256]{1,0:T(8,128)(2,1)}, u32[]{:S(2)}) copy-start(bf16[512,256]{1,0:T(8,128)(2,1)} %get-tuple-element.31.refs_2_) | copy-start | bytes 786436
  44.6 25.9 %collective-permute-start.6 = (bf16[2048,256]{1,0:T(8,128)(2,1)}, bf16[2048,256]{1,0:T(8,128)(2,1)S(1)}, u32[]{:S(2)}, u32[]{:S(2)}) collective-permute-start(bf16[2048,256]{1,0:T(8,128)(2,1)} %own.1), channel_id=1, source_target_pairs={{0,1},{1,2},{2,3},{3,0},{4,5},{5,6},{6,7},{7,4},{8,9},{9,10},{10,1... | collective-permute-start | bytes 3145736 | tf_op jit(solution)/shard_map/ppermute | solution.py:479
  45.9 25.9 %collective-permute-start.7 = (bf16[2048,256]{1,0:T(8,128)(2,1)}, bf16[2048,256]{1,0:T(8,128)(2,1)S(1)}, u32[]{:S(2)}, u32[]{:S(2)}) collective-permute-start(bf16[2048,256]{1,0:T(8,128)(2,1)} %own.1), channel_id=1, source_target_pairs={{0,3},{1,0},{2,1},{3,2},{4,7},{5,4},{6,5},{7,6},{8,11},{9,8},{10,9... | collective-permute-start | bytes 3145736 | tf_op jit(solution)/shard_map/ppermute | solution.py:479
  47.5 97.5 %copy-start = (bf16[16,40,640]{2,1,0:T(8,128)(2,1)}, bf16[16,40,640]{2,1,0:T(8,128)(2,1)S(1)}, u32[]{:S(2)}) copy-start(bf16[16,40,640]{2,1,0:T(8,128)(2,1)S(1)} %get-tuple-element.59) | copy-start | bytes 2457604
  47.5 53.9 %collective-permute-start = (bf16[640,640]{1,0:T(8,128)(2,1)S(1)}, bf16[640,640]{1,0:T(8,128)(2,1)S(1)}, u32[]{:S(2)}, u32[]{:S(2)}) collective-permute-start(bf16[640,640]{1,0:T(8,128)(2,1)S(1)} %bitcast.36), channel_id=1, source_target_pairs={{0,1},{1,2},{2,3},{3,0},{4,5},{5,6},{6,7},{7,4},{8,9},{9,10},{10,1... | collective-permute-start | bytes 2457608 | tf_op jit(solution)/shard_map/ppermute | solution.py:479
  47.6 53.9 %collective-permute-start.3 = (bf16[640,640]{1,0:T(8,128)(2,1)S(1)}, bf16[640,640]{1,0:T(8,128)(2,1)S(1)}, u32[]{:S(2)}, u32[]{:S(2)}) collective-permute-start(bf16[640,640]{1,0:T(8,128)(2,1)S(1)} %bitcast.32), channel_id=1, source_target_pairs={{0,3},{1,0},{2,1},{3,2},{4,7},{5,4},{6,5},{7,6},{8,11},{9,8},{10,9... | collective-permute-start | bytes 2457608 | tf_op jit(solution)/shard_map/ppermute | solution.py:479
  70.5 31.0 %copy-start.6 = (bf16[2048,256]{1,0:T(8,128)(2,1)}, bf16[2048,256]{1,0:T(8,128)(2,1)S(1)}, u32[]{:S(2)}) copy-start(bf16[2048,256]{1,0:T(8,128)(2,1)S(1)} %collective-permute-done.6.left) | copy-start | bytes 3145732
  70.5 28.6 %collective-permute-start.8 = (bf16[1024,256]{1,0:T(8,128)(2,1)S(1)}, bf16[1024,256]{1,0:T(8,128)(2,1)S(1)}, u32[]{:S(2)}, u32[]{:S(2)}) collective-permute-start(bf16[1024,256]{1,0:T(8,128)(2,1)S(1)} %slice.109), channel_id=1, source_target_pairs={{0,1},{1,2},{2,3},{3,0},{4,5},{5,6},{6,7},{7,4},{8,9},{9,10},{10,1... | collective-permute-start | bytes 1572872 | tf_op jit(solution)/shard_map/ppermute | solution.py:479
  70.6 46.2 %collective-permute-start.1 = (bf16[640,640]{1,0:T(8,128)(2,1)S(1)}, bf16[640,640]{1,0:T(8,128)(2,1)}, u32[]{:S(2)}, u32[]{:S(2)}) collective-permute-start(bf16[640,640]{1,0:T(8,128)(2,1)S(1)} %bitcast.33), channel_id=1, source_target_pairs={{0,1},{1,2},{2,3},{3,0},{4,5},{5,6},{6,7},{7,4},{8,9},{9,10},{10,1... | collective-permute-start | bytes 2457608 | tf_op jit(solution)/shard_map/ppermute | solution.py:479
  72.7 1.0 copy-start.8
  73.6 34.7 %collective-permute-start.9 = (bf16[1024,256]{1,0:T(8,128)(2,1)}, bf16[1024,256]{1,0:T(8,128)(2,1)}, u32[]{:S(2)}, u32[]{:S(2)}) collective-permute-start(bf16[1024,256]{1,0:T(8,128)(2,1)} %slice.110), channel_id=1, source_target_pairs={{0,3},{1,0},{2,1},{3,2},{4,7},{5,4},{6,5},{7,6},{8,11},{9,8},{10,9... | collective-permute-start | bytes 1572872 | tf_op jit(solution)/shard_map/ppermute | solution.py:479
  99.2 0.8 copy-start.10
  100.0 28.5 %collective-permute-start.2 = (bf16[640,640]{1,0:T(8,128)(2,1)S(1)}, bf16[640,640]{1,0:T(8,128)(2,1)}, u32[]{:S(2)}, u32[]{:S(2)}) collective-permute-start(bf16[640,640]{1,0:T(8,128)(2,1)S(1)} %bitcast.37), channel_id=1, source_target_pairs={{0,3},{1,0},{2,1},{3,2},{4,7},{5,4},{6,5},{7,6},{8,11},{9,8},{10,9... | collective-permute-start | bytes 2457608 | tf_op jit(solution)/shard_map/ppermute | solution.py:479
  101.3 43.7 %copy-start.2 = (bf16[640,640]{1,0:T(8,128)(2,1)}, bf16[640,640]{1,0:T(8,128)(2,1)S(1)}, u32[]{:S(2)}) copy-start(bf16[640,640]{1,0:T(8,128)(2,1)S(1)} %collective-permute-done.refs_2_) | copy-start | bytes 2457604
  101.3 33.0 %collective-permute-start.4 = (bf16[640,640]{1,0:T(8,128)(2,1)S(1)}, bf16[640,640]{1,0:T(8,128)(2,1)}, u32[]{:S(2)}, u32[]{:S(2)}) collective-permute-start(bf16[640,640]{1,0:T(8,128)(2,1)S(1)} %collective-permute-done.refs_2_), channel_id=1, source_target_pairs={{0,1},{1,2},{2,3},{3,0},{4,5},{5,6},{6,7},{7,4},{8,9},{9,10},{10,1... | collective-permute-start | bytes 2457608 | tf_op jit(solution)/shard_map/ppermute | solution.py:479
  101.4 43.6 %copy-start.4 = (bf16[640,640]{1,0:T(8,128)(2,1)}, bf16[640,640]{1,0:T(8,128)(2,1)S(1)}, u32[]{:S(2)}) copy-start(bf16[640,640]{1,0:T(8,128)(2,1)S(1)} %collective-permute-done.3.refs_5_) | copy-start | bytes 2457604
  101.4 43.6 %collective-permute-start.5 = (bf16[640,640]{1,0:T(8,128)(2,1)S(1)}, bf16[640,640]{1,0:T(8,128)(2,1)}, u32[]{:S(2)}, u32[]{:S(2)}) collective-permute-start(bf16[640,640]{1,0:T(8,128)(2,1)S(1)} %collective-permute-done.3.refs_5_), channel_id=1, source_target_pairs={{0,3},{1,0},{2,1},{3,2},{4,7},{5,4},{6,5},{7,6},{8,11},{9,8},{10,9... | collective-permute-start | bytes 2457608 | tf_op jit(solution)/shard_map/ppermute | solution.py:479
  108.3 33.1 %collective-permute-start.10 = (bf16[640,256]{1,0:T(8,128)(2,1)}, bf16[640,256]{1,0:T(8,128)(2,1)}, u32[]{:S(2)}, u32[]{:S(2)}) collective-permute-start(bf16[640,256]{1,0:T(8,128)(2,1)} %get-tuple-element.57.refs_0_), channel_id=1, source_target_pairs={{0,1},{1,2},{2,3},{3,0},{4,5},{5,6},{6,7},{7,4},{8,9},{9,10},{10,1... | collective-permute-start | bytes 983048 | tf_op jit(solution)/shard_map/ppermute | solution.py:479
  116.8 25.5 %collective-permute-start.13 = (bf16[640,256]{1,0:T(8,128)(2,1)}, bf16[640,256]{1,0:T(8,128)(2,1)}, u32[]{:S(2)}, u32[]{:S(2)}) collective-permute-start(bf16[640,256]{1,0:T(8,128)(2,1)} %get-tuple-element.56.refs_1_), channel_id=1, source_target_pairs={{0,3},{1,0},{2,1},{3,2},{4,7},{5,4},{6,5},{7,6},{8,11},{9,8},{10,9... | collective-permute-start | bytes 983048 | tf_op jit(solution)/shard_map/ppermute | solution.py:479
  118.1 1.2 copy-start.7
  119.3 1.2 copy-start.9
  120.6 1.0 copy-start.11
  128.5 42.1 %collective-permute-start.11 = (bf16[640,256]{1,0:T(8,128)(2,1)}, bf16[640,256]{1,0:T(8,128)(2,1)}, u32[]{:S(2)}, u32[]{:S(2)}) collective-permute-start(bf16[640,256]{1,0:T(8,128)(2,1)} %get-tuple-element.56.refs_1_), channel_id=1, source_target_pairs={{0,1},{1,2},{2,3},{3,0},{4,5},{5,6},{6,7},{7,4},{8,9},{9,10},{10,1... | collective-permute-start | bytes 983048 | tf_op jit(solution)/shard_map/ppermute | solution.py:479
  134.4 36.2 %collective-permute-start.12 = (bf16[640,256]{1,0:T(8,128)(2,1)}, bf16[640,256]{1,0:T(8,128)(2,1)}, u32[]{:S(2)}, u32[]{:S(2)}) collective-permute-start(bf16[640,256]{1,0:T(8,128)(2,1)} %get-tuple-element.57.refs_0_), channel_id=1, source_target_pairs={{0,3},{1,0},{2,1},{3,2},{4,7},{5,4},{6,5},{7,6},{8,11},{9,8},{10,9... | collective-permute-start | bytes 983048 | tf_op jit(solution)/shard_map/ppermute | solution.py:479
  141.4 29.2 %collective-permute-start.14 = (bf16[640,256]{1,0:T(8,128)(2,1)}, bf16[640,256]{1,0:T(8,128)(2,1)}, u32[]{:S(2)}, u32[]{:S(2)}) collective-permute-start(bf16[640,256]{1,0:T(8,128)(2,1)} %collective-permute-done.10.refs_2_), channel_id=1, source_target_pairs={{0,1},{1,2},{2,3},{3,0},{4,5},{5,6},{6,7},{7,4},{8,9},{9,10},{10,1... | collective-permute-start | bytes 983048 | tf_op jit(solution)/shard_map/ppermute | solution.py:479
  142.3 28.3 %collective-permute-start.15 = (bf16[640,256]{1,0:T(8,128)(2,1)}, bf16[640,256]{1,0:T(8,128)(2,1)}, u32[]{:S(2)}, u32[]{:S(2)}) collective-permute-start(bf16[640,256]{1,0:T(8,128)(2,1)} %collective-permute-done.13.refs_5_), channel_id=1, source_target_pairs={{0,3},{1,0},{2,1},{3,2},{4,7},{5,4},{6,5},{7,6},{8,11},{9,8},{10,9... | collective-permute-start | bytes 983048 | tf_op jit(solution)/shard_map/ppermute | solution.py:479
  158.4 48.1 %all-to-all-start.3 = ((bf16[128,40,256]{2,1,0:T(8,128)(2,1)}), bf16[128,40,256]{2,1,0:T(8,128)(2,1)S(1)}, u32[]{:S(2)}, u32[]{:S(2)}) async-start(bf16[128,40,256]{2,1,0:T(8,128)(2,1)} %bitcast.43), calls=%async_computation.3 | async-start | bytes 5242880 | tf_op jit(solution)/shard_map/all_to_all | solution.py:567
  180.3 6.8 %copy-start.13 = (bf16[2,4,16,64,256]{4,3,2,1,0:T(8,128)(2,1)S(1)}, bf16[2,4,16,64,256]{4,3,2,1,0:T(8,128)(2,1)}, u32[]{:S(2)}) copy-start(bf16[2,4,16,64,256]{4,3,2,1,0:T(8,128)(2,1)} %proj.1) | copy-start | bytes 12582916
  182.1 4.9 %collective-permute-start.16 = (bf16[4,16,64,256]{3,2,1,0:T(8,128)(2,1)S(1)}, bf16[4,16,64,256]{3,2,1,0:T(8,128)(2,1)S(1)}, u32[]{:S(2)}, u32[]{:S(2)}) collective-permute-start(bf16[4,16,64,256]{3,2,1,0:T(8,128)(2,1)S(1)} %slice_bitcast_fusion), channel_id=1, source_target_pairs={{0,4},{4,0},{1,5},{5,1},{2,6},{6,2},{3,7},{7,3},{8,12},{12,8},{9,1... | collective-permute-start | bytes 6291464 | tf_op jit(solution)/shard_map/ppermute | solution.py:577
  206.5 58.0 %all-to-all-start.2 = ((bf16[64,64,256]{2,1,0:T(8,128)(2,1)}), bf16[64,64,256]{2,1,0:T(8,128)(2,1)}, u32[]{:S(2)}, u32[]{:S(2)}) async-start(bf16[64,64,256]{2,1,0:T(8,128)(2,1)} %bitcast.40), calls=%async_computation.2 | async-start | bytes 4194304 | tf_op jit(solution)/shard_map/all_to_all | solution.py:579
  215.7 35.0 %copy-start.1 = (bf16[16,40,640]{2,1,0:T(8,128)(2,1)S(1)}, bf16[16,40,640]{2,1,0:T(8,128)(2,1)}, u32[]{:S(2)}) copy-start(bf16[16,40,640]{2,1,0:T(8,128)(2,1)} %copy-done) | copy-start | bytes 2457604
  215.7 35.0 %copy-start.3 = (bf16[640,640]{1,0:T(8,128)(2,1)S(1)}, bf16[640,640]{1,0:T(8,128)(2,1)}, u32[]{:S(2)}) copy-start(bf16[640,640]{1,0:T(8,128)(2,1)} %copy-done.2) | copy-start | bytes 2457604
  215.7 35.0 %copy-start.5 = (bf16[640,640]{1,0:T(8,128)(2,1)S(1)}, bf16[640,640]{1,0:T(8,128)(2,1)}, u32[]{:S(2)}) copy-start(bf16[640,640]{1,0:T(8,128)(2,1)} %copy-done.4) | copy-start | bytes 2457604
  220.3 11.3 %collective-permute-start.17 = (f32[2,256]{1,0:T(2,128)}, f32[2,256]{1,0:T(2,128)S(1)}, u32[]{:S(2)}, u32[]{:S(2)}) collective-permute-start(f32[2,256]{1,0:T(2,128)} %get-tuple-element.49), channel_id=1, source_target_pairs={{4,0},{8,4},{12,8},{16,12},{20,16},{24,20},{28,24},{32,28},{36,32}... | collective-permute-start | bytes 6152 | tf_op jit(solution)/shard_map/ppermute | solution.py:497
  223.4 8.2 %collective-permute-start.18 = (f32[2,256]{1,0:T(2,128)}, f32[2,256]{1,0:T(2,128)S(1)}, u32[]{:S(2)}, u32[]{:S(2)}) collective-permute-start(f32[2,256]{1,0:T(2,128)} %get-tuple-element.49), channel_id=1, source_target_pairs={{8,0},{12,4},{16,8},{20,12},{24,16},{28,20},{32,24},{36,28},{40,32... | collective-permute-start | bytes 6152 | tf_op jit(solution)/shard_map/ppermute | solution.py:497
  224.7 11.2 %collective-permute-start.19 = (f32[2,256]{1,0:T(2,128)}, f32[2,256]{1,0:T(2,128)S(1)}, u32[]{:S(2)}, u32[]{:S(2)}) collective-permute-start(f32[2,256]{1,0:T(2,128)} %get-tuple-element.49), channel_id=1, source_target_pairs={{12,0},{16,4},{20,8},{24,12},{28,16},{32,20},{36,24},{40,28},{44,3... | collective-permute-start | bytes 6152 | tf_op jit(solution)/shard_map/ppermute | solution.py:497
  226.0 10.0 %collective-permute-start.20 = (f32[2,256]{1,0:T(2,128)}, f32[2,256]{1,0:T(2,128)S(1)}, u32[]{:S(2)}, u32[]{:S(2)}) collective-permute-start(f32[2,256]{1,0:T(2,128)} %get-tuple-element.49), channel_id=1, source_target_pairs={{16,0},{20,4},{24,8},{28,12},{32,16},{36,20},{40,24},{44,28},{48,3... | collective-permute-start | bytes 6152 | tf_op jit(solution)/shard_map/ppermute | solution.py:497
  236.0 6.2 %collective-permute-start.21 = (f32[2,256]{1,0:T(2,128)S(1)}, f32[2,256]{1,0:T(2,128)S(1)}, u32[]{:S(2)}, u32[]{:S(2)}) collective-permute-start(f32[2,256]{1,0:T(2,128)S(1)} %pad_maximum_fusion), channel_id=1, source_target_pairs={{16,0},{20,4},{24,8},{28,12},{32,16},{36,20},{40,24},{44,28},{48,3... | collective-permute-start | bytes 6152 | tf_op jit(solution)/shard_map/ppermute | solution.py:497
  237.3 7.3 %collective-permute-start.22 = (f32[2,256]{1,0:T(2,128)S(1)}, f32[2,256]{1,0:T(2,128)S(1)}, u32[]{:S(2)}, u32[]{:S(2)}) collective-permute-start(f32[2,256]{1,0:T(2,128)S(1)} %pad_maximum_fusion), channel_id=1, source_target_pairs={{32,0},{36,4},{40,8},{44,12},{48,16},{52,20},{56,24},{60,28},{64,3... | collective-permute-start | bytes 6152 | tf_op jit(solution)/shard_map/ppermute | solution.py:497
  238.6 10.7 %collective-permute-start.23 = (f32[2,256]{1,0:T(2,128)S(1)}, f32[2,256]{1,0:T(2,128)S(1)}, u32[]{:S(2)}, u32[]{:S(2)}) collective-permute-start(f32[2,256]{1,0:T(2,128)S(1)} %pad_maximum_fusion), channel_id=1, source_target_pairs={{48,0},{52,4},{56,8},{60,12},{64,16},{68,20},{72,24},{76,28},{80,3... | collective-permute-start | bytes 6152 | tf_op jit(solution)/shard_map/ppermute | solution.py:497
  249.3 12.3 %collective-permute-start.24 = (f32[2,256]{1,0:T(2,128)S(1)}, f32[2,256]{1,0:T(2,128)S(1)}, u32[]{:S(2)}, u32[]{:S(2)}) collective-permute-start(f32[2,256]{1,0:T(2,128)S(1)} %pad_maximum_fusion.1), channel_id=1, source_target_pairs={{64,0},{68,4},{72,8},{76,12},{80,16},{84,20},{88,24},{92,28},{96,3... | collective-permute-start | bytes 6152 | tf_op jit(solution)/shard_map/ppermute | solution.py:497

commit v2 on v1

--- a/solution.py
+++ b/solution.py
@@ -445,25 +445,30 @@
     )(back, *kept(args[1:]))
 
 
-def final_kernel(where_ref, carry, local, exp, ca, ci, cs, map_a, map_i, out):
+def final_kernel(where_ref, *refs):
+    carry = refs[:-8]
+    local, exp, ca, ci, cs, map_a, map_i, out = refs[-8:]
     channels = local.shape[1]
     heads = channels // 128
     first = where_ref[0] * heads
+    total = jnp.zeros((1, channels), F32)
+    for pair in reversed(carry):
+        total = pair[0:1, :] + pair[1:2, :] * total
     for h in range(heads):
         cols = slice(h * 128, (h + 1) * 128)
-        cot = local[:, cols] + exp[:, cols] * carry[0:1, cols]
+        cot = local[:, cols] + exp[:, cols] * total[:, cols]
         a_cot = (cot * ca[:, cols]).astype(BF16)
         i_cot = (cot * ci[:, cols]).astype(BF16)
-        total = (
+        result = (
             cot * cs[:, cols]
             + dot(a_cot, map_a[first + h], ((1,), (1,)))
             + dot(i_cot, map_i[first + h], ((1,), (1,)))
         )
-        out[:, cols] = total.astype(BF16)
+        out[:, cols] = result.astype(BF16)
 
 
 def final(position, carry, local, exp, ca, ci, cs, map_a, map_i):
-    args = (position, carry, local, exp, ca, ci, cs, map_a, map_i)
+    args = (position, *carry, local, exp, ca, ci, cs, map_a, map_i)
     return pl.pallas_call(
         final_kernel,
         out_shape=made(local.shape, BF16),
@@ -472,7 +477,7 @@
         compiler_params=params(8),
         cost_estimate=cost(10**8, 4 * 2**20),
         name="final",
-    )(position, carry, *kept(args[2:]))
+    )(position, *carry, *kept(args[1 + len(carry) :]))
 
 
 def shifted(piece, by):
@@ -503,10 +508,8 @@
 
 def carried(pair, length):
     one, two, three, four = (later(pair, by, length) for by in (1, 2, 3, 4))
-    pair = joined(joined(one, two), joined(three, four))
-    one, two, three = (later(pair, by, length) for by in (4, 8, 12))
-    pair = joined(joined(pair, one), joined(two, three))
-    return joined(pair, later(pair, 16, length))
+    near = joined(joined(one, two), joined(three, four))
+    return [near, *(later(near, by, length) for by in range(4, length, 4))]
 
 
 def per_device(

time: 271 us -> 269 us (level)
  waiting for transfers between devices: 112 us -> 106 us
  starting transfers between devices: 64.7 us -> 68.6 us
    ppermute x8 -> x11, waiting for transfers between devices: 18.1 us -> 11.5 us  [later(): lax.ppermute(pair, ('sq', 'core'), [(i, i - by) for i in range(by, length)])]
    ppermute x8 -> x11, starting transfers between devices: 12.1 us -> 16 us  [later(): lax.ppermute(pair, ('sq', 'core'), [(i, i - by) for i in range(by, length)])]
  transfers between devices with their start and end apart: 29 -> 32, of which waited for: 14 -> 13; matrix products, arithmetic and copies ran while one was open for 6% -> 6% of each run, Pallas kernels for 23% -> 23%
where the time goes in v2:
time: 269 us; the launch traced here: 264 us
  waiting for transfers between devices  106 us (39%)
  starting transfers between devices  68.6 us (26%)
  Pallas kernels  66.3 us (25%)
  local copies, waits for them, and re-layouts  11.9 us (4%)
  matrix products  5.61 us (2%)
  other arithmetic  5.43 us (2%)
    ppermute x16, waiting for transfers between devices, shifted(): return lax.ppermute(piece, 'tp', [(i, (i + by) % 4) for i in range(4)])  65 us
    ppermute x16, starting transfers between devices, shifted(): return lax.ppermute(piece, 'tp', [(i, (i + by) % 4) for i in range(4)])  17.9 us
    all_to_all x1, waiting for transfers between devices, per_device(): lax.all_to_all(mix.reshape(4 * sources, capacity, -1), ('tp', *sp_axes),...  17.2 us
    ppermute x11, starting transfers between devices, later(): lax.ppermute(pair, ('sq', 'core'), [(i, i - by) for i in range(by, length)])  16 us
    all_to_all x2, starting transfers between devices, exchanged(): lax.all_to_all(rows.reshape(sources, capacity, -1), sp_axes, 0, 0, tiled=...  15.5 us
    pallas_call x1, Pallas kernels, expert(): pl.pallas_call(functools.partial(expert_kernel, row_part=row_part), out_s...  13.4 us
    all_to_all x1, starting transfers between devices, per_device(): lax.all_to_all(mix.reshape(4 * sources, capacity, -1), ('tp', *sp_axes),...  12.2 us
    pallas_call x2, Pallas kernels, build(): pl.pallas_call(functools.partial(build_kernel, capacity=capacity, group=g...  11.5 us
  transfers between devices with their start and end apart: 32, of which 13 were waited for; matrix products, arithmetic and copies ran while one was open for 6% of the time, Pallas kernels for 23%

profile of v2, /device:TPU:1, one launch (start us, length us, event | category | flops | bytes accessed | tf_op | source)
XLA Modules:
  0.0 264.4 jit_solution(1695549793139705126)
XLA Ops:
  0.7 4.7 %shard_map.191 = bf16[1280,640]{1,0:T(8,128)(2,1)} custom-call(s32[2]{0:T(128)S(1)} %pad_add_fusion.where_ref, s32[2,512]{1,0:T(2,128)} %bitcast.45, f32[2,512]{1,0:T(2,128)} %bitcast.47, bf16[512,2048]{1,0:T(8,128)(2,1)} %refs_0_.3, bf16[512,2048]{1,0:T(8,128)(2,1)} %refs_1_.3), custom_call_target="tpu_custom_call" | custom-call | flops 896000000 | bytes 3200000 | tf_op jit(solution)/shard_map/pallas_call | solution.py:185
  5.4 9.7 %all-to-all-start.1 = ((bf16[32,40,640]{2,1,0:T(8,128)(2,1)}), bf16[32,40,640]{2,1,0:T(8,128)(2,1)S(1)}, u32[]{:S(2)}, u32[]{:S(2)}) async-start(bf16[32,40,640]{2,1,0:T(8,128)(2,1)} %bitcast.41), calls=%async_computation.1 | async-start | bytes 3276800 | tf_op jit(solution)/shard_map/all_to_all | solution.py:533
  15.2 0.9 copy.22.ids
  16.0 0.9 copy.21
  16.9 0.6 fusion.2.rates
  17.5 6.4 %early.1 = (bf16[512,256]{1,0:T(8,128)(2,1)}, f32[512,256]{1,0:T(8,128)}, f32[512,256]{1,0:T(8,128)}, f32[512,256]{1,0:T(8,128)}, f32[512,256]{1,0:T(8,128)}, /*...) custom-call(s32[2]{0:T(128)S(1)} %pad_add_fusion.where_ref, ...), custom_call_target="tpu_custom_call" | custom-call | flops 3000000000 | bytes 8388608 | tf_op jit(solution)/shard_map/early/pallas_call | solution.py:131
  23.9 6.8 %shard_map.190 = bf16[1280,1792]{1,0:T(8,128)(2,1)} custom-call(s32[2]{0:T(128)S(1)} %pad_add_fusion.where_ref, s32[2,512]{1,0:T(2,128)} %bitcast.46, f32[2,512]{1,0:T(2,128)} %bitcast.48, bf16[512,2048]{1,0:T(8,128)(2,1)} %refs_0_.3, bf16[512,2048]{1,0:T(8,128)(2,1)} %refs_1_.3, bf16[512,256]{1,0:T(8,128)(2,1)} %get-tuple-element.31.refs_2_), custom_call_target="tpu_custom_call" | custom-call | flops 2508800000 | bytes 8960000 | tf_op jit(solution)/shard_map/pallas_call | solution.py:185
  30.8 8.0 %all-to-all-done.1 = bf16[32,40,640]{2,1,0:T(8,128)(2,1)S(1)} async-done(((bf16[32,40,640]{2,1,0:T(8,128)(2,1)}), bf16[32,40,640]{2,1,0:T(8,128)(2,1)S(1)}, u32[]{:S(2)}, u32[]{:S(2)}) %all-to-all-start.1) | async-done | bytes 1638432 | tf_op jit(solution)/shard_map/all_to_all | solution.py:533
  38.8 5.8 %all-to-all-start = ((bf16[32,40,1792]{2,1,0:T(8,128)(2,1)}), bf16[32,40,1792]{2,1,0:T(8,128)(2,1)}, u32[]{:S(2)}, u32[]{:S(2)}) async-start(bf16[32,40,1792]{2,1,0:T(8,128)(2,1)} %bitcast.42), calls=%async_computation | async-start | bytes 9175040 | tf_op jit(solution)/shard_map/all_to_all | solution.py:533
  44.6 1.3 collective-permute-start.6
  45.9 1.5 collective-permute-start.7
  47.6 2.7 %collective-permute-start.3 = (bf16[640,640]{1,0:T(8,128)(2,1)S(1)}, bf16[640,640]{1,0:T(8,128)(2,1)S(1)}, u32[]{:S(2)}, u32[]{:S(2)}) collective-permute-start(bf16[640,640]{1,0:T(8,128)(2,1)S(1)} %bitcast.32), channel_id=1, source_target_pairs={{0,3},{1,0},{2,1},{3,2},{4,7},{5,4},{6,5},{7,6},{8,11},{9,8},{10,9... | collective-permute-start | bytes 2457608 | tf_op jit(solution)/shard_map/ppermute | solution.py:484
  50.2 20.2 %collective-permute-done.6.left = bf16[2048,256]{1,0:T(8,128)(2,1)S(1)} collective-permute-done((bf16[2048,256]{1,0:T(8,128)(2,1)}, bf16[2048,256]{1,0:T(8,128)(2,1)S(1)}, u32[]{:S(2)}, u32[]{:S(2)}) %collective-permute-start.6) | collective-permute-done | bytes 1048608 | tf_op jit(solution)/shard_map/ppermute | solution.py:484
  70.6 1.2 collective-permute-start.1
  71.8 0.9 slice.77
  72.7 1.0 copy-done.8
  73.6 1.5 collective-permute-start.9
  75.2 24.0 %collective-permute-done.8.far_top = bf16[1024,256]{1,0:T(8,128)(2,1)S(1)} collective-permute-done((bf16[1024,256]{1,0:T(8,128)(2,1)S(1)}, bf16[1024,256]{1,0:T(8,128)(2,1)S(1)}, u32[]{:S(2)}, u32[]{:S(2)}) %collective-permute-start.8) | collective-permute-done | bytes 524320 | tf_op jit(solution)/shard_map/ppermute | solution.py:484
  99.2 0.8 copy-done.10
  100.0 1.4 collective-permute-start.2
  101.4 2.7 %collective-permute-start.5 = (bf16[640,640]{1,0:T(8,128)(2,1)S(1)}, bf16[640,640]{1,0:T(8,128)(2,1)}, u32[]{:S(2)}, u32[]{:S(2)}) collective-permute-start(bf16[640,640]{1,0:T(8,128)(2,1)S(1)} %collective-permute-done.3.refs_5_), channel_id=1, source_target_pairs={{0,3},{1,0},{2,1},{3,2},{4,7},{5,4},{6,5},{7,6},{8,11},{9,8},{10,9... | collective-permute-start | bytes 2457608 | tf_op jit(solution)/shard_map/ppermute | solution.py:484
  104.1 2.2 convolution_bitcast_fusion.local
  106.4 2.0 fusion.8
  108.3 8.5 %collective-permute-done.1.refs_3_ = bf16[640,640]{1,0:T(8,128)(2,1)} collective-permute-done((bf16[640,640]{1,0:T(8,128)(2,1)S(1)}, bf16[640,640]{1,0:T(8,128)(2,1)}, u32[]{:S(2)}, u32[]{:S(2)}) %collective-permute-start.1) | collective-permute-done | bytes 819232 | tf_op jit(solution)/shard_map/ppermute | solution.py:484
  116.8 1.3 collective-permute-start.13
  118.1 1.2 copy-done.7
  119.3 1.2 copy-done.9
  120.6 1.0 copy-done.11
  121.6 6.9 %folded.1 = (bf16[2048,512]{1,0:T(8,128)(2,1)}, bf16[2048,256]{1,0:T(8,128)(2,1)}, bf16[4,256,256]{2,1,0:T(8,128)(2,1)}, bf16[4,256,256]{2,1,0:T(8,128)(2,1)}) custom-call(s32[2]{0:T(128)S(1)} %pad_add_fusion.where_ref, bf16[2048,256]{1,0:T(8,128)(2,1)} %bitcast.50, bf16[2048,256]{1,0:T(8,128)(2,1)} %bitcast.52, bf16[256,2048]{1,0:T(8,128)(2,1)} %bitcast.49, ...), custom_call_target="tpu_custom_call" | custom-call | flops 4000000000 | bytes 7340032 | tf_op jit(solution)/shard_map/folded/pallas_call | solution.py:247
  128.5 0.3 collective-permute-start.11
  128.8 5.6 %collective-permute-done.4.refs_6_ = bf16[640,640]{1,0:T(8,128)(2,1)} collective-permute-done((bf16[640,640]{1,0:T(8,128)(2,1)S(1)}, bf16[640,640]{1,0:T(8,128)(2,1)}, u32[]{:S(2)}, u32[]{:S(2)}) %collective-permute-start.4) | collective-permute-done | bytes 819232 | tf_op jit(solution)/shard_map/ppermute | solution.py:484
  134.4 1.3 collective-permute-start.12
  135.7 5.7 %collective-permute-done.10.refs_2_ = bf16[640,256]{1,0:T(8,128)(2,1)} collective-permute-done((bf16[640,256]{1,0:T(8,128)(2,1)}, bf16[640,256]{1,0:T(8,128)(2,1)}, u32[]{:S(2)}, u32[]{:S(2)}) %collective-permute-start.10) | collective-permute-done | bytes 327712 | tf_op jit(solution)/shard_map/ppermute | solution.py:484
  141.4 0.9 collective-permute-done.13.refs_5_
  142.3 2.7 %collective-permute-start.15 = (bf16[640,256]{1,0:T(8,128)(2,1)}, bf16[640,256]{1,0:T(8,128)(2,1)}, u32[]{:S(2)}, u32[]{:S(2)}) collective-permute-start(bf16[640,256]{1,0:T(8,128)(2,1)} %collective-permute-done.13.refs_5_), channel_id=1, source_target_pairs={{0,3},{1,0},{2,1},{3,2},{4,7},{5,4},{6,5},{7,6},{8,11},{9,8},{10,9... | collective-permute-start | bytes 983048 | tf_op jit(solution)/shard_map/ppermute | solution.py:484
  145.0 13.4 %expert.1 = (bf16[1280,256]{1,0:T(8,128)(2,1)}, bf16[1280,256]{1,0:T(8,128)(2,1)}, bf16[1280,256]{1,0:T(8,128)(2,1)}, bf16[4,1280,256]{2,1,0:T(8,128)(2,1)}) custom-call(bf16[1280,1792]{1,0:T(8,128)(2,1)} %bitcast.7.got_rows.got_cot, bf16[1280,1792]{1,0:T(8,128)(2,1)} %bitcast.7.got_rows.got_cot, bf16[640,640]{1,0:T(8,128)(2,1)S(1)} %bitcast.38, ...), custom_call_target="tpu_custom_call" | custom-call | flops 7000000000 | bytes 18874368 | tf_op jit(solution)/shard_map/expert/pallas_call | solution.py:291
  158.4 12.2 %all-to-all-start.3 = ((bf16[128,40,256]{2,1,0:T(8,128)(2,1)}), bf16[128,40,256]{2,1,0:T(8,128)(2,1)S(1)}, u32[]{:S(2)}, u32[]{:S(2)}) async-start(bf16[128,40,256]{2,1,0:T(8,128)(2,1)} %bitcast.43), calls=%async_computation.3 | async-start | bytes 5242880 | tf_op jit(solution)/shard_map/all_to_all | solution.py:570
  170.6 9.7 %proj.1 = bf16[2,4,16,64,256]{4,3,2,1,0:T(8,128)(2,1)} custom-call(s32[2]{0:T(128)S(1)} %pad_add_fusion.where_ref, bf16[1280,256]{1,0:T(8,128)(2,1)} %get-tuple-element.37.refs_9_.gate_cot, bf16[1280,256]{1,0:T(8,128)(2,1)} %get-tuple-element.38.refs_10_.up_cot, bf16[2048,256]{1,0:T(8,128)(2,1)} %bitcast.51, bf16[2048,256]{1,0:T(8,128)(2,1)} %bitcast.53, ...), custom_call_target="tpu_custom_call" | custom-call | flops 4000000000 | bytes 14680064 | tf_op jit(solution)/shard_map/proj/pallas_call | solution.py:387
  180.3 1.9 slice_bitcast_fusion
  182.2 1.1 collective-permute-start.16
  183.3 3.8 %collective-permute-done.16 = bf16[4,16,64,256]{3,2,1,0:T(8,128)(2,1)S(1)} collective-permute-done((bf16[4,16,64,256]{3,2,1,0:T(8,128)(2,1)S(1)}, bf16[4,16,64,256]{3,2,1,0:T(8,128)(2,1)S(1)}, u32[]{:S(2)}, u32[]{:S(2)}) %collective-permute-start.16) | collective-permute-done | bytes 2097184 | tf_op jit(solution)/shard_map/ppermute | solution.py:580
  187.1 2.2 fusion
  189.3 17.2 %all-to-all-done.3 = bf16[128,40,256]{2,1,0:T(8,128)(2,1)S(1)} async-done(((bf16[128,40,256]{2,1,0:T(8,128)(2,1)}), bf16[128,40,256]{2,1,0:T(8,128)(2,1)S(1)}, u32[]{:S(2)}, u32[]{:S(2)}) %all-to-all-start.3) | async-done | bytes 2621472 | tf_op jit(solution)/shard_map/all_to_all | solution.py:570
  206.5 5.8 %all-to-all-start.2 = ((bf16[64,64,256]{2,1,0:T(8,128)(2,1)}), bf16[64,64,256]{2,1,0:T(8,128)(2,1)}, u32[]{:S(2)}, u32[]{:S(2)}) async-start(bf16[64,64,256]{2,1,0:T(8,128)(2,1)} %bitcast.40), calls=%async_computation.2 | async-start | bytes 4194304 | tf_op jit(solution)/shard_map/all_to_all | solution.py:582
  212.3 3.4 %fusion.10.base = f32[512,256]{1,0:T(8,128)} fusion(bf16[512,2048]{1,0:T(8,128)(2,1)} %refs_1_.3, bf16[2048,256]{1,0:T(8,128)(2,1)} %own.1), kind=kOutput, calls=%fused_computation.22 | convolution fusion | flops 536870912 | bytes 3670016 | tf_op jit(solution)/shard_map/dot_general | solution.py:563
  215.7 4.6 %scanned.1 = (bf16[512,256]{1,0:T(8,128)(2,1)}, f32[512,256]{1,0:T(8,128)}, f32[2,256]{1,0:T(2,128)}) custom-call(bf16[4,1280,256]{2,1,0:T(8,128)(2,1)S(1)} %bitcast.31, bf16[512,1280]{1,0:T(8,128)(2,1)} %get-tuple-element.43.sel, f32[512,256]{1,0:T(8,128)} %fusion.10.base, f32[512,256]{1,0:T(8,128)} %get-tuple-element.44.act, ...), custom_call_target="tpu_custom_call" | custom-call | flops 400000000 | bytes 8388608 | tf_op jit(solution)/shard_map/scanned/pallas_call | solution.py:436
  220.3 3.1 %collective-permute-start.17 = (f32[2,256]{1,0:T(2,128)}, f32[2,256]{1,0:T(2,128)S(1)}, u32[]{:S(2)}, u32[]{:S(2)}) collective-permute-start(f32[2,256]{1,0:T(2,128)} %get-tuple-element.49), channel_id=1, source_target_pairs={{4,0},{8,4},{12,8},{16,12},{20,16},{24,20},{28,24},{32,28},{36,32}... | collective-permute-start | bytes 6152 | tf_op jit(solution)/shard_map/ppermute | solution.py:502
  223.4 1.3 collective-permute-start.18
  224.7 1.3 collective-permute-start.19
  226.0 1.3 collective-permute-start.20
  227.3 4.3 %collective-permute-done.17 = f32[2,256]{1,0:T(2,128)S(1)} collective-permute-done((f32[2,256]{1,0:T(2,128)}, f32[2,256]{1,0:T(2,128)S(1)}, u32[]{:S(2)}, u32[]{:S(2)}) %collective-permute-start.17) | collective-permute-done | bytes 2080 | tf_op jit(solution)/shard_map/ppermute | solution.py:502
  231.6 4.3 %collective-permute-done.19 = f32[2,256]{1,0:T(2,128)S(1)} collective-permute-done((f32[2,256]{1,0:T(2,128)}, f32[2,256]{1,0:T(2,128)S(1)}, u32[]{:S(2)}, u32[]{:S(2)}) %collective-permute-start.19) | collective-permute-done | bytes 2080 | tf_op jit(solution)/shard_map/ppermute | solution.py:502
  236.0 1.3 collective-permute-start.21
  237.3 1.3 collective-permute-start.22
  238.6 1.3 collective-permute-start.23
  239.9 1.3 collective-permute-start.24
  241.2 1.3 collective-permute-start.25
  242.5 1.3 collective-permute-start.26
  243.8 0.8 collective-permute-done.22.refs_2_
  244.6 1.3 collective-permute-start.27
  245.9 11.0 %grads.1 = (f32[1,2048,256]{2,1,0:T(8,128)}, f32[1,2048,256]{2,1,0:T(8,128)}, f32[1,256,2048]{2,1,0:T(8,128)}) custom-call(s32[2]{0:T(128)S(1)} %pad_add_fusion.where_ref, bf16[1280,1792]{1,0:T(8,128)(2,1)} %bitcast.7.got_rows.got_cot, bf16[1280,1792]{1,0:T(8,128)(2,1)} %bitcast.7.got_rows.got_cot, bf16[640,640]{1,0:T(8,128)(2,1)S(1)} %bitcast.39, ...), custom_call_target="tpu_custom_call" | custom-call | flops 4000000000 | bytes 17825792 | tf_op jit(solution)/shard_map/grads/pallas_call | solution.py:341
  256.9 2.1 collective-permute-done.27.refs_7_
  259.0 2.8 %final.1 = bf16[512,256]{1,0:T(8,128)(2,1)} custom-call(s32[2]{0:T(128)S(1)} %pad_add_fusion.where_ref, f32[2,256]{1,0:T(2,128)S(1)} %pad_maximum_fusion.refs_0_, f32[2,256]{1,0:T(2,128)S(1)} %collective-permute-done.21.refs_1_, f32[2,256]{1,0:T(2,128)S(1)} %collective-permute-done.22.refs_2_, f32[2,256]{1,0:T(2,128)S(1)} %collective-permute-done.23.refs_3_, ...), custom_call_target="tpu_custom_call" | custom-call | flops 100000000 | bytes 4194304 | tf_op jit(solution)/shard_map/final/pallas_call | solution.py:472
  261.8 2.5 convert_reduce_fusion
  (60 shorter events, 0.6 us)
Async XLA Ops:
  5.4 9.8 %copy-start.15 = (s32[512,2]{0,1:T(2,128)S(1)}, s32[512,2]{0,1:T(2,128)}, u32[]{:S(2)}) copy-start(s32[512,2]{0,1:T(2,128)} %param.17) | copy-start | bytes 12292
  5.4 10.6 %copy-start.16 = (f32[2,512]{1,0:T(2,128)S(1)}, f32[2,512]{1,0:T(2,128)}, u32[]{:S(2)}) copy-start(f32[2,512]{1,0:T(2,128)} %param.27) | copy-start | bytes 12292
  5.4 11.5 %copy-start.17 = (f32[1024]{0:T(1024)S(1)}, f32[1024]{0:T(1024)}, u32[]{:S(2)}) copy-start(f32[1024]{0:T(1024)} %param.26) | copy-start | bytes 12292
  5.4 33.3 %all-to-all-start.1 = ((bf16[32,40,640]{2,1,0:T(8,128)(2,1)}), bf16[32,40,640]{2,1,0:T(8,128)(2,1)S(1)}, u32[]{:S(2)}, u32[]{:S(2)}) async-start(bf16[32,40,640]{2,1,0:T(8,128)(2,1)} %bitcast.41), calls=%async_computation.1 | async-start | bytes 3276800 | tf_op jit(solution)/shard_map/all_to_all | solution.py:533
  38.8 67.6 %all-to-all-start = ((bf16[32,40,1792]{2,1,0:T(8,128)(2,1)}), bf16[32,40,1792]{2,1,0:T(8,128)(2,1)}, u32[]{:S(2)}, u32[]{:S(2)}) async-start(bf16[32,40,1792]{2,1,0:T(8,128)(2,1)} %bitcast.42), calls=%async_computation | async-start | bytes 9175040 | tf_op jit(solution)/shard_map/all_to_all | solution.py:533
  44.6 59.5 %copy-start.12 = (bf16[512,2048]{1,0:T(8,128)(2,1)S(1)}, bf16[512,2048]{1,0:T(8,128)(2,1)}, u32[]{:S(2)}) copy-start(bf16[512,2048]{1,0:T(8,128)(2,1)} %refs_1_.3) | copy-start | bytes 6291460
  44.6 59.5 %copy-start.14 = (bf16[512,256]{1,0:T(8,128)(2,1)S(1)}, bf16[512,256]{1,0:T(8,128)(2,1)}, u32[]{:S(2)}) copy-start(bf16[512,256]{1,0:T(8,128)(2,1)} %get-tuple-element.31.refs_2_) | copy-start | bytes 786436
  44.6 25.9 %collective-permute-start.6 = (bf16[2048,256]{1,0:T(8,128)(2,1)}, bf16[2048,256]{1,0:T(8,128)(2,1)S(1)}, u32[]{:S(2)}, u32[]{:S(2)}) collective-permute-start(bf16[2048,256]{1,0:T(8,128)(2,1)} %own.1), channel_id=1, source_target_pairs={{0,1},{1,2},{2,3},{3,0},{4,5},{5,6},{6,7},{7,4},{8,9},{9,10},{10,1... | collective-permute-start | bytes 3145736 | tf_op jit(solution)/shard_map/ppermute | solution.py:484
  45.9 25.9 %collective-permute-start.7 = (bf16[2048,256]{1,0:T(8,128)(2,1)}, bf16[2048,256]{1,0:T(8,128)(2,1)S(1)}, u32[]{:S(2)}, u32[]{:S(2)}) collective-permute-start(bf16[2048,256]{1,0:T(8,128)(2,1)} %own.1), channel_id=1, source_target_pairs={{0,3},{1,0},{2,1},{3,2},{4,7},{5,4},{6,5},{7,6},{8,11},{9,8},{10,9... | collective-permute-start | bytes 3145736 | tf_op jit(solution)/shard_map/ppermute | solution.py:484
  47.5 97.5 %copy-start = (bf16[16,40,640]{2,1,0:T(8,128)(2,1)}, bf16[16,40,640]{2,1,0:T(8,128)(2,1)S(1)}, u32[]{:S(2)}) copy-start(bf16[16,40,640]{2,1,0:T(8,128)(2,1)S(1)} %get-tuple-element.59) | copy-start | bytes 2457604
  47.5 53.9 %collective-permute-start = (bf16[640,640]{1,0:T(8,128)(2,1)S(1)}, bf16[640,640]{1,0:T(8,128)(2,1)S(1)}, u32[]{:S(2)}, u32[]{:S(2)}) collective-permute-start(bf16[640,640]{1,0:T(8,128)(2,1)S(1)} %bitcast.36), channel_id=1, source_target_pairs={{0,1},{1,2},{2,3},{3,0},{4,5},{5,6},{6,7},{7,4},{8,9},{9,10},{10,1... | collective-permute-start | bytes 2457608 | tf_op jit(solution)/shard_map/ppermute | solution.py:484
  47.6 53.9 %collective-permute-start.3 = (bf16[640,640]{1,0:T(8,128)(2,1)S(1)}, bf16[640,640]{1,0:T(8,128)(2,1)S(1)}, u32[]{:S(2)}, u32[]{:S(2)}) collective-permute-start(bf16[640,640]{1,0:T(8,128)(2,1)S(1)} %bitcast.32), channel_id=1, source_target_pairs={{0,3},{1,0},{2,1},{3,2},{4,7},{5,4},{6,5},{7,6},{8,11},{9,8},{10,9... | collective-permute-start | bytes 2457608 | tf_op jit(solution)/shard_map/ppermute | solution.py:484
  70.5 31.0 %copy-start.6 = (bf16[2048,256]{1,0:T(8,128)(2,1)}, bf16[2048,256]{1,0:T(8,128)(2,1)S(1)}, u32[]{:S(2)}) copy-start(bf16[2048,256]{1,0:T(8,128)(2,1)S(1)} %collective-permute-done.6.left) | copy-start | bytes 3145732
  70.5 28.6 %collective-permute-start.8 = (bf16[1024,256]{1,0:T(8,128)(2,1)S(1)}, bf16[1024,256]{1,0:T(8,128)(2,1)S(1)}, u32[]{:S(2)}, u32[]{:S(2)}) collective-permute-start(bf16[1024,256]{1,0:T(8,128)(2,1)S(1)} %slice.76), channel_id=1, source_target_pairs={{0,1},{1,2},{2,3},{3,0},{4,5},{5,6},{6,7},{7,4},{8,9},{9,10},{10,1... | collective-permute-start | bytes 1572872 | tf_op jit(solution)/shard_map/ppermute | solution.py:484
  70.6 46.2 %collective-permute-start.1 = (bf16[640,640]{1,0:T(8,128)(2,1)S(1)}, bf16[640,640]{1,0:T(8,128)(2,1)}, u32[]{:S(2)}, u32[]{:S(2)}) collective-permute-start(bf16[640,640]{1,0:T(8,128)(2,1)S(1)} %bitcast.33), channel_id=1, source_target_pairs={{0,1},{1,2},{2,3},{3,0},{4,5},{5,6},{6,7},{7,4},{8,9},{9,10},{10,1... | collective-permute-start | bytes 2457608 | tf_op jit(solution)/shard_map/ppermute | solution.py:484
  72.7 1.0 copy-start.8
  73.6 34.7 %collective-permute-start.9 = (bf16[1024,256]{1,0:T(8,128)(2,1)}, bf16[1024,256]{1,0:T(8,128)(2,1)}, u32[]{:S(2)}, u32[]{:S(2)}) collective-permute-start(bf16[1024,256]{1,0:T(8,128)(2,1)} %slice.77), channel_id=1, source_target_pairs={{0,3},{1,0},{2,1},{3,2},{4,7},{5,4},{6,5},{7,6},{8,11},{9,8},{10,9... | collective-permute-start | bytes 1572872 | tf_op jit(solution)/shard_map/ppermute | solution.py:484
  99.2 0.8 copy-start.10
  100.0 28.5 %collective-permute-start.2 = (bf16[640,640]{1,0:T(8,128)(2,1)S(1)}, bf16[640,640]{1,0:T(8,128)(2,1)}, u32[]{:S(2)}, u32[]{:S(2)}) collective-permute-start(bf16[640,640]{1,0:T(8,128)(2,1)S(1)} %bitcast.37), channel_id=1, source_target_pairs={{0,3},{1,0},{2,1},{3,2},{4,7},{5,4},{6,5},{7,6},{8,11},{9,8},{10,9... | collective-permute-start | bytes 2457608 | tf_op jit(solution)/shard_map/ppermute | solution.py:484
  101.3 43.7 %copy-start.2 = (bf16[640,640]{1,0:T(8,128)(2,1)}, bf16[640,640]{1,0:T(8,128)(2,1)S(1)}, u32[]{:S(2)}) copy-start(bf16[640,640]{1,0:T(8,128)(2,1)S(1)} %collective-permute-done.refs_2_) | copy-start | bytes 2457604
  101.3 33.0 %collective-permute-start.4 = (bf16[640,640]{1,0:T(8,128)(2,1)S(1)}, bf16[640,640]{1,0:T(8,128)(2,1)}, u32[]{:S(2)}, u32[]{:S(2)}) collective-permute-start(bf16[640,640]{1,0:T(8,128)(2,1)S(1)} %collective-permute-done.refs_2_), channel_id=1, source_target_pairs={{0,1},{1,2},{2,3},{3,0},{4,5},{5,6},{6,7},{7,4},{8,9},{9,10},{10,1... | collective-permute-start | bytes 2457608 | tf_op jit(solution)/shard_map/ppermute | solution.py:484
  101.4 43.6 %copy-start.4 = (bf16[640,640]{1,0:T(8,128)(2,1)}, bf16[640,640]{1,0:T(8,128)(2,1)S(1)}, u32[]{:S(2)}) copy-start(bf16[640,640]{1,0:T(8,128)(2,1)S(1)} %collective-permute-done.3.refs_5_) | copy-start | bytes 2457604
  101.4 43.6 %collective-permute-start.5 = (bf16[640,640]{1,0:T(8,128)(2,1)S(1)}, bf16[640,640]{1,0:T(8,128)(2,1)}, u32[]{:S(2)}, u32[]{:S(2)}) collective-permute-start(bf16[640,640]{1,0:T(8,128)(2,1)S(1)} %collective-permute-done.3.refs_5_), channel_id=1, source_target_pairs={{0,3},{1,0},{2,1},{3,2},{4,7},{5,4},{6,5},{7,6},{8,11},{9,8},{10,9... | collective-permute-start | bytes 2457608 | tf_op jit(solution)/shard_map/ppermute | solution.py:484
  108.3 33.1 %collective-permute-start.10 = (bf16[640,256]{1,0:T(8,128)(2,1)}, bf16[640,256]{1,0:T(8,128)(2,1)}, u32[]{:S(2)}, u32[]{:S(2)}) collective-permute-start(bf16[640,256]{1,0:T(8,128)(2,1)} %get-tuple-element.57.refs_0_), channel_id=1, source_target_pairs={{0,1},{1,2},{2,3},{3,0},{4,5},{5,6},{6,7},{7,4},{8,9},{9,10},{10,1... | collective-permute-start | bytes 983048 | tf_op jit(solution)/shard_map/ppermute | solution.py:484
  116.8 25.5 %collective-permute-start.13 = (bf16[640,256]{1,0:T(8,128)(2,1)}, bf16[640,256]{1,0:T(8,128)(2,1)}, u32[]{:S(2)}, u32[]{:S(2)}) collective-permute-start(bf16[640,256]{1,0:T(8,128)(2,1)} %get-tuple-element.56.refs_1_), channel_id=1, source_target_pairs={{0,3},{1,0},{2,1},{3,2},{4,7},{5,4},{6,5},{7,6},{8,11},{9,8},{10,9... | collective-permute-start | bytes 983048 | tf_op jit(solution)/shard_map/ppermute | solution.py:484
  118.1 1.2 copy-start.7
  119.3 1.2 copy-start.9
  120.6 1.0 copy-start.11
  128.5 42.1 %collective-permute-start.11 = (bf16[640,256]{1,0:T(8,128)(2,1)}, bf16[640,256]{1,0:T(8,128)(2,1)}, u32[]{:S(2)}, u32[]{:S(2)}) collective-permute-start(bf16[640,256]{1,0:T(8,128)(2,1)} %get-tuple-element.56.refs_1_), channel_id=1, source_target_pairs={{0,1},{1,2},{2,3},{3,0},{4,5},{5,6},{6,7},{7,4},{8,9},{9,10},{10,1... | collective-permute-start | bytes 983048 | tf_op jit(solution)/shard_map/ppermute | solution.py:484
  134.4 36.2 %collective-permute-start.12 = (bf16[640,256]{1,0:T(8,128)(2,1)}, bf16[640,256]{1,0:T(8,128)(2,1)}, u32[]{:S(2)}, u32[]{:S(2)}) collective-permute-start(bf16[640,256]{1,0:T(8,128)(2,1)} %get-tuple-element.57.refs_0_), channel_id=1, source_target_pairs={{0,3},{1,0},{2,1},{3,2},{4,7},{5,4},{6,5},{7,6},{8,11},{9,8},{10,9... | collective-permute-start | bytes 983048 | tf_op jit(solution)/shard_map/ppermute | solution.py:484
  141.4 29.2 %collective-permute-start.14 = (bf16[640,256]{1,0:T(8,128)(2,1)}, bf16[640,256]{1,0:T(8,128)(2,1)}, u32[]{:S(2)}, u32[]{:S(2)}) collective-permute-start(bf16[640,256]{1,0:T(8,128)(2,1)} %collective-permute-done.10.refs_2_), channel_id=1, source_target_pairs={{0,1},{1,2},{2,3},{3,0},{4,5},{5,6},{6,7},{7,4},{8,9},{9,10},{10,1... | collective-permute-start | bytes 983048 | tf_op jit(solution)/shard_map/ppermute | solution.py:484
  142.3 28.3 %collective-permute-start.15 = (bf16[640,256]{1,0:T(8,128)(2,1)}, bf16[640,256]{1,0:T(8,128)(2,1)}, u32[]{:S(2)}, u32[]{:S(2)}) collective-permute-start(bf16[640,256]{1,0:T(8,128)(2,1)} %collective-permute-done.13.refs_5_), channel_id=1, source_target_pairs={{0,3},{1,0},{2,1},{3,2},{4,7},{5,4},{6,5},{7,6},{8,11},{9,8},{10,9... | collective-permute-start | bytes 983048 | tf_op jit(solution)/shard_map/ppermute | solution.py:484
  158.4 48.1 %all-to-all-start.3 = ((bf16[128,40,256]{2,1,0:T(8,128)(2,1)}), bf16[128,40,256]{2,1,0:T(8,128)(2,1)S(1)}, u32[]{:S(2)}, u32[]{:S(2)}) async-start(bf16[128,40,256]{2,1,0:T(8,128)(2,1)} %bitcast.43), calls=%async_computation.3 | async-start | bytes 5242880 | tf_op jit(solution)/shard_map/all_to_all | solution.py:570
  180.3 6.8 %copy-start.13 = (bf16[2,4,16,64,256]{4,3,2,1,0:T(8,128)(2,1)S(1)}, bf16[2,4,16,64,256]{4,3,2,1,0:T(8,128)(2,1)}, u32[]{:S(2)}) copy-start(bf16[2,4,16,64,256]{4,3,2,1,0:T(8,128)(2,1)} %proj.1) | copy-start | bytes 12582916
  182.2 4.9 %collective-permute-start.16 = (bf16[4,16,64,256]{3,2,1,0:T(8,128)(2,1)S(1)}, bf16[4,16,64,256]{3,2,1,0:T(8,128)(2,1)S(1)}, u32[]{:S(2)}, u32[]{:S(2)}) collective-permute-start(bf16[4,16,64,256]{3,2,1,0:T(8,128)(2,1)S(1)} %slice_bitcast_fusion), channel_id=1, source_target_pairs={{0,4},{4,0},{1,5},{5,1},{2,6},{6,2},{3,7},{7,3},{8,12},{12,8},{9,1... | collective-permute-start | bytes 6291464 | tf_op jit(solution)/shard_map/ppermute | solution.py:580
  206.5 55.3 %all-to-all-start.2 = ((bf16[64,64,256]{2,1,0:T(8,128)(2,1)}), bf16[64,64,256]{2,1,0:T(8,128)(2,1)}, u32[]{:S(2)}, u32[]{:S(2)}) async-start(bf16[64,64,256]{2,1,0:T(8,128)(2,1)} %bitcast.40), calls=%async_computation.2 | async-start | bytes 4194304 | tf_op jit(solution)/shard_map/all_to_all | solution.py:582
  215.7 30.2 %copy-start.1 = (bf16[16,40,640]{2,1,0:T(8,128)(2,1)S(1)}, bf16[16,40,640]{2,1,0:T(8,128)(2,1)}, u32[]{:S(2)}) copy-start(bf16[16,40,640]{2,1,0:T(8,128)(2,1)} %copy-done) | copy-start | bytes 2457604
  215.7 30.2 %copy-start.3 = (bf16[640,640]{1,0:T(8,128)(2,1)S(1)}, bf16[640,640]{1,0:T(8,128)(2,1)}, u32[]{:S(2)}) copy-start(bf16[640,640]{1,0:T(8,128)(2,1)} %copy-done.2) | copy-start | bytes 2457604
  215.7 30.2 %copy-start.5 = (bf16[640,640]{1,0:T(8,128)(2,1)S(1)}, bf16[640,640]{1,0:T(8,128)(2,1)}, u32[]{:S(2)}) copy-start(bf16[640,640]{1,0:T(8,128)(2,1)} %copy-done.4) | copy-start | bytes 2457604
  220.3 11.3 %collective-permute-start.17 = (f32[2,256]{1,0:T(2,128)}, f32[2,256]{1,0:T(2,128)S(1)}, u32[]{:S(2)}, u32[]{:S(2)}) collective-permute-start(f32[2,256]{1,0:T(2,128)} %get-tuple-element.49), channel_id=1, source_target_pairs={{4,0},{8,4},{12,8},{16,12},{20,16},{24,20},{28,24},{32,28},{36,32}... | collective-permute-start | bytes 6152 | tf_op jit(solution)/shard_map/ppermute | solution.py:502
  223.4 8.2 %collective-permute-start.18 = (f32[2,256]{1,0:T(2,128)}, f32[2,256]{1,0:T(2,128)S(1)}, u32[]{:S(2)}, u32[]{:S(2)}) collective-permute-start(f32[2,256]{1,0:T(2,128)} %get-tuple-element.49), channel_id=1, source_target_pairs={{8,0},{12,4},{16,8},{20,12},{24,16},{28,20},{32,24},{36,28},{40,32... | collective-permute-start | bytes 6152 | tf_op jit(solution)/shard_map/ppermute | solution.py:502
  224.7 11.3 %collective-permute-start.19 = (f32[2,256]{1,0:T(2,128)}, f32[2,256]{1,0:T(2,128)S(1)}, u32[]{:S(2)}, u32[]{:S(2)}) collective-permute-start(f32[2,256]{1,0:T(2,128)} %get-tuple-element.49), channel_id=1, source_target_pairs={{12,0},{16,4},{20,8},{24,12},{28,16},{32,20},{36,24},{40,28},{44,3... | collective-permute-start | bytes 6152 | tf_op jit(solution)/shard_map/ppermute | solution.py:502
  226.0 10.0 %collective-permute-start.20 = (f32[2,256]{1,0:T(2,128)}, f32[2,256]{1,0:T(2,128)S(1)}, u32[]{:S(2)}, u32[]{:S(2)}) collective-permute-start(f32[2,256]{1,0:T(2,128)} %get-tuple-element.49), channel_id=1, source_target_pairs={{16,0},{20,4},{24,8},{28,12},{32,16},{36,20},{40,24},{44,28},{48,3... | collective-permute-start | bytes 6152 | tf_op jit(solution)/shard_map/ppermute | solution.py:502
  236.0 6.5 %collective-permute-start.21 = (f32[2,256]{1,0:T(2,128)S(1)}, f32[2,256]{1,0:T(2,128)S(1)}, u32[]{:S(2)}, u32[]{:S(2)}) collective-permute-start(f32[2,256]{1,0:T(2,128)S(1)} %pad_maximum_fusion.refs_0_), channel_id=1, source_target_pairs={{16,0},{20,4},{24,8},{28,12},{32,16},{36,20},{40,24},{44,28},{48,3... | collective-permute-start | bytes 6152 | tf_op jit(solution)/shard_map/ppermute | solution.py:502
  237.3 7.3 %collective-permute-start.22 = (f32[2,256]{1,0:T(2,128)S(1)}, f32[2,256]{1,0:T(2,128)S(1)}, u32[]{:S(2)}, u32[]{:S(2)}) collective-permute-start(f32[2,256]{1,0:T(2,128)S(1)} %pad_maximum_fusion.refs_0_), channel_id=1, source_target_pairs={{32,0},{36,4},{40,8},{44,12},{48,16},{52,20},{56,24},{60,28},{64,3... | collective-permute-start | bytes 6152 | tf_op jit(solution)/shard_map/ppermute | solution.py:502
  238.6 18.3 %collective-permute-start.23 = (f32[2,256]{1,0:T(2,128)S(1)}, f32[2,256]{1,0:T(2,128)S(1)}, u32[]{:S(2)}, u32[]{:S(2)}) collective-permute-start(f32[2,256]{1,0:T(2,128)S(1)} %pad_maximum_fusion.refs_0_), channel_id=1, source_target_pairs={{48,0},{52,4},{56,8},{60,12},{64,16},{68,20},{72,24},{76,28},{80,3... | collective-permute-start | bytes 6152 | tf_op jit(solution)/shard_map/ppermute | solution.py:502
  239.9 17.0 %collective-permute-start.24 = (f32[2,256]{1,0:T(2,128)S(1)}, f32[2,256]{1,0:T(2,128)S(1)}, u32[]{:S(2)}, u32[]{:S(2)}) collective-permute-start(f32[2,256]{1,0:T(2,128)S(1)} %pad_maximum_fusion.refs_0_), channel_id=1, source_target_pairs={{64,0},{68,4},{72,8},{76,12},{80,16},{84,20},{88,24},{92,28},{96,3... | collective-permute-start | bytes 6152 | tf_op jit(solution)/shard_map/ppermute | solution.py:502
  241.2 15.7 %collective-permute-start.25 = (f32[2,256]{1,0:T(2,128)S(1)}, f32[2,256]{1,0:T(2,128)S(1)}, u32[]{:S(2)}, u32[]{:S(2)}) collective-permute-start(f32[2,256]{1,0:T(2,128)S(1)} %pad_maximum_fusion.refs_0_), channel_id=1, source_target_pairs={{80,0},{84,4},{88,8},{92,12},{96,16},{100,20},{104,24},{108,28},{1... | collective-permute-start | bytes 6152 | tf_op jit(solution)/shard_map/ppermute | solution.py:502
  242.5 14.4 %collective-permute-start.26 = (f32[2,256]{1,0:T(2,128)S(1)}, f32[2,256]{1,0:T(2,128)S(1)}, u32[]{:S(2)}, u32[]{:S(2)}) collective-permute-start(f32[2,256]{1,0:T(2,128)S(1)} %pad_maximum_fusion.refs_0_), channel_id=1, source_target_pairs={{96,0},{100,4},{104,8},{108,12},{112,16},{116,20},{120,24},{124,28... | collective-permute-start | bytes 6152 | tf_op jit(solution)/shard_map/ppermute | solution.py:502
  244.6 14.4 %collective-permute-start.27 = (f32[2,256]{1,0:T(2,128)S(1)}, f32[2,256]{1,0:T(2,128)S(1)}, u32[]{:S(2)}, u32[]{:S(2)}) collective-permute-start(f32[2,256]{1,0:T(2,128)S(1)} %pad_maximum_fusion.refs_0_), channel_id=1, source_target_pairs={{112,0},{116,4},{120,8},{124,12},{113,1},{117,5},{121,9},{125,13},... | collective-permute-start | bytes 6152 | tf_op jit(solution)/shard_map/ppermute | solution.py:502

commit v3 on v2

--- a/solution.py
+++ b/solution.py
@@ -61,31 +61,37 @@
     tokens, channels = rec.shape
     heads = channels // 128
     first = where_ref[0] * heads
-    for h in range(heads):
-        cols = slice(h * 128, (h + 1) * 128)
-        values_bf = rec[:, cols]
-        x = values_bf.astype(F32)
-        ra = sigmoid(dot(values_bf, map_a[first + h]))
-        ig = sigmoid(dot(values_bf, map_i[first + h]))
-        rate = rates[pl.ds(first + h, 1), :]
-        log_decay = -rate * ra + extra[:, h : h + 1]
-        decay = jnp.exp(log_decay)
-        scale = jnp.sqrt(minus_expm1(2.0 * log_decay))
-        before = prev[:, cols]
-        state = decay * before + scale * ig * x
-        g = gate_in[:, cols].astype(F32)
-        bend = jnp.tanh(gelu_scale * (g + gelu_cubic * g * g * g))
-        act = 0.5 * g * (1.0 + bend)
-        slope = 0.5 * (1.0 + bend) + 0.5 * g * (1.0 - bend * bend) * gelu_scale * (
-            1.0 + 3.0 * gelu_cubic * g * g
-        )
-        out_rec[:, cols] = (state * act).astype(BF16)
-        out_act[:, cols] = act
-        out_b[:, cols] = state * slope
-        out_ca[:, cols] = (decay * before - decay * decay / scale * ig * x) * -rate * ra * (1.0 - ra)
-        out_ci[:, cols] = scale * x * ig * (1.0 - ig)
-        out_cs[:, cols] = scale * ig
-        out_decay[h] = decay
+
+    def block_of_tokens(i, _):
+        rows = pl.ds(pl.multiple_of(i * 128, 128), 128)
+        for h in range(heads):
+            cols = slice(h * 128, (h + 1) * 128)
+            values_bf = rec[rows, cols]
+            x = values_bf.astype(F32)
+            ra = sigmoid(dot(values_bf, map_a[first + h]))
+            ig = sigmoid(dot(values_bf, map_i[first + h]))
+            rate = rates[pl.ds(first + h, 1), :]
+            log_decay = -rate * ra + extra[rows, h : h + 1]
+            decay = jnp.exp(log_decay)
+            scale = jnp.sqrt(minus_expm1(2.0 * log_decay))
+            before = prev[rows, cols]
+            state = decay * before + scale * ig * x
+            g = gate_in[rows, cols].astype(F32)
+            bend = jnp.tanh(gelu_scale * (g + gelu_cubic * g * g * g))
+            act = 0.5 * g * (1.0 + bend)
+            slope = 0.5 * (1.0 + bend) + 0.5 * g * (1.0 - bend * bend) * gelu_scale * (
+                1.0 + 3.0 * gelu_cubic * g * g
+            )
+            out_rec[rows, cols] = (state * act).astype(BF16)
+            out_act[rows, cols] = act
+            out_b[rows, cols] = state * slope
+            out_ca[rows, cols] = (decay * before - decay * decay / scale * ig * x) * -rate * ra * (1.0 - ra)
+            out_ci[rows, cols] = scale * x * ig * (1.0 - ig)
+            out_cs[rows, cols] = scale * ig
+            out_decay[h, rows, :] = decay
+        return 0
+
+    lax.fori_loop(0, tokens // 128, block_of_tokens, 0)
     length = tokens // 8
     for h in range(heads):
         cols = slice(h * 128, (h + 1) * 128)
@@ -204,26 +210,35 @@
 
 
 def weights_kernel(
-    where_ref, w_gate, w_up, w_down, own, left, right, far_top, far_bottom,
-    out_gate_up, out_down, out_gate, out_up, *, row_part, cot_part,
+    where_ref, w_gate, w_up, w_down, whole_own, *refs, row_part, cot_part,
 ):
-    at = where_ref[0]
+    pieces = refs[:8]
+    out_gate_up, out_down, out_gate, out_up = refs[8:]
+    at, core = where_ref[0], where_ref[1]
     width, units = w_gate.shape
     half = width // 2
     first = ((0,), (0,))
+    mine = pl.multiple_of(core * half, half)
+    other = pl.multiple_of(half - core * half, half)
     for weights, out in ((w_gate, out_gate), (w_up, out_up)):
-        for step, piece in ((0, own), (3, left), (1, right)):
-            out[lax.rem(at + step, 4)] = dot(weights[...], piece[...], first).astype(BF16)
-        out[lax.rem(at + 2, 4)] = (
-            dot(weights[:half, :], far_top[...], first)
-            + dot(weights[half:, :], far_bottom[...], first)
+        out[at] = dot(weights[...], whole_own[...], first).astype(BF16)
+        for step, n in ((3, 0), (1, 1)):
+            out[lax.rem(at + step, 4)] = (
+                dot(weights[pl.ds(mine, half), :], pieces[n][...], first)
+                + dot(weights[pl.ds(other, half), :], pieces[4 + n][...], first)
+            ).astype(BF16)
+        quarter = half // 2
+        out[lax.rem(at + 2, 4)] = sum(
+            dot(weights[pl.ds(start + n * quarter, quarter), :], pieces[side + 2 + n][...], first)
+            for start, side in ((mine, 0), (other, 4))
+            for n in range(2)
         ).astype(BF16)
     rest = width - 4 * row_part
     out_gate_up[:rest, :units] = w_gate[4 * row_part :, :]
     out_gate_up[:rest, units:] = w_up[4 * row_part :, :]
     cot_rest = width - 4 * cot_part
     out_down[:cot_rest, :] = w_down[:, 4 * cot_part :].T
-    for n, step in enumerate(ring_steps):
+    for n, step in enumerate((2, 0, 3, 1)):
         group = lax.rem(at + step, 4)
         lines = pl.ds(pl.multiple_of(group * row_part, row_part), row_part)
         columns = pl.ds(pl.multiple_of(group * cot_part, 128), cot_part)
@@ -234,16 +249,11 @@
         out_down[to, :] = w_down[:, columns].T
 
 
-def folded_weights(position, w_gate, w_up, w_down, pieces, row_part, cot_part):
+def folded_weights(position, w_gate, w_up, w_down, own, pieces, row_part, cot_part):
     width, units = w_gate.shape
-    args = (position, w_gate, w_up, w_down, *pieces)
-    fold = made((4, units, pieces[0].shape[1]), BF16)
-    outs = (
-        made((width, 2 * units), BF16),
-        made((width, units), BF16),
-        fold,
-        fold,
-    )
+    args = (position, w_gate, w_up, w_down, own, *pieces)
+    fold = made((4, units, own.shape[1]), BF16)
+    outs = (made((width, 2 * units), BF16), made((width, units), BF16), fold, fold)
     return pl.pallas_call(
         functools.partial(weights_kernel, row_part=row_part, cot_part=cot_part),
         out_shape=outs,
@@ -252,20 +262,53 @@
         compiler_params=params(24),
         cost_estimate=cost(4 * 10**9, 7 * 2**20),
         name="folded",
-    )(position, *kept([w_gate, w_up, w_down]), *pieces)
-
-
-def expert_kernel(got_rows, got_cot, *refs, row_part):
-    pieces = refs[:8]
-    gate_up, down, fold_gate, fold_up, out_hidden, out_gate, out_up, out_mix = refs[8:]
+    )(position, *kept([w_gate, w_up, w_down, own]), *pieces)
+
+
+def ahead_kernel(gate_up, down, *refs, row_part, row_from, cot_from):
+    pieces, out = refs[:-1], refs[-1]
+    half = pieces[0].shape[0]
+    wide = gate_up.shape[1]
+    for n in range(2):
+        lines = slice(n * half, (n + 1) * half)
+        rows = jnp.concatenate([p[:, :row_part] for p in pieces[n::2]], axis=1)
+        cots = jnp.concatenate([p[:, row_part:] for p in pieces[n::2]], axis=1)
+        out[lines, :wide] = dot(rows, gate_up[row_from:, :])
+        out[lines, wide:] = dot(cots, down[cot_from:, :])
+
+
+def ahead(pieces, gate_up, down, row_part, cot_part):
+    width = gate_up.shape[0]
+    out = made((2 * pieces[0].shape[0], gate_up.shape[1] + down.shape[1]), F32)
+    args = (gate_up, down, *pieces)
+    return pl.pallas_call(
+        functools.partial(
+            ahead_kernel,
+            row_part=row_part,
+            row_from=width - 3 * row_part,
+            cot_from=width - 3 * cot_part,
+        ),
+        out_shape=out,
+        in_specs=[whole(a.shape) for a in args],
+        out_specs=whole(out.shape),
+        compiler_params=params(20),
+        cost_estimate=cost(2 * 10**9, 12 * 2**20),
+        name="ahead",
+    )(*kept([gate_up, down]), *pieces)
+
+
+def expert_kernel(
+    got_rows, got_cot, far_top, far_bottom, before, gate_up, down, fold_gate, fold_up,
+    out_hidden, out_gate, out_up, out_mix, *, row_part,
+):
     units = down.shape[1]
     upper = pl.program_id(0) < pl.num_programs(0) // 2
-    parts = [jnp.where(upper, pieces[2 * n][...], pieces[2 * n + 1][...]) for n in range(4)]
-    rows = jnp.concatenate([got_rows[...], *(p[:, :row_part] for p in parts)], axis=1)
-    cots = jnp.concatenate([got_cot[...], *(p[:, row_part:] for p in parts)], axis=1)
-    both = dot(rows, gate_up[...])
+    far = jnp.where(upper, far_top[...], far_bottom[...])
+    rows = jnp.concatenate([got_rows[...], far[:, :row_part]], axis=1)
+    cots = jnp.concatenate([got_cot[...], far[:, row_part:]], axis=1)
+    both = dot(rows, gate_up[...]) + before[:, : 2 * units]
     gate_pre, up_pre = both[:, :units], both[:, units:]
-    hidden_cot = dot(cots, down[...])
+    hidden_cot = dot(cots, down[...]) + before[:, 2 * units :]
     sigma = sigmoid(gate_pre)
     swish = gate_pre * sigma
     out_hidden[...] = (swish * up_pre).astype(BF16)
@@ -277,7 +320,13 @@
         out_mix[c] = (dot(gate_cot, fold_gate[c]) + dot(up_cot, fold_up[c])).astype(BF16)
 
 
-def expert(got, pieces, gate_up, down, fold_gate, fold_up, row_part, cot_part, steps=4):
+def first_rows(array, count):
+    return pl.BlockSpec(
+        (count, array.shape[1]), lambda i: (0, 0), pipeline_mode=pl.Buffered(1)
+    )
+
+
+def expert(got, far, before, gate_up, down, fold_gate, fold_up, row_part, cot_part, steps=4):
     rows = got.shape[0]
     width, hidden = down.shape
     block = rows // steps
@@ -286,8 +335,6 @@
     row_rest, cot_rest = width - 4 * row_part, width - 4 * cot_part
     narrow = made((rows, hidden), BF16)
     mine = pl.BlockSpec((block, hidden), lambda i: (i, 0))
-    top = pl.BlockSpec((block, row_part + cot_part), lambda i: (jnp.minimum(i, half - 1), 0))
-    bottom = pl.BlockSpec((block, row_part + cot_part), lambda i: (jnp.maximum(i - half, 0), 0))
     return pl.pallas_call(
         functools.partial(expert_kernel, row_part=row_part),
         out_shape=(narrow, narrow, narrow, made((4, rows, part), BF16)),
@@ -295,14 +342,19 @@
         in_specs=[
             pl.BlockSpec((block, row_rest), lambda i: (i, 0)),
             pl.BlockSpec((block, cot_rest), lambda i: (i, row_rest // cot_rest)),
-            *([top, bottom] * 4),
-            *(whole(a.shape) for a in (gate_up, down, fold_gate, fold_up)),
+            pl.BlockSpec((block, row_part + cot_part), lambda i: (jnp.minimum(i, half - 1), 0)),
+            pl.BlockSpec((block, row_part + cot_part), lambda i: (jnp.maximum(i - half, 0), 0)),
+            pl.BlockSpec((block, before.shape[1]), lambda i: (i, 0)),
+            first_rows(gate_up, row_rest + row_part),
+            first_rows(down, cot_rest + cot_part),
+            whole(fold_gate.shape),
+            whole(fold_up.shape),
         ],
         out_specs=[mine, mine, mine, pl.BlockSpec((4, block, part), lambda i: (0, i, 0))],
         compiler_params=params(26),
-        cost_estimate=cost(7 * 10**9, 18 * 2**20),
+        cost_estimate=cost(5 * 10**9, 16 * 2**20),
         name="expert",
-    )(*kept([got, got]), *pieces, *kept([gate_up, down, fold_gate, fold_up]))
+    )(*kept([got, got]), *far, *kept([before, gate_up, down, fold_gate, fold_up]))
 
 
 def grads_kernel(where_ref, got_rows, got_cot, *refs, row_part, cot_part):
@@ -422,16 +474,17 @@
             out_local[rows, cols] = part[h, rows, :] + seg[h, rows, :] * carry
             one = slice(k, k + 1)
             carry = lead[one, :] * (value[one, :] + inner[one, :] * carry)
-        out_pair[:, cols] = jnp.concatenate([carry, block[0:1, cols]], axis=0)
-
-
-def scanned(back, sel, base, act, b, decay, seg, block):
+        pair = jnp.concatenate([carry, block[0:1, cols]], axis=0)
+        out_pair[:, :, cols] = jnp.broadcast_to(pair[None], (out_pair.shape[0], *pair.shape))
+
+
+def scanned(back, sel, base, act, b, decay, seg, block, sources):
     tokens, channels = base.shape
     args = (back, sel, base, act, b, decay, seg, block)
     outs = (
         made((tokens, channels), BF16),
         made((tokens, channels), F32),
-        made((2, channels), F32),
+        made((sources, 2, channels), F32),
     )
     return pl.pallas_call(
         scan_kernel,
@@ -445,15 +498,14 @@
     )(back, *kept(args[1:]))
 
 
-def final_kernel(where_ref, *refs):
-    carry = refs[:-8]
-    local, exp, ca, ci, cs, map_a, map_i, out = refs[-8:]
+def final_kernel(where_ref, pairs, local, exp, ca, ci, cs, map_a, map_i, out):
     channels = local.shape[1]
     heads = channels // 128
     first = where_ref[0] * heads
     total = jnp.zeros((1, channels), F32)
-    for pair in reversed(carry):
-        total = pair[0:1, :] + pair[1:2, :] * total
+    me = where_ref[2]
+    for s in range(pairs.shape[0] - 1, 0, -1):
+        total = jnp.where(me < s, pairs[s, 0:1, :] + pairs[s, 1:2, :] * total, total)
     for h in range(heads):
         cols = slice(h * 128, (h + 1) * 128)
         cot = local[:, cols] + exp[:, cols] * total[:, cols]
@@ -467,8 +519,8 @@
         out[:, cols] = result.astype(BF16)
 
 
-def final(position, carry, local, exp, ca, ci, cs, map_a, map_i):
-    args = (position, *carry, local, exp, ca, ci, cs, map_a, map_i)
+def final(position, pairs, local, exp, ca, ci, cs, map_a, map_i):
+    args = (position, pairs, local, exp, ca, ci, cs, map_a, map_i)
     return pl.pallas_call(
         final_kernel,
         out_shape=made(local.shape, BF16),
@@ -477,7 +529,7 @@
         compiler_params=params(8),
         cost_estimate=cost(10**8, 4 * 2**20),
         name="final",
-    )(position, *carry, *kept(args[1 + len(carry) :]))
+    )(position, pairs, *kept(args[2:]))
 
 
 def shifted(piece, by):
@@ -491,25 +543,15 @@
     return top, bottom, left_top, left_bottom, right_top, right_bottom, far_top, far_bottom
 
 
-def whole_ring_gather(own):
+def shared_ring_gather(own, core):
     half = own.shape[0] // 2
-    left, right = shifted(own, 1), shifted(own, -1)
-    far_top, far_bottom = shifted(left[:half], 1), shifted(right[half:], -1)
-    return own, left, right, far_top, far_bottom
-
-
-def later(pair, by, length):
-    return lax.ppermute(pair, ("sq", "core"), [(i, i - by) for i in range(by, length)])
-
-
-def joined(near, far):
-    return jnp.stack([near[0] + near[1] * far[0], near[1] * far[1]])
-
-
-def carried(pair, length):
-    one, two, three, four = (later(pair, by, length) for by in (1, 2, 3, 4))
-    near = joined(joined(one, two), joined(three, four))
-    return [near, *(later(near, by, length) for by in range(4, length, 4))]
+    mine = lax.dynamic_slice_in_dim(own, core * half, half, 0)
+    left, right = shifted(mine, 1), shifted(mine, -1)
+    quarter = half // 2
+    far_top, far_bottom = shifted(left[:quarter], 1), shifted(right[quarter:], -1)
+    pieces = (left, right, far_top, far_bottom)
+    others = tuple(lax.ppermute(p, "core", [(0, 1), (1, 0)]) for p in pieces)
+    return pieces + others
 
 
 def per_device(
@@ -520,7 +562,8 @@
     tp = lax.axis_index("tp")
     core = lax.axis_index("core")
     sp_axes = ("sq", "core")
-    position = jnp.stack([tp, core]).astype(jnp.int32)
+    sp = lax.axis_index("sq") * 2 + core
+    position = jnp.stack([tp, core, sp]).astype(jnp.int32)
     w_gate, w_up, w_down = w_gate[0], w_up[0], w_down[0]
     tokens, width = layer_input.shape
     capacity = 5 * tokens * expert_ids.shape[1] // (4 * sources)
@@ -540,9 +583,9 @@
         capacity, sources,
     )
     spread = exchanged(spread)
-    projections = whole_ring_gather(out_proj)
+    projections = shared_ring_gather(out_proj, core)
     gate_up, down, fold_gate, fold_up = folded_weights(
-        position, w_gate, w_up, w_down, projections, row_part, cot_part
+        position, w_gate, w_up, w_down, out_proj, projections, row_part, cot_part
     )
     rates = (decay_factor * jax.nn.softplus(-decay_param)).reshape(-1, gate_a_w.shape[1])
     rec_output, act, b, ca, ci, cs, decay, seg, exp, block, sel = early(
@@ -564,8 +607,9 @@
     local_proj = lax.dot_general(
         out_cot, rec_output, (((0,), (0,)), ((), ())), preferred_element_type=F32
     )
+    before = ahead(pieces[:6], gate_up, down, row_part, cot_part)
     hidden, gate_cot, up_cot, mix = expert(
-        got, pieces, gate_up, down, fold_gate, fold_up, row_part, cot_part
+        got, pieces[6:], before, gate_up, down, fold_gate, fold_up, row_part, cot_part
     )
     back = lax.all_to_all(
         mix.reshape(4 * sources, capacity, -1), ("tp", *sp_axes), 0, 0, tiled=True
@@ -583,9 +627,11 @@
         chip.reshape(4 * chip.shape[1], lines, -1), ("tp", "sq"), 0, 0, tiled=True
     )
     grad_out_proj = arrived.astype(F32).sum(axis=0)
-    gate_input_grad, local, pair = scanned(back, sel, base, act, b, decay, seg, block)
-    carry = carried(pair, sources)
-    rec_input_grad = final(position, carry, local, exp, ca, ci, cs, gate_a_w, gate_i_w)
+    gate_input_grad, local, pair = scanned(
+        back, sel, base, act, b, decay, seg, block, sources
+    )
+    pairs = lax.all_to_all(pair, sp_axes, 0, 0, tiled=True)
+    rec_input_grad = final(position, pairs, local, exp, ca, ci, cs, gate_a_w, gate_i_w)
     return (grad_gate, grad_up, grad_down, grad_out_proj, rec_input_grad, gate_input_grad)
 
 

time: 269 us -> 247 us (0.918)
  waiting for transfers between devices: 106 us -> 78.4 us
  local copies, waits for them, and re-layouts: 11.9 us -> 21.1 us
  starting transfers between devices: 68.6 us -> 62.2 us
  Pallas kernels: 66.3 us -> 70.1 us
    ppermute x16, waiting for transfers between devices: 65 us -> 30.4 us  [shifted(): return lax.ppermute(piece, 'tp', [(i, (i + by) % 4) for i in range(4)])]
    all_to_all x1, waiting for transfers between devices: 0.01 us -> 13.4 us  [per_device(): lax.all_to_all(chip.reshape(4 * chip.shape[1], lines, -1), ('tp', 'sq'),...]
    ppermute x11 -> x4, starting transfers between devices: 16 us -> 4.07 us  [shared_ring_gather(): others = tuple((lax.ppermute(p, 'core', [(0, 1), (1, 0)]) for p in pieces))]
    ppermute x11 -> x4, waiting for transfers between devices: 11.5 us -> 0.01 us  [shared_ring_gather(): others = tuple((lax.ppermute(p, 'core', [(0, 1), (1, 0)]) for p in pieces))]
    pallas_call x0 -> x1, Pallas kernels: none -> 6.35 us  [ahead(): pl.pallas_call(functools.partial(ahead_kernel, row_part=row_part, row_fro...]
    unnamed x38 -> x56, local copies, waits for them, and re-layouts: 7.03 us -> 13.2 us
    ppermute x16, starting transfers between devices: 17.9 us -> 22.7 us  [shifted(): return lax.ppermute(piece, 'tp', [(i, (i + by) % 4) for i in range(4)])]
    all_to_all x0 -> x1, starting transfers between devices: none -> 4.69 us  [per_device(): pairs = lax.all_to_all(pair, sp_axes, 0, 0, tiled=True)]
  transfers between devices with their start and end apart: 32 -> 26, of which waited for: 13 -> 10; matrix products, arithmetic and copies ran while one was open for 6% -> 8% of each run, Pallas kernels for 23% -> 27%
where the time goes in v3:
time: 247 us; the launch traced here: 244 us
  waiting for transfers between devices  78.4 us (32%)
  Pallas kernels  70.1 us (28%)
  starting transfers between devices  62.2 us (25%)
  local copies, waits for them, and re-layouts  21.1 us (9%)
  other arithmetic  7.68 us (3%)
  matrix products  3.76 us (2%)
    ppermute x16, waiting for transfers between devices, shifted(): return lax.ppermute(piece, 'tp', [(i, (i + by) % 4) for i in range(4)])  30.4 us
    ppermute x16, starting transfers between devices, shifted(): return lax.ppermute(piece, 'tp', [(i, (i + by) % 4) for i in range(4)])  22.7 us
    all_to_all x1, waiting for transfers between devices, per_device(): lax.all_to_all(mix.reshape(4 * sources, capacity, -1), ('tp', *sp_axes),...  20.3 us
    all_to_all x2, starting transfers between devices, exchanged(): lax.all_to_all(rows.reshape(sources, capacity, -1), sp_axes, 0, 0, tiled=...  15.5 us
    all_to_all x1, waiting for transfers between devices, per_device(): lax.all_to_all(chip.reshape(4 * chip.shape[1], lines, -1), ('tp', 'sq'),...  13.4 us
    unnamed x56, local copies, waits for them, and re-layouts  13.2 us
    pallas_call x2, Pallas kernels, build(): pl.pallas_call(functools.partial(build_kernel, capacity=capacity, group=g...  11.5 us
    all_to_all x2, waiting for transfers between devices, exchanged(): lax.all_to_all(rows.reshape(sources, capacity, -1), sp_axes, 0, 0, tiled=...  11.3 us
  transfers between devices with their start and end apart: 26, of which 10 were waited for; matrix products, arithmetic and copies ran while one was open for 8% of the time, Pallas kernels for 27%

profile of v3, /device:TPU:1, one launch (start us, length us, event | category | flops | bytes accessed | tf_op | source)
XLA Modules:
  0.0 244.2 jit_solution(12238987892616206372)
XLA Ops:
  0.7 4.7 %shard_map.191 = bf16[1280,640]{1,0:T(8,128)(2,1)} custom-call(s32[3]{0:T(128)S(1)} %pad_add_fusion.where_ref, s32[2,512]{1,0:T(2,128)} %bitcast.46, f32[2,512]{1,0:T(2,128)} %bitcast.48, bf16[512,2048]{1,0:T(8,128)(2,1)} %refs_0_.3, bf16[512,2048]{1,0:T(8,128)(2,1)} %refs_1_.3), custom_call_target="tpu_custom_call" | custom-call | flops 896000000 | bytes 3200000 | tf_op jit(solution)/shard_map/pallas_call | solution.py:191
  5.4 9.7 %all-to-all-start.1 = ((bf16[32,40,640]{2,1,0:T(8,128)(2,1)}), bf16[32,40,640]{2,1,0:T(8,128)(2,1)S(1)}, u32[]{:S(2)}, u32[]{:S(2)}) async-start(bf16[32,40,640]{2,1,0:T(8,128)(2,1)} %bitcast.42), calls=%async_computation.1 | async-start | bytes 3276800 | tf_op jit(solution)/shard_map/all_to_all | solution.py:576
  15.2 0.9 copy.22.ids
  16.0 0.9 copy.21
  16.9 0.6 fusion.2.rates
  17.5 6.9 %early.1 = (bf16[512,256]{1,0:T(8,128)(2,1)}, f32[512,256]{1,0:T(8,128)}, f32[512,256]{1,0:T(8,128)}, f32[512,256]{1,0:T(8,128)}, f32[512,256]{1,0:T(8,128)}, /*...) custom-call(s32[3]{0:T(128)S(1)} %pad_add_fusion.where_ref, ...), custom_call_target="tpu_custom_call" | custom-call | flops 3000000000 | bytes 8388608 | tf_op jit(solution)/shard_map/early/pallas_call | solution.py:137
  24.5 6.8 %shard_map.190 = bf16[1280,1792]{1,0:T(8,128)(2,1)} custom-call(s32[3]{0:T(128)S(1)} %pad_add_fusion.where_ref, s32[2,512]{1,0:T(2,128)} %bitcast.47, f32[2,512]{1,0:T(2,128)} %bitcast.49, bf16[512,2048]{1,0:T(8,128)(2,1)} %refs_0_.3, bf16[512,2048]{1,0:T(8,128)(2,1)} %refs_1_.3, bf16[512,256]{1,0:T(8,128)(2,1)} %get-tuple-element.31.refs_2_), custom_call_target="tpu_custom_call" | custom-call | flops 2508800000 | bytes 8960000 | tf_op jit(solution)/shard_map/pallas_call | solution.py:191
  31.3 7.5 %all-to-all-done.1 = bf16[32,40,640]{2,1,0:T(8,128)(2,1)S(1)} async-done(((bf16[32,40,640]{2,1,0:T(8,128)(2,1)}), bf16[32,40,640]{2,1,0:T(8,128)(2,1)S(1)}, u32[]{:S(2)}, u32[]{:S(2)}) %all-to-all-start.1) | async-done | bytes 1638432 | tf_op jit(solution)/shard_map/all_to_all | solution.py:576
  38.8 1.2 copy-done.20
  39.9 5.8 %all-to-all-start = ((bf16[32,40,1792]{2,1,0:T(8,128)(2,1)}), bf16[32,40,1792]{2,1,0:T(8,128)(2,1)}, u32[]{:S(2)}, u32[]{:S(2)}) async-start(bf16[32,40,1792]{2,1,0:T(8,128)(2,1)} %bitcast.43), calls=%async_computation | async-start | bytes 9175040 | tf_op jit(solution)/shard_map/all_to_all | solution.py:576
  45.8 1.3 collective-permute-start.6
  47.1 1.5 collective-permute-start.7
  48.6 1.5 fusion.4
  50.2 2.7 %collective-permute-start.3 = (bf16[640,640]{1,0:T(8,128)(2,1)S(1)}, bf16[640,640]{1,0:T(8,128)(2,1)S(1)}, u32[]{:S(2)}, u32[]{:S(2)}) collective-permute-start(bf16[640,640]{1,0:T(8,128)(2,1)S(1)} %bitcast.33), channel_id=1, source_target_pairs={{0,3},{1,0},{2,1},{3,2},{4,7},{5,4},{6,5},{7,6},{8,11},{9,8},{10,9... | collective-permute-start | bytes 2457608 | tf_op jit(solution)/shard_map/ppermute | solution.py:536
  52.8 7.4 %collective-permute-done.6.refs_0_ = bf16[1024,256]{1,0:T(8,128)(2,1)S(1)} collective-permute-done((bf16[1024,256]{1,0:T(8,128)(2,1)S(1)}, bf16[1024,256]{1,0:T(8,128)(2,1)S(1)}, u32[]{:S(2)}, u32[]{:S(2)}) %collective-permute-start.6) | collective-permute-done | bytes 524320 | tf_op jit(solution)/shard_map/ppermute | solution.py:536
  60.4 1.0 slice.43
  61.3 2.7 %collective-permute-start.9 = (bf16[512,256]{1,0:T(8,128)(2,1)S(1)}, bf16[512,256]{1,0:T(8,128)(2,1)S(1)}, u32[]{:S(2)}, u32[]{:S(2)}) collective-permute-start(bf16[512,256]{1,0:T(8,128)(2,1)S(1)} %slice.43), channel_id=1, source_target_pairs={{0,3},{1,0},{2,1},{3,2},{4,7},{5,4},{6,5},{7,6},{8,11},{9,8},{10,9... | collective-permute-start | bytes 786440 | tf_op jit(solution)/shard_map/ppermute | solution.py:536
  64.1 2.6 %collective-permute-start.10 = (bf16[1024,256]{1,0:T(8,128)(2,1)S(1)}, bf16[1024,256]{1,0:T(8,128)(2,1)S(1)}, u32[]{:S(2)}, u32[]{:S(2)}) collective-permute-start(bf16[1024,256]{1,0:T(8,128)(2,1)S(1)} %collective-permute-done.6.refs_0_), channel_id=1, source_target_pairs={{0,4},{4,0},{1,5},{5,1},{2,6},{6,2},{3,7},{7,3},{8,12},{12,8},{9,1... | collective-permute-start | bytes 1572872 | tf_op jit(solution)/shard_map/ppermute | solution.py:553
  66.7 0.8 copy-done.6
  67.5 16.0 %collective-permute-done.8.refs_2_ = bf16[512,256]{1,0:T(8,128)(2,1)S(1)} collective-permute-done((bf16[512,256]{1,0:T(8,128)(2,1)S(1)}, bf16[512,256]{1,0:T(8,128)(2,1)S(1)}, u32[]{:S(2)}, u32[]{:S(2)}) %collective-permute-start.8) | collective-permute-done | bytes 262176 | tf_op jit(solution)/shard_map/ppermute | solution.py:536
  83.4 1.2 collective-permute-start.12
  84.6 0.7 copy-done.10
  85.3 0.7 copy-done.12
  86.0 0.7 copy-done.14
  86.7 0.5 collective-permute-start.1
  87.2 0.7 copy-done.16
  88.0 0.3 collective-permute-start.11
  88.2 0.8 copy-done.8
  89.0 2.7 %collective-permute-start.2 = (bf16[640,640]{1,0:T(8,128)(2,1)S(1)}, bf16[640,640]{1,0:T(8,128)(2,1)}, u32[]{:S(2)}, u32[]{:S(2)}) collective-permute-start(bf16[640,640]{1,0:T(8,128)(2,1)S(1)} %bitcast.38), channel_id=1, source_target_pairs={{0,3},{1,0},{2,1},{3,2},{4,7},{5,4},{6,5},{7,6},{8,11},{9,8},{10,9... | collective-permute-start | bytes 2457608 | tf_op jit(solution)/shard_map/ppermute | solution.py:536
  91.7 2.7 %collective-permute-start.5 = (bf16[640,640]{1,0:T(8,128)(2,1)S(1)}, bf16[640,640]{1,0:T(8,128)(2,1)}, u32[]{:S(2)}, u32[]{:S(2)}) collective-permute-start(bf16[640,640]{1,0:T(8,128)(2,1)S(1)} %collective-permute-done.3.refs_5_), channel_id=1, source_target_pairs={{0,3},{1,0},{2,1},{3,2},{4,7},{5,4},{6,5},{7,6},{8,11},{9,8},{10,9... | collective-permute-start | bytes 2457608 | tf_op jit(solution)/shard_map/ppermute | solution.py:536
  94.4 2.3 convolution_bitcast_fusion.local
  96.7 3.8 %all-to-all-done = bf16[32,40,1792]{2,1,0:T(8,128)(2,1)} async-done(((bf16[32,40,1792]{2,1,0:T(8,128)(2,1)}), bf16[32,40,1792]{2,1,0:T(8,128)(2,1)}, u32[]{:S(2)}, u32[]{:S(2)}) %all-to-all-start) | async-done | bytes 4587552 | tf_op jit(solution)/shard_map/all_to_all | solution.py:576
  100.5 2.0 fusion.3
  102.4 1.2 collective-permute-start.14
  103.7 3.7 %collective-permute-done.1.refs_3_ = bf16[640,640]{1,0:T(8,128)(2,1)} collective-permute-done((bf16[640,640]{1,0:T(8,128)(2,1)S(1)}, bf16[640,640]{1,0:T(8,128)(2,1)}, u32[]{:S(2)}, u32[]{:S(2)}) %collective-permute-start.1) | collective-permute-done | bytes 819232 | tf_op jit(solution)/shard_map/ppermute | solution.py:536
  107.3 1.3 collective-permute-start.17
  108.6 1.0 copy-done.7
  109.6 1.0 copy-done.9
  110.7 0.9 copy-done.11
  111.6 0.9 copy-done.13
  112.6 0.9 copy-done.15
  113.5 0.9 copy-done.17
  114.5 7.1 %folded.1 = (bf16[2048,512]{1,0:T(8,128)(2,1)}, bf16[2048,256]{1,0:T(8,128)(2,1)}, bf16[4,256,256]{2,1,0:T(8,128)(2,1)}, bf16[4,256,256]{2,1,0:T(8,128)(2,1)}) custom-call(s32[3]{0:T(128)S(1)} %pad_add_fusion.where_ref, bf16[2048,256]{1,0:T(8,128)(2,1)} %bitcast.51, bf16[2048,256]{1,0:T(8,128)(2,1)} %bitcast.53, bf16[256,2048]{1,0:T(8,128)(2,1)} %bitcast.50, ...), custom_call_target="tpu_custom_call" | custom-call | flops 4000000000 | bytes 7340032 | tf_op jit(solution)/shard_map/folded/pallas_call | solution.py:257
  121.6 6.4 %ahead.1.before = f32[1280,768]{1,0:T(8,128)} custom-call(bf16[2048,512]{1,0:T(8,128)(2,1)} %get-tuple-element.32.gate_up, bf16[2048,256]{1,0:T(8,128)(2,1)} %get-tuple-element.33.down, bf16[640,640]{1,0:T(8,128)(2,1)S(1)} %bitcast.39, bf16[640,640]{1,0:T(8,128)(2,1)S(1)} %bitcast.35, bf16[640,640]{1,0:T(8,128)(2,1)S(1)} %collective-permute-done.refs_2_, ...), custom_call_target="tpu_custom_call" | custom-call | flops 2000000000 | bytes 12582912 | tf_op jit(solution)/shard_map/ahead/pallas_call | solution.py:284
  128.2 2.5 %collective-permute-start.16 = (bf16[640,256]{1,0:T(8,128)(2,1)}, bf16[640,256]{1,0:T(8,128)(2,1)}, u32[]{:S(2)}, u32[]{:S(2)}) collective-permute-start(bf16[640,256]{1,0:T(8,128)(2,1)} %get-tuple-element.57.refs_0_), channel_id=1, source_target_pairs={{0,3},{1,0},{2,1},{3,2},{4,7},{5,4},{6,5},{7,6},{8,11},{9,8},{10,9... | collective-permute-start | bytes 983048 | tf_op jit(solution)/shard_map/ppermute | solution.py:536
  130.6 1.3 collective-permute-done.14.refs_2_
  131.9 2.1 collective-permute-done.17.refs_5_
  134.0 3.4 %collective-permute-start.19 = (bf16[640,256]{1,0:T(8,128)(2,1)}, bf16[640,256]{1,0:T(8,128)(2,1)}, u32[]{:S(2)}, u32[]{:S(2)}) collective-permute-start(bf16[640,256]{1,0:T(8,128)(2,1)} %collective-permute-done.17.refs_5_), channel_id=1, source_target_pairs={{0,3},{1,0},{2,1},{3,2},{4,7},{5,4},{6,5},{7,6},{8,11},{9,8},{10,9... | collective-permute-start | bytes 983048 | tf_op jit(solution)/shard_map/ppermute | solution.py:536
  137.4 10.2 %expert.1 = (bf16[1280,256]{1,0:T(8,128)(2,1)}, bf16[1280,256]{1,0:T(8,128)(2,1)}, bf16[1280,256]{1,0:T(8,128)(2,1)}, bf16[4,1280,256]{2,1,0:T(8,128)(2,1)}) custom-call(bf16[1280,1792]{1,0:T(8,128)(2,1)} %bitcast.8.got_rows.got_cot, bf16[1280,1792]{1,0:T(8,128)(2,1)} %bitcast.8.got_rows.got_cot, bf16[640,640]{1,0:T(8,128)(2,1)} %collective-permute-done.4.far_top.refs_6_, ...), custom_call_target="tpu_custom_call" | custom-call | flops 5000000000 | bytes 16777216 | tf_op jit(solution)/shard_map/expert/pallas_call | solution.py:338
  147.6 8.1 %all-to-all-start.3 = ((bf16[128,40,256]{2,1,0:T(8,128)(2,1)}), bf16[128,40,256]{2,1,0:T(8,128)(2,1)S(1)}, u32[]{:S(2)}, u32[]{:S(2)}) async-start(bf16[128,40,256]{2,1,0:T(8,128)(2,1)} %bitcast.44), calls=%async_computation.3 | async-start | bytes 5242880 | tf_op jit(solution)/shard_map/all_to_all | solution.py:614
  155.8 9.7 %proj.1 = bf16[2,4,16,64,256]{4,3,2,1,0:T(8,128)(2,1)} custom-call(s32[3]{0:T(128)S(1)} %pad_add_fusion.where_ref, bf16[1280,256]{1,0:T(8,128)(2,1)} %get-tuple-element.37.refs_9_.gate_cot, bf16[1280,256]{1,0:T(8,128)(2,1)} %get-tuple-element.38.refs_10_.up_cot, bf16[2048,256]{1,0:T(8,128)(2,1)} %bitcast.52, bf16[2048,256]{1,0:T(8,128)(2,1)} %bitcast.54, ...), custom_call_target="tpu_custom_call" | custom-call | flops 4000000000 | bytes 14680064 | tf_op jit(solution)/shard_map/proj/pallas_call | solution.py:439
  165.5 3.3 %slice_bitcast_fusion = bf16[4,16,64,256]{3,2,1,0:T(8,128)(2,1)} fusion(bf16[2,4,16,64,256]{4,3,2,1,0:T(8,128)(2,1)} %proj.1), kind=kLoop, calls=%fused_computation.4 | loop fusion | bytes 4194304 | tf_op jit(solution)/shard_map/squeeze | solution.py:624
  168.8 1.1 collective-permute-start.20
  169.8 1.5 fusion.5.base
  171.3 20.3 %all-to-all-done.3 = bf16[128,40,256]{2,1,0:T(8,128)(2,1)S(1)} async-done(((bf16[128,40,256]{2,1,0:T(8,128)(2,1)}), bf16[128,40,256]{2,1,0:T(8,128)(2,1)S(1)}, u32[]{:S(2)}, u32[]{:S(2)}) %all-to-all-start.3) | async-done | bytes 2621472 | tf_op jit(solution)/shard_map/all_to_all | solution.py:614
  191.7 4.5 %scanned.1 = (bf16[512,256]{1,0:T(8,128)(2,1)}, f32[512,256]{1,0:T(8,128)}, f32[32,2,256]{2,1,0:T(2,128)}) custom-call(bf16[4,1280,256]{2,1,0:T(8,128)(2,1)S(1)} %bitcast.32, bf16[512,1280]{1,0:T(8,128)(2,1)} %get-tuple-element.43.sel, f32[512,256]{1,0:T(8,128)} %fusion.5.base, f32[512,256]{1,0:T(8,128)} %get-tuple-element.44.act, ...), custom_call_target="tpu_custom_call" | custom-call | flops 400000000 | bytes 8388608 | tf_op jit(solution)/shard_map/scanned/pallas_call | solution.py:489
  196.2 4.7 %all-to-all-start.4 = ((f32[32,2,256]{2,1,0:T(2,128)}), f32[32,2,256]{2,1,0:T(2,128)S(1)}, u32[]{:S(2)}, u32[]{:S(2)}) async-start(f32[32,2,256]{2,1,0:T(2,128)} %get-tuple-element.49), calls=%async_computation.4 | async-start | bytes 131072 | tf_op jit(solution)/shard_map/all_to_all | solution.py:633
  200.9 4.5 %fusion = bf16[4,16,64,256]{3,2,1,0:T(8,128)(2,1)} fusion(bf16[4,16,64,256]{3,2,1,0:T(8,128)(2,1)} %collective-permute-done.20, bf16[2,4,16,64,256]{4,3,2,1,0:T(8,128)(2,1)} %proj.1), kind=kLoop, calls=%fused_computation.1 | loop fusion | flops 4194304 | bytes 6291456 | tf_op jit(solution)/shard_map/convert_element_type | solution.py:625
  205.3 3.0 %all-to-all-done.4.pairs = f32[32,2,256]{2,1,0:T(2,128)S(1)} async-done(((f32[32,2,256]{2,1,0:T(2,128)}), f32[32,2,256]{2,1,0:T(2,128)S(1)}, u32[]{:S(2)}, u32[]{:S(2)}) %all-to-all-start.4) | async-done | bytes 65568 | tf_op jit(solution)/shard_map/all_to_all | solution.py:633
  208.3 6.0 %all-to-all-start.2 = ((bf16[64,64,256]{2,1,0:T(8,128)(2,1)}), bf16[64,64,256]{2,1,0:T(8,128)(2,1)}, u32[]{:S(2)}, u32[]{:S(2)}) async-start(bf16[64,64,256]{2,1,0:T(8,128)(2,1)} %bitcast.41), calls=%async_computation.2 | async-start | bytes 4194304 | tf_op jit(solution)/shard_map/all_to_all | solution.py:626
  214.4 11.0 %grads.1 = (f32[1,2048,256]{2,1,0:T(8,128)}, f32[1,2048,256]{2,1,0:T(8,128)}, f32[1,256,2048]{2,1,0:T(8,128)}) custom-call(s32[3]{0:T(128)S(1)} %pad_add_fusion.where_ref, bf16[1280,1792]{1,0:T(8,128)(2,1)} %bitcast.8.got_rows.got_cot, bf16[1280,1792]{1,0:T(8,128)(2,1)} %bitcast.8.got_rows.got_cot, bf16[640,640]{1,0:T(8,128)(2,1)S(1)} %bitcast.40, ...), custom_call_target="tpu_custom_call" | custom-call | flops 4000000000 | bytes 17825792 | tf_op jit(solution)/shard_map/grads/pallas_call | solution.py:393
  225.4 2.9 %final.1 = bf16[512,256]{1,0:T(8,128)(2,1)} custom-call(s32[3]{0:T(128)S(1)} %pad_add_fusion.where_ref, f32[32,2,256]{2,1,0:T(2,128)S(1)} %all-to-all-done.4.pairs, f32[512,256]{1,0:T(8,128)} %get-tuple-element.50.local, f32[512,256]{1,0:T(8,128)} %get-tuple-element.51.exp, f32[512,256]{1,0:T(8,128)} %get-tuple-element.52.ca, ...), custom_call_target="tpu_custom_call" | custom-call | flops 100000000 | bytes 4194304 | tf_op jit(solution)/shard_map/final/pallas_call | solution.py:524
  228.3 13.4 %all-to-all-done.2 = bf16[64,64,256]{2,1,0:T(8,128)(2,1)} async-done(((bf16[64,64,256]{2,1,0:T(8,128)(2,1)}), bf16[64,64,256]{2,1,0:T(8,128)(2,1)}, u32[]{:S(2)}, u32[]{:S(2)}) %all-to-all-start.2) | async-done | bytes 2097184 | tf_op jit(solution)/shard_map/all_to_all | solution.py:626
  241.6 2.5 %convert_reduce_fusion = f32[64,256]{1,0:T(8,128)} fusion(bf16[64,64,256]{2,1,0:T(8,128)(2,1)} %all-to-all-done.2), kind=kLoop, calls=%fused_computation.2 | loop fusion | flops 2080768 | bytes 2162688 | tf_op jit(solution)/shard_map/reduce_sum | solution.py:629
  (66 shorter events, 0.6 us)
Async XLA Ops:
  5.4 9.8 %copy-start.24 = (s32[512,2]{0,1:T(2,128)S(1)}, s32[512,2]{0,1:T(2,128)}, u32[]{:S(2)}) copy-start(s32[512,2]{0,1:T(2,128)} %param.17) | copy-start | bytes 12292
  5.4 10.6 %copy-start.25 = (f32[2,512]{1,0:T(2,128)S(1)}, f32[2,512]{1,0:T(2,128)}, u32[]{:S(2)}) copy-start(f32[2,512]{1,0:T(2,128)} %param.27) | copy-start | bytes 12292
  5.4 11.5 %copy-start.26 = (f32[1024]{0:T(1024)S(1)}, f32[1024]{0:T(1024)}, u32[]{:S(2)}) copy-start(f32[1024]{0:T(1024)} %param.26) | copy-start | bytes 12292
  5.4 33.3 %all-to-all-start.1 = ((bf16[32,40,640]{2,1,0:T(8,128)(2,1)}), bf16[32,40,640]{2,1,0:T(8,128)(2,1)S(1)}, u32[]{:S(2)}, u32[]{:S(2)}) async-start(bf16[32,40,640]{2,1,0:T(8,128)(2,1)} %bitcast.42), calls=%async_computation.1 | async-start | bytes 3276800 | tf_op jit(solution)/shard_map/all_to_all | solution.py:576
  38.8 1.2 copy-start.20
  38.8 7.0 %copy-start.22 = (bf16[2048,256]{1,0:T(8,128)(2,1)S(1)}, bf16[2048,256]{1,0:T(8,128)(2,1)}, u32[]{:S(2)}) copy-start(bf16[2048,256]{1,0:T(8,128)(2,1)} %whole_own.1) | copy-start | bytes 3145732
  39.9 60.5 %all-to-all-start = ((bf16[32,40,1792]{2,1,0:T(8,128)(2,1)}), bf16[32,40,1792]{2,1,0:T(8,128)(2,1)}, u32[]{:S(2)}, u32[]{:S(2)}) async-start(bf16[32,40,1792]{2,1,0:T(8,128)(2,1)} %bitcast.43), calls=%async_computation | async-start | bytes 9175040 | tf_op jit(solution)/shard_map/all_to_all | solution.py:576
  45.8 48.6 %copy-start.18 = (bf16[512,2048]{1,0:T(8,128)(2,1)S(1)}, bf16[512,2048]{1,0:T(8,128)(2,1)}, u32[]{:S(2)}) copy-start(bf16[512,2048]{1,0:T(8,128)(2,1)} %refs_1_.3) | copy-start | bytes 6291460
  45.8 48.6 %copy-start.21 = (bf16[512,256]{1,0:T(8,128)(2,1)S(1)}, bf16[512,256]{1,0:T(8,128)(2,1)}, u32[]{:S(2)}) copy-start(bf16[512,256]{1,0:T(8,128)(2,1)} %get-tuple-element.31.refs_2_) | copy-start | bytes 786436
  45.8 14.5 %collective-permute-start.6 = (bf16[1024,256]{1,0:T(8,128)(2,1)S(1)}, bf16[1024,256]{1,0:T(8,128)(2,1)S(1)}, u32[]{:S(2)}, u32[]{:S(2)}) collective-permute-start(bf16[1024,256]{1,0:T(8,128)(2,1)S(1)} %constant_dynamic-slice_fusion), channel_id=1, source_target_pairs={{0,1},{1,2},{2,3},{3,0},{4,5},{5,6},{6,7},{7,4},{8,9},{9,10},{10,1... | collective-permute-start | bytes 1572872 | tf_op jit(solution)/shard_map/ppermute | solution.py:536
  47.1 13.3 %collective-permute-start.7 = (bf16[1024,256]{1,0:T(8,128)(2,1)S(1)}, bf16[1024,256]{1,0:T(8,128)(2,1)}, u32[]{:S(2)}, u32[]{:S(2)}) collective-permute-start(bf16[1024,256]{1,0:T(8,128)(2,1)S(1)} %constant_dynamic-slice_fusion), channel_id=1, source_target_pairs={{0,3},{1,0},{2,1},{3,2},{4,7},{5,4},{6,5},{7,6},{8,11},{9,8},{10,9... | collective-permute-start | bytes 1572872 | tf_op jit(solution)/shard_map/ppermute | solution.py:536
  50.1 71.5 %copy-start = (bf16[16,40,640]{2,1,0:T(8,128)(2,1)}, bf16[16,40,640]{2,1,0:T(8,128)(2,1)S(1)}, u32[]{:S(2)}) copy-start(bf16[16,40,640]{2,1,0:T(8,128)(2,1)S(1)} %get-tuple-element.59) | copy-start | bytes 2457604
  50.1 41.6 %collective-permute-start = (bf16[640,640]{1,0:T(8,128)(2,1)S(1)}, bf16[640,640]{1,0:T(8,128)(2,1)S(1)}, u32[]{:S(2)}, u32[]{:S(2)}) collective-permute-start(bf16[640,640]{1,0:T(8,128)(2,1)S(1)} %bitcast.37), channel_id=1, source_target_pairs={{0,1},{1,2},{2,3},{3,0},{4,5},{5,6},{6,7},{7,4},{8,9},{9,10},{10,1... | collective-permute-start | bytes 2457608 | tf_op jit(solution)/shard_map/ppermute | solution.py:536
  50.2 41.5 %collective-permute-start.3 = (bf16[640,640]{1,0:T(8,128)(2,1)S(1)}, bf16[640,640]{1,0:T(8,128)(2,1)S(1)}, u32[]{:S(2)}, u32[]{:S(2)}) collective-permute-start(bf16[640,640]{1,0:T(8,128)(2,1)S(1)} %bitcast.33), channel_id=1, source_target_pairs={{0,3},{1,0},{2,1},{3,2},{4,7},{5,4},{6,5},{7,6},{8,11},{9,8},{10,9... | collective-permute-start | bytes 2457608 | tf_op jit(solution)/shard_map/ppermute | solution.py:536
  60.3 23.2 %collective-permute-start.8 = (bf16[512,256]{1,0:T(8,128)(2,1)S(1)}, bf16[512,256]{1,0:T(8,128)(2,1)S(1)}, u32[]{:S(2)}, u32[]{:S(2)}) collective-permute-start(bf16[512,256]{1,0:T(8,128)(2,1)S(1)} %slice.42), channel_id=1, source_target_pairs={{0,1},{1,2},{2,3},{3,0},{4,5},{5,6},{6,7},{7,4},{8,9},{9,10},{10,1... | collective-permute-start | bytes 786440 | tf_op jit(solution)/shard_map/ppermute | solution.py:536
  61.3 24.0 %collective-permute-start.9 = (bf16[512,256]{1,0:T(8,128)(2,1)S(1)}, bf16[512,256]{1,0:T(8,128)(2,1)S(1)}, u32[]{:S(2)}, u32[]{:S(2)}) collective-permute-start(bf16[512,256]{1,0:T(8,128)(2,1)S(1)} %slice.43), channel_id=1, source_target_pairs={{0,3},{1,0},{2,1},{3,2},{4,7},{5,4},{6,5},{7,6},{8,11},{9,8},{10,9... | collective-permute-start | bytes 786440 | tf_op jit(solution)/shard_map/ppermute | solution.py:536
  64.1 24.2 %collective-permute-start.10 = (bf16[1024,256]{1,0:T(8,128)(2,1)S(1)}, bf16[1024,256]{1,0:T(8,128)(2,1)S(1)}, u32[]{:S(2)}, u32[]{:S(2)}) collective-permute-start(bf16[1024,256]{1,0:T(8,128)(2,1)S(1)} %collective-permute-done.6.refs_0_), channel_id=1, source_target_pairs={{0,4},{4,0},{1,5},{5,1},{2,6},{6,2},{3,7},{7,3},{8,12},{12,8},{9,1... | collective-permute-start | bytes 1572872 | tf_op jit(solution)/shard_map/ppermute | solution.py:553
  66.7 0.8 copy-start.6
  83.4 2.6 %collective-permute-start.12 = (bf16[512,256]{1,0:T(8,128)(2,1)S(1)}, bf16[512,256]{1,0:T(8,128)(2,1)S(1)}, u32[]{:S(2)}, u32[]{:S(2)}) collective-permute-start(bf16[512,256]{1,0:T(8,128)(2,1)S(1)} %collective-permute-done.8.refs_2_), channel_id=1, source_target_pairs={{0,4},{4,0},{1,5},{5,1},{2,6},{6,2},{3,7},{7,3},{8,12},{12,8},{9,1... | collective-permute-start | bytes 786440 | tf_op jit(solution)/shard_map/ppermute | solution.py:553
  84.6 0.7 copy-start.10
  85.3 1.9 collective-permute-start.13
  85.3 0.7 copy-start.12
  86.0 0.7 copy-start.14
  86.7 20.6 %collective-permute-start.1 = (bf16[640,640]{1,0:T(8,128)(2,1)S(1)}, bf16[640,640]{1,0:T(8,128)(2,1)}, u32[]{:S(2)}, u32[]{:S(2)}) collective-permute-start(bf16[640,640]{1,0:T(8,128)(2,1)S(1)} %bitcast.34), channel_id=1, source_target_pairs={{0,1},{1,2},{2,3},{3,0},{4,5},{5,6},{6,7},{7,4},{8,9},{9,10},{10,1... | collective-permute-start | bytes 2457608 | tf_op jit(solution)/shard_map/ppermute | solution.py:536
  87.2 0.7 copy-start.16
  88.0 14.5 %collective-permute-start.11 = (bf16[1024,256]{1,0:T(8,128)(2,1)}, bf16[1024,256]{1,0:T(8,128)(2,1)}, u32[]{:S(2)}, u32[]{:S(2)}) collective-permute-start(bf16[1024,256]{1,0:T(8,128)(2,1)} %collective-permute-done.7.refs_1_), channel_id=1, source_target_pairs={{0,4},{4,0},{1,5},{5,1},{2,6},{6,2},{3,7},{7,3},{8,12},{12,8},{9,1... | collective-permute-start | bytes 1572872 | tf_op jit(solution)/shard_map/ppermute | solution.py:553
  88.2 0.8 copy-start.8
  89.0 32.5 %collective-permute-start.2 = (bf16[640,640]{1,0:T(8,128)(2,1)S(1)}, bf16[640,640]{1,0:T(8,128)(2,1)}, u32[]{:S(2)}, u32[]{:S(2)}) collective-permute-start(bf16[640,640]{1,0:T(8,128)(2,1)S(1)} %bitcast.38), channel_id=1, source_target_pairs={{0,3},{1,0},{2,1},{3,2},{4,7},{5,4},{6,5},{7,6},{8,11},{9,8},{10,9... | collective-permute-start | bytes 2457608 | tf_op jit(solution)/shard_map/ppermute | solution.py:536
  91.7 29.9 %copy-start.2 = (bf16[640,640]{1,0:T(8,128)(2,1)}, bf16[640,640]{1,0:T(8,128)(2,1)S(1)}, u32[]{:S(2)}) copy-start(bf16[640,640]{1,0:T(8,128)(2,1)S(1)} %collective-permute-done.refs_2_) | copy-start | bytes 2457604
  91.7 36.4 %collective-permute-start.4 = (bf16[640,640]{1,0:T(8,128)(2,1)S(1)}, bf16[640,640]{1,0:T(8,128)(2,1)}, u32[]{:S(2)}, u32[]{:S(2)}) collective-permute-start(bf16[640,640]{1,0:T(8,128)(2,1)S(1)} %collective-permute-done.refs_2_), channel_id=1, source_target_pairs={{0,1},{1,2},{2,3},{3,0},{4,5},{5,6},{6,7},{7,4},{8,9},{9,10},{10,1... | collective-permute-start | bytes 2457608 | tf_op jit(solution)/shard_map/ppermute | solution.py:536
  91.7 29.9 %copy-start.4 = (bf16[640,640]{1,0:T(8,128)(2,1)}, bf16[640,640]{1,0:T(8,128)(2,1)S(1)}, u32[]{:S(2)}) copy-start(bf16[640,640]{1,0:T(8,128)(2,1)S(1)} %collective-permute-done.3.refs_5_) | copy-start | bytes 2457604
  91.7 45.7 %collective-permute-start.5 = (bf16[640,640]{1,0:T(8,128)(2,1)S(1)}, bf16[640,640]{1,0:T(8,128)(2,1)}, u32[]{:S(2)}, u32[]{:S(2)}) collective-permute-start(bf16[640,640]{1,0:T(8,128)(2,1)S(1)} %collective-permute-done.3.refs_5_), channel_id=1, source_target_pairs={{0,3},{1,0},{2,1},{3,2},{4,7},{5,4},{6,5},{7,6},{8,11},{9,8},{10,9... | collective-permute-start | bytes 2457608 | tf_op jit(solution)/shard_map/ppermute | solution.py:536
  102.4 29.5 %collective-permute-start.14 = (bf16[640,256]{1,0:T(8,128)(2,1)}, bf16[640,256]{1,0:T(8,128)(2,1)}, u32[]{:S(2)}, u32[]{:S(2)}) collective-permute-start(bf16[640,256]{1,0:T(8,128)(2,1)} %get-tuple-element.57.refs_0_), channel_id=1, source_target_pairs={{0,1},{1,2},{2,3},{3,0},{4,5},{5,6},{6,7},{7,4},{8,9},{9,10},{10,1... | collective-permute-start | bytes 983048 | tf_op jit(solution)/shard_map/ppermute | solution.py:536
  107.3 26.7 %collective-permute-start.17 = (bf16[640,256]{1,0:T(8,128)(2,1)}, bf16[640,256]{1,0:T(8,128)(2,1)}, u32[]{:S(2)}, u32[]{:S(2)}) collective-permute-start(bf16[640,256]{1,0:T(8,128)(2,1)} %get-tuple-element.56.refs_1_), channel_id=1, source_target_pairs={{0,3},{1,0},{2,1},{3,2},{4,7},{5,4},{6,5},{7,6},{8,11},{9,8},{10,9... | collective-permute-start | bytes 983048 | tf_op jit(solution)/shard_map/ppermute | solution.py:536
  108.6 1.0 copy-start.7
  109.6 1.0 copy-start.9
  110.7 0.9 copy-start.11
  111.6 0.9 copy-start.13
  112.6 0.9 copy-start.15
  113.5 0.9 copy-start.17
  128.0 27.8 %collective-permute-start.15 = (bf16[640,256]{1,0:T(8,128)(2,1)}, bf16[640,256]{1,0:T(8,128)(2,1)}, u32[]{:S(2)}, u32[]{:S(2)}) collective-permute-start(bf16[640,256]{1,0:T(8,128)(2,1)} %get-tuple-element.56.refs_1_), channel_id=1, source_target_pairs={{0,1},{1,2},{2,3},{3,0},{4,5},{5,6},{6,7},{7,4},{8,9},{9,10},{10,1... | collective-permute-start | bytes 983048 | tf_op jit(solution)/shard_map/ppermute | solution.py:536
  128.2 27.6 %collective-permute-start.16 = (bf16[640,256]{1,0:T(8,128)(2,1)}, bf16[640,256]{1,0:T(8,128)(2,1)}, u32[]{:S(2)}, u32[]{:S(2)}) collective-permute-start(bf16[640,256]{1,0:T(8,128)(2,1)} %get-tuple-element.57.refs_0_), channel_id=1, source_target_pairs={{0,3},{1,0},{2,1},{3,2},{4,7},{5,4},{6,5},{7,6},{8,11},{9,8},{10,9... | collective-permute-start | bytes 983048 | tf_op jit(solution)/shard_map/ppermute | solution.py:536
  131.9 23.9 %collective-permute-start.18 = (bf16[640,256]{1,0:T(8,128)(2,1)}, bf16[640,256]{1,0:T(8,128)(2,1)}, u32[]{:S(2)}, u32[]{:S(2)}) collective-permute-start(bf16[640,256]{1,0:T(8,128)(2,1)} %collective-permute-done.14.refs_2_), channel_id=1, source_target_pairs={{0,1},{1,2},{2,3},{3,0},{4,5},{5,6},{6,7},{7,4},{8,9},{9,10},{10,1... | collective-permute-start | bytes 983048 | tf_op jit(solution)/shard_map/ppermute | solution.py:536
  134.0 21.8 %collective-permute-start.19 = (bf16[640,256]{1,0:T(8,128)(2,1)}, bf16[640,256]{1,0:T(8,128)(2,1)}, u32[]{:S(2)}, u32[]{:S(2)}) collective-permute-start(bf16[640,256]{1,0:T(8,128)(2,1)} %collective-permute-done.17.refs_5_), channel_id=1, source_target_pairs={{0,3},{1,0},{2,1},{3,2},{4,7},{5,4},{6,5},{7,6},{8,11},{9,8},{10,9... | collective-permute-start | bytes 983048 | tf_op jit(solution)/shard_map/ppermute | solution.py:536
  147.6 44.1 %all-to-all-start.3 = ((bf16[128,40,256]{2,1,0:T(8,128)(2,1)}), bf16[128,40,256]{2,1,0:T(8,128)(2,1)S(1)}, u32[]{:S(2)}, u32[]{:S(2)}) async-start(bf16[128,40,256]{2,1,0:T(8,128)(2,1)} %bitcast.44), calls=%async_computation.3 | async-start | bytes 5242880 | tf_op jit(solution)/shard_map/all_to_all | solution.py:614
  165.4 4.4 %copy-start.19 = (bf16[512,2048]{1,0:T(8,128)(2,1)S(1)}, bf16[512,2048]{1,0:T(8,128)(2,1)}, u32[]{:S(2)}) copy-start(bf16[512,2048]{1,0:T(8,128)(2,1)} %refs_1_.3) | copy-start | bytes 6291460
  165.5 4.4 %copy-start.23 = (bf16[2048,256]{1,0:T(8,128)(2,1)S(1)}, bf16[2048,256]{1,0:T(8,128)(2,1)}, u32[]{:S(2)}) copy-start(bf16[2048,256]{1,0:T(8,128)(2,1)} %whole_own.1) | copy-start | bytes 3145732
  168.8 32.1 %collective-permute-start.20 = (bf16[4,16,64,256]{3,2,1,0:T(8,128)(2,1)}, bf16[4,16,64,256]{3,2,1,0:T(8,128)(2,1)}, u32[]{:S(2)}, u32[]{:S(2)}) collective-permute-start(bf16[4,16,64,256]{3,2,1,0:T(8,128)(2,1)} %slice_bitcast_fusion), channel_id=1, source_target_pairs={{0,4},{4,0},{1,5},{5,1},{2,6},{6,2},{3,7},{7,3},{8,12},{12,8},{9,1... | collective-permute-start | bytes 6291464 | tf_op jit(solution)/shard_map/ppermute | solution.py:624
  196.2 12.1 %all-to-all-start.4 = ((f32[32,2,256]{2,1,0:T(2,128)}), f32[32,2,256]{2,1,0:T(2,128)S(1)}, u32[]{:S(2)}, u32[]{:S(2)}) async-start(f32[32,2,256]{2,1,0:T(2,128)} %get-tuple-element.49), calls=%async_computation.4 | async-start | bytes 131072 | tf_op jit(solution)/shard_map/all_to_all | solution.py:633
  208.3 6.1 %copy-start.1 = (bf16[16,40,640]{2,1,0:T(8,128)(2,1)S(1)}, bf16[16,40,640]{2,1,0:T(8,128)(2,1)}, u32[]{:S(2)}) copy-start(bf16[16,40,640]{2,1,0:T(8,128)(2,1)} %copy-done) | copy-start | bytes 2457604
  208.3 6.1 %copy-start.3 = (bf16[640,640]{1,0:T(8,128)(2,1)S(1)}, bf16[640,640]{1,0:T(8,128)(2,1)}, u32[]{:S(2)}) copy-start(bf16[640,640]{1,0:T(8,128)(2,1)} %copy-done.2) | copy-start | bytes 2457604
  208.3 6.1 %copy-start.5 = (bf16[640,640]{1,0:T(8,128)(2,1)S(1)}, bf16[640,640]{1,0:T(8,128)(2,1)}, u32[]{:S(2)}) copy-start(bf16[640,640]{1,0:T(8,128)(2,1)} %copy-done.4) | copy-start | bytes 2457604
  208.3 33.3 %all-to-all-start.2 = ((bf16[64,64,256]{2,1,0:T(8,128)(2,1)}), bf16[64,64,256]{2,1,0:T(8,128)(2,1)}, u32[]{:S(2)}, u32[]{:S(2)}) async-start(bf16[64,64,256]{2,1,0:T(8,128)(2,1)} %bitcast.41), calls=%async_computation.2 | async-start | bytes 4194304 | tf_op jit(solution)/shard_map/all_to_all | solution.py:626

commit v4 on v3

--- a/solution.py
+++ b/solution.py
@@ -117,10 +117,15 @@
     place_one = first_id * capacity + jnp.sum(rank * one, axis=1, keepdims=True).astype(jnp.int32)
     place_two = second_id * capacity + jnp.sum(rank * two, axis=1, keepdims=True).astype(jnp.int32)
     slots = experts * capacity
-    for at in range(0, slots, 256):
+
+    def block_of_slots(i, _):
+        at = pl.multiple_of(i * 256, 256)
         slot = lax.broadcasted_iota(jnp.int32, (tokens, 256), 1) + at
         hit = (slot == place_one) | (slot == place_two)
-        out_sel[:, at : at + 256] = jnp.where(hit, 1.0, 0.0).astype(BF16)
+        out_sel[:, pl.ds(at, 256)] = jnp.where(hit, 1.0, 0.0).astype(BF16)
+        return 0
+
+    lax.fori_loop(0, slots // 256, block_of_slots, 0)
 
 
 def early(position, ids, rec, gate_in, prev, rates, extra, map_a, map_i, capacity, experts):
@@ -406,16 +411,14 @@
         compiler_params=params(30),
         cost_estimate=cost(4 * 10**9, 17 * 2**20),
         name="grads",
-    )(position, *kept([got, got]), *pieces, *kept(tail[len(pieces) :]))
+    )(position, *kept([got, got, *tail]))
 
 
 def proj_kernel(where_ref, gate_cot, up_cot, w_gate, w_up, local, *refs):
     pieces, out = refs[:-1], refs[-1]
-    at = where_ref[0]
     core = where_ref[1]
     first = ((0,), (0,))
     for n, step in enumerate(ring_steps):
-        group = lax.rem(at + step, 4)
         top, bottom = pieces[2 * n], pieces[2 * n + 1]
         half = top.shape[0]
         push_gate, push_up = (
@@ -429,7 +432,7 @@
         lines = out.shape[3]
         for s in range(2 * out.shape[2]):
             slot = lax.rem(s % 2 + core, 2)
-            out[slot, group, s // 2] = term[s * lines : (s + 1) * lines, :]
+            out[slot, n, s // 2] = term[s * lines : (s + 1) * lines, :]
 
 
 def proj(position, gate_cot, up_cot, w_gate, w_up, local, pieces, lines):
@@ -445,6 +448,38 @@
         cost_estimate=cost(4 * 10**9, 14 * 2**20),
         name="proj",
     )(position, *kept(args[1:6]), *pieces)
+
+
+def chip_kernel(kept_ref, other, out_own, *outs):
+    half = out_own.shape[0] // 2
+    out_own[...] = (kept_ref[0, 0].astype(F32) + other[0].astype(F32)).astype(BF16)
+    for n in range(6):
+        lines = slice((n % 2) * half, (n % 2 + 1) * half)
+        at = 1 + n // 2
+        outs[n][...] = (
+            kept_ref[0, at, lines].astype(F32) + other[at, lines].astype(F32)
+        ).astype(BF16)
+
+
+def chip_sum(parts, other):
+    groups, lines, width = other.shape[1:]
+    half = made((groups // 2, lines, width), BF16)
+    outs = (made((groups, lines, width), BF16),) + (half,) * 6
+    return pl.pallas_call(
+        chip_kernel,
+        out_shape=outs,
+        grid=(1,),
+        in_specs=[
+            pl.BlockSpec(
+                (1, *parts.shape[1:]), lambda i: (0, 0, 0, 0, 0), pipeline_mode=pl.Buffered(1)
+            ),
+            whole(other.shape),
+        ],
+        out_specs=[whole(o.shape) for o in outs],
+        compiler_params=params(16),
+        cost_estimate=cost(10**7, 6 * 2**20),
+        name="chipsum",
+    )(*kept([parts]), other)
 
 
 def scan_kernel(back, sel, base, act, b, decay, seg, block, out_grad, out_local, out_pair, drive, part):
@@ -622,10 +657,20 @@
     lines = width // sources
     parts = proj(position, gate_cot, up_cot, w_gate, w_up, local_proj, recs, lines)
     other = lax.ppermute(parts[1], "core", [(0, 1), (1, 0)])
-    chip = (parts[0].astype(F32) + other.astype(F32)).astype(BF16)
-    arrived = lax.all_to_all(
-        chip.reshape(4 * chip.shape[1], lines, -1), ("tp", "sq"), 0, 0, tiled=True
-    )
+    own, left_top, left_bottom, right_top, right_bottom, far_top, far_bottom = chip_sum(
+        parts, other
+    )
+    through_top, through_bottom = shifted(far_top, 1), shifted(far_bottom, -1)
+    from_left, from_right = shifted(right_bottom, 1), shifted(left_top, -1)
+    both_top = (right_top.astype(F32) + through_top.astype(F32)).astype(BF16)
+    both_bottom = (left_bottom.astype(F32) + through_bottom.astype(F32)).astype(BF16)
+    last_top, last_bottom = shifted(both_top, 1), shifted(both_bottom, -1)
+    arriving = (
+        jnp.concatenate([last_top, last_bottom], axis=0).astype(F32)
+        + jnp.concatenate([from_right, from_left], axis=0).astype(F32)
+        + own.astype(F32)
+    ).astype(BF16)
+    arrived = lax.all_to_all(arriving, "sq", 0, 0, tiled=True)
     grad_out_proj = arrived.astype(F32).sum(axis=0)
     gate_input_grad, local, pair = scanned(
         back, sel, base, act, b, decay, seg, block, sources

time: 247 us -> 255 us (1.032)
  starting transfers between devices: 62.2 us -> 72.5 us
  Pallas kernels: 70.1 us -> 75.6 us
  waiting for transfers between devices: 78.4 us -> 74.9 us
    ppermute x16 -> x22, waiting for transfers between devices: 30.4 us -> 60 us  [shifted(): return lax.ppermute(piece, 'tp', [(i, (i + by) % 4) for i in range(4)])]
    all_to_all x1, waiting for transfers between devices: 20.3 us -> 0.01 us  [per_device(): lax.all_to_all(mix.reshape(4 * sources, capacity, -1), ('tp', *sp_axes),...]
    all_to_all x1, waiting for transfers between devices: 13.4 us -> 0.01 us  [per_device(): arrived = lax.all_to_all(arriving, 'sq', 0, 0, tiled=True)]
    ppermute x16 -> x22, starting transfers between devices: 22.7 us -> 29.6 us  [shifted(): return lax.ppermute(piece, 'tp', [(i, (i + by) % 4) for i in range(4)])]
    all_to_all x1, starting transfers between devices: 4.69 us -> 9.11 us  [per_device(): pairs = lax.all_to_all(pair, sp_axes, 0, 0, tiled=True)]
    pallas_call x0 -> x1, Pallas kernels: none -> 3.73 us  [chip_sum(): pl.pallas_call(chip_kernel, out_shape=outs, grid=(1,), in_specs=[pl.Block...]
    unnamed x56 -> x54, local copies, waits for them, and re-layouts: 13.2 us -> 13.2 us
  transfers between devices with their start and end apart: 26 -> 32, of which waited for: 10 -> 10; matrix products, arithmetic and copies ran while one was open for 8% -> 6% of each run, Pallas kernels for 27% -> 24%
where the time goes in v4:
time: 255 us; the launch traced here: 254 us
  Pallas kernels  75.6 us (30%)
  waiting for transfers between devices  74.9 us (29%)
  starting transfers between devices  72.5 us (28%)
  local copies, waits for them, and re-layouts  20.1 us (8%)
  other arithmetic  6.37 us (2%)
  matrix products  3.76 us (1%)
    ppermute x22, waiting for transfers between devices, shifted(): return lax.ppermute(piece, 'tp', [(i, (i + by) % 4) for i in range(4)])  60 us
    ppermute x22, starting transfers between devices, shifted(): return lax.ppermute(piece, 'tp', [(i, (i + by) % 4) for i in range(4)])  29.6 us
    all_to_all x2, starting transfers between devices, exchanged(): lax.all_to_all(rows.reshape(sources, capacity, -1), sp_axes, 0, 0, tiled=...  15.5 us
    unnamed x54, local copies, waits for them, and re-layouts  13.2 us
    pallas_call x1, Pallas kernels, grads(): pl.pallas_call(functools.partial(grads_kernel, row_part=row_part, cot_par...  12 us
    pallas_call x2, Pallas kernels, build(): pl.pallas_call(functools.partial(build_kernel, capacity=capacity, group=g...  11.5 us
    pallas_call x1, Pallas kernels, expert(): pl.pallas_call(functools.partial(expert_kernel, row_part=row_part), out_s...  10.2 us
    all_to_all x2, waiting for transfers between devices, exchanged(): lax.all_to_all(rows.reshape(sources, capacity, -1), sp_axes, 0, 0, tiled=...  9.86 us
  transfers between devices with their start and end apart: 32, of which 10 were waited for; matrix products, arithmetic and copies ran while one was open for 6% of the time, Pallas kernels for 24%

profile of v4, /device:TPU:1, one launch (start us, length us, event | category | flops | bytes accessed | tf_op | source)
XLA Modules:
  0.0 254.2 jit_solution(16758746129355108940)
XLA Ops:
  0.7 4.7 %shard_map.191 = bf16[1280,640]{1,0:T(8,128)(2,1)} custom-call(s32[3]{0:T(128)S(1)} %pad_add_fusion.where_ref, s32[2,512]{1,0:T(2,128)} %bitcast.39, f32[2,512]{1,0:T(2,128)} %bitcast.41, bf16[512,2048]{1,0:T(8,128)(2,1)} %refs_0_.3, bf16[512,2048]{1,0:T(8,128)(2,1)} %refs_1_.3), custom_call_target="tpu_custom_call" | custom-call | flops 896000000 | bytes 3200000 | tf_op jit(solution)/shard_map/pallas_call | solution.py:196
  5.4 9.7 %all-to-all-start.1 = ((bf16[32,40,640]{2,1,0:T(8,128)(2,1)}), bf16[32,40,640]{2,1,0:T(8,128)(2,1)S(1)}, u32[]{:S(2)}, u32[]{:S(2)}) async-start(bf16[32,40,640]{2,1,0:T(8,128)(2,1)} %bitcast.35), calls=%async_computation.1 | async-start | bytes 3276800 | tf_op jit(solution)/shard_map/all_to_all | solution.py:611
  15.2 0.9 copy.22.ids
  16.0 0.9 copy.21
  17.5 8.4 %early.1 = (bf16[512,256]{1,0:T(8,128)(2,1)}, f32[512,256]{1,0:T(8,128)}, f32[512,256]{1,0:T(8,128)}, f32[512,256]{1,0:T(8,128)}, f32[512,256]{1,0:T(8,128)}, /*...) custom-call(s32[3]{0:T(128)S(1)} %pad_add_fusion.where_ref, ...), custom_call_target="tpu_custom_call" | custom-call | flops 3000000000 | bytes 8388608 | tf_op jit(solution)/shard_map/early/pallas_call | solution.py:142
  25.9 6.8 %shard_map.190 = bf16[1280,1792]{1,0:T(8,128)(2,1)} custom-call(s32[3]{0:T(128)S(1)} %pad_add_fusion.where_ref, s32[2,512]{1,0:T(2,128)} %bitcast.40, f32[2,512]{1,0:T(2,128)} %bitcast.42, bf16[512,2048]{1,0:T(8,128)(2,1)} %refs_0_.3, bf16[512,2048]{1,0:T(8,128)(2,1)} %refs_1_.3, bf16[512,256]{1,0:T(8,128)(2,1)} %get-tuple-element.38.refs_2_), custom_call_target="tpu_custom_call" | custom-call | flops 2508800000 | bytes 8960000 | tf_op jit(solution)/shard_map/pallas_call | solution.py:196
  32.7 6.0 %all-to-all-done.1 = bf16[32,40,640]{2,1,0:T(8,128)(2,1)S(1)} async-done(((bf16[32,40,640]{2,1,0:T(8,128)(2,1)}), bf16[32,40,640]{2,1,0:T(8,128)(2,1)S(1)}, u32[]{:S(2)}, u32[]{:S(2)}) %all-to-all-start.1) | async-done | bytes 1638432 | tf_op jit(solution)/shard_map/all_to_all | solution.py:611
  38.8 1.2 copy-done.18
  39.9 5.8 %all-to-all-start = ((bf16[32,40,1792]{2,1,0:T(8,128)(2,1)}), bf16[32,40,1792]{2,1,0:T(8,128)(2,1)}, u32[]{:S(2)}, u32[]{:S(2)}) async-start(bf16[32,40,1792]{2,1,0:T(8,128)(2,1)} %bitcast.36), calls=%async_computation | async-start | bytes 9175040 | tf_op jit(solution)/shard_map/all_to_all | solution.py:611
  45.8 1.3 collective-permute-start.6
  47.1 1.5 collective-permute-start.7
  48.6 1.5 fusion.3
  50.2 2.7 %collective-permute-start.3 = (bf16[640,640]{1,0:T(8,128)(2,1)S(1)}, bf16[640,640]{1,0:T(8,128)(2,1)S(1)}, u32[]{:S(2)}, u32[]{:S(2)}) collective-permute-start(bf16[640,640]{1,0:T(8,128)(2,1)S(1)} %bitcast.27), channel_id=1, source_target_pairs={{0,3},{1,0},{2,1},{3,2},{4,7},{5,4},{6,5},{7,6},{8,11},{9,8},{10,9... | collective-permute-start | bytes 2457608 | tf_op jit(solution)/shard_map/ppermute | solution.py:571
  52.9 7.4 %collective-permute-done.6.refs_0_ = bf16[1024,256]{1,0:T(8,128)(2,1)S(1)} collective-permute-done((bf16[1024,256]{1,0:T(8,128)(2,1)S(1)}, bf16[1024,256]{1,0:T(8,128)(2,1)S(1)}, u32[]{:S(2)}, u32[]{:S(2)}) %collective-permute-start.6) | collective-permute-done | bytes 524320 | tf_op jit(solution)/shard_map/ppermute | solution.py:571
  60.4 1.0 slice.39
  61.3 2.7 %collective-permute-start.9 = (bf16[512,256]{1,0:T(8,128)(2,1)S(1)}, bf16[512,256]{1,0:T(8,128)(2,1)S(1)}, u32[]{:S(2)}, u32[]{:S(2)}) collective-permute-start(bf16[512,256]{1,0:T(8,128)(2,1)S(1)} %slice.39), channel_id=1, source_target_pairs={{0,3},{1,0},{2,1},{3,2},{4,7},{5,4},{6,5},{7,6},{8,11},{9,8},{10,9... | collective-permute-start | bytes 786440 | tf_op jit(solution)/shard_map/ppermute | solution.py:571
  64.1 2.6 %collective-permute-start.10 = (bf16[1024,256]{1,0:T(8,128)(2,1)S(1)}, bf16[1024,256]{1,0:T(8,128)(2,1)S(1)}, u32[]{:S(2)}, u32[]{:S(2)}) collective-permute-start(bf16[1024,256]{1,0:T(8,128)(2,1)S(1)} %collective-permute-done.6.refs_0_), channel_id=1, source_target_pairs={{0,4},{4,0},{1,5},{5,1},{2,6},{6,2},{3,7},{7,3},{8,12},{12,8},{9,1... | collective-permute-start | bytes 1572872 | tf_op jit(solution)/shard_map/ppermute | solution.py:588
  66.7 0.8 copy-done.4
  67.5 16.0 %collective-permute-done.8.refs_2_ = bf16[512,256]{1,0:T(8,128)(2,1)S(1)} collective-permute-done((bf16[512,256]{1,0:T(8,128)(2,1)S(1)}, bf16[512,256]{1,0:T(8,128)(2,1)S(1)}, u32[]{:S(2)}, u32[]{:S(2)}) %collective-permute-start.8) | collective-permute-done | bytes 262176 | tf_op jit(solution)/shard_map/ppermute | solution.py:571
  83.4 1.2 collective-permute-start.12
  86.0 0.7 copy-done.12
  88.2 0.8 copy-done.6
  89.0 2.7 %collective-permute-start.2 = (bf16[640,640]{1,0:T(8,128)(2,1)S(1)}, bf16[640,640]{1,0:T(8,128)(2,1)}, u32[]{:S(2)}, u32[]{:S(2)}) collective-permute-start(bf16[640,640]{1,0:T(8,128)(2,1)S(1)} %bitcast.32), channel_id=1, source_target_pairs={{0,3},{1,0},{2,1},{3,2},{4,7},{5,4},{6,5},{7,6},{8,11},{9,8},{10,9... | collective-permute-start | bytes 2457608 | tf_op jit(solution)/shard_map/ppermute | solution.py:571
  91.7 2.7 %collective-permute-start.5 = (bf16[640,640]{1,0:T(8,128)(2,1)S(1)}, bf16[640,640]{1,0:T(8,128)(2,1)}, u32[]{:S(2)}, u32[]{:S(2)}) collective-permute-start(bf16[640,640]{1,0:T(8,128)(2,1)S(1)} %collective-permute-done.3.refs_5_), channel_id=1, source_target_pairs={{0,3},{1,0},{2,1},{3,2},{4,7},{5,4},{6,5},{7,6},{8,11},{9,8},{10,9... | collective-permute-start | bytes 2457608 | tf_op jit(solution)/shard_map/ppermute | solution.py:571
  94.4 2.3 convolution_bitcast_fusion.local
  96.7 3.8 %all-to-all-done = bf16[32,40,1792]{2,1,0:T(8,128)(2,1)} async-done(((bf16[32,40,1792]{2,1,0:T(8,128)(2,1)}), bf16[32,40,1792]{2,1,0:T(8,128)(2,1)}, u32[]{:S(2)}, u32[]{:S(2)}) %all-to-all-start) | async-done | bytes 4587552 | tf_op jit(solution)/shard_map/all_to_all | solution.py:611
  100.5 1.1 fusion.2
  101.6 1.3 collective-permute-start.14
  102.9 4.5 %collective-permute-done.1.refs_3_ = bf16[640,640]{1,0:T(8,128)(2,1)} collective-permute-done((bf16[640,640]{1,0:T(8,128)(2,1)S(1)}, bf16[640,640]{1,0:T(8,128)(2,1)}, u32[]{:S(2)}, u32[]{:S(2)}) %collective-permute-start.1) | collective-permute-done | bytes 819232 | tf_op jit(solution)/shard_map/ppermute | solution.py:571
  107.4 1.3 collective-permute-start.17
  108.6 1.0 copy-done.5
  109.7 1.0 copy-done.7
  110.7 0.9 copy-done.9
  111.6 0.9 copy-done.11
  112.6 0.9 copy-done.13
  113.6 0.9 copy-done.15
  114.5 7.1 %folded.1 = (bf16[2048,512]{1,0:T(8,128)(2,1)}, bf16[2048,256]{1,0:T(8,128)(2,1)}, bf16[4,256,256]{2,1,0:T(8,128)(2,1)}, bf16[4,256,256]{2,1,0:T(8,128)(2,1)}) custom-call(s32[3]{0:T(128)S(1)} %pad_add_fusion.where_ref, bf16[2048,256]{1,0:T(8,128)(2,1)} %bitcast.44, bf16[2048,256]{1,0:T(8,128)(2,1)} %bitcast.46, bf16[256,2048]{1,0:T(8,128)(2,1)} %bitcast.43, ...), custom_call_target="tpu_custom_call" | custom-call | flops 4000000000 | bytes 7340032 | tf_op jit(solution)/shard_map/folded/pallas_call | solution.py:262
  121.6 6.4 %ahead.1.before = f32[1280,768]{1,0:T(8,128)} custom-call(bf16[2048,512]{1,0:T(8,128)(2,1)} %get-tuple-element.39.gate_up, bf16[2048,256]{1,0:T(8,128)(2,1)} %get-tuple-element.40.down, bf16[640,640]{1,0:T(8,128)(2,1)S(1)} %bitcast.33, bf16[640,640]{1,0:T(8,128)(2,1)S(1)} %bitcast.29, bf16[640,640]{1,0:T(8,128)(2,1)S(1)} %collective-permute-done.refs_2_, ...), custom_call_target="tpu_custom_call" | custom-call | flops 2000000000 | bytes 12582912 | tf_op jit(solution)/shard_map/ahead/pallas_call | solution.py:289
  128.2 2.5 collective-permute-start.16
  130.7 1.2 collective-permute-done.14.refs_2_
  131.8 2.1 collective-permute-done.17.refs_5_
  133.9 3.4 %collective-permute-start.19 = (bf16[640,256]{1,0:T(8,128)(2,1)S(1)}, bf16[640,256]{1,0:T(8,128)(2,1)S(1)}, u32[]{:S(2)}, u32[]{:S(2)}) collective-permute-start(bf16[640,256]{1,0:T(8,128)(2,1)S(1)} %collective-permute-done.17.refs_5_), channel_id=1, source_target_pairs={{0,3},{1,0},{2,1},{3,2},{4,7},{5,4},{6,5},{7,6},{8,11},{9,8},{10,9... | collective-permute-start | bytes 983048 | tf_op jit(solution)/shard_map/ppermute | solution.py:571
  137.3 10.2 %expert.1 = (bf16[1280,256]{1,0:T(8,128)(2,1)}, bf16[1280,256]{1,0:T(8,128)(2,1)}, bf16[1280,256]{1,0:T(8,128)(2,1)}, bf16[4,1280,256]{2,1,0:T(8,128)(2,1)}) custom-call(bf16[1280,1792]{1,0:T(8,128)(2,1)} %bitcast.8.got_rows.got_cot, bf16[1280,1792]{1,0:T(8,128)(2,1)} %bitcast.8.got_rows.got_cot, bf16[640,640]{1,0:T(8,128)(2,1)} %collective-permute-done.4.far_top.refs_6_, ...), custom_call_target="tpu_custom_call" | custom-call | flops 5000000000 | bytes 16777216 | tf_op jit(solution)/shard_map/expert/pallas_call | solution.py:343
  147.9 8.9 %proj.1.kept_ref = bf16[2,4,16,64,256]{4,3,2,1,0:T(8,128)(2,1)} custom-call(s32[3]{0:T(128)S(1)} %pad_add_fusion.where_ref, bf16[1280,256]{1,0:T(8,128)(2,1)} %get-tuple-element.44.refs_9_.gate_cot, bf16[1280,256]{1,0:T(8,128)(2,1)} %get-tuple-element.45.refs_10_.up_cot, bf16[2048,256]{1,0:T(8,128)(2,1)} %bitcast.45, bf16[2048,256]{1,0:T(8,128)(2,1)} %bitcast.47, ...), custom_call_target="tpu_custom_call" | custom-call | flops 4000000000 | bytes 14680064 | tf_op jit(solution)/shard_map/proj/pallas_call | solution.py:442
  156.8 3.2 %slice_bitcast_fusion = bf16[4,16,64,256]{3,2,1,0:T(8,128)(2,1)} fusion(bf16[2,4,16,64,256]{4,3,2,1,0:T(8,128)(2,1)} %proj.1.kept_ref), kind=kLoop, calls=%fused_computation.1 | loop fusion | bytes 4194304 | tf_op jit(solution)/shard_map/squeeze | solution.py:659
  160.0 1.2 collective-permute-start.20
  161.2 9.5 %all-to-all-start.3 = ((bf16[128,40,256]{2,1,0:T(8,128)(2,1)}), bf16[128,40,256]{2,1,0:T(8,128)(2,1)S(1)}, u32[]{:S(2)}, u32[]{:S(2)}) async-start(bf16[128,40,256]{2,1,0:T(8,128)(2,1)} %bitcast.37), calls=%async_computation.3 | async-start | bytes 5242880 | tf_op jit(solution)/shard_map/all_to_all | solution.py:649
  170.7 3.7 %chipsum.1 = (bf16[16,64,256]{2,1,0:T(8,128)(2,1)}, bf16[8,64,256]{2,1,0:T(8,128)(2,1)}, bf16[8,64,256]{2,1,0:T(8,128)(2,1)}, bf16[8,64,256]{2,1,0:T(8,128)(2,1)...) custom-call(bf16[2,4,16,64,256]{4,3,2,1,0:T(8,128)(2,1)} %proj.1.kept_ref, ...), custom_call_target="tpu_custom_call" | custom-call | flops 10000000 | bytes 6291456 | tf_op jit(solution)/shard_map/chipsum/pallas_call | solution.py:468
  174.4 1.4 collective-permute-start.21
  175.8 1.3 collective-permute-start.23
  177.1 1.4 collective-permute-start.25
  178.6 28.5 %collective-permute-done.21 = bf16[8,64,256]{2,1,0:T(8,128)(2,1)S(1)} collective-permute-done((bf16[8,64,256]{2,1,0:T(8,128)(2,1)}, bf16[8,64,256]{2,1,0:T(8,128)(2,1)S(1)}, u32[]{:S(2)}, u32[]{:S(2)}) %collective-permute-start.21) | collective-permute-done | bytes 262176 | tf_op jit(solution)/shard_map/ppermute | solution.py:571
  207.1 1.0 add_convert_fusion.2
  208.2 1.7 add_convert_fusion.1
  209.9 2.7 %collective-permute-start.24 = (bf16[8,64,256]{2,1,0:T(8,128)(2,1)}, bf16[8,64,256]{2,1,0:T(8,128)(2,1)}, u32[]{:S(2)}, u32[]{:S(2)}) collective-permute-start(bf16[8,64,256]{2,1,0:T(8,128)(2,1)} %add_convert_fusion.1), channel_id=1, source_target_pairs={{0,3},{1,0},{2,1},{3,2},{4,7},{5,4},{6,5},{7,6},{8,11},{9,8},{10,9... | collective-permute-start | bytes 786440 | tf_op jit(solution)/shard_map/ppermute | solution.py:571
  212.6 1.5 fusion.4.base
  214.1 4.6 %scanned.1 = (bf16[512,256]{1,0:T(8,128)(2,1)}, f32[512,256]{1,0:T(8,128)}, f32[32,2,256]{2,1,0:T(2,128)}) custom-call(bf16[4,1280,256]{2,1,0:T(8,128)(2,1)S(1)} %bitcast.26, bf16[512,1280]{1,0:T(8,128)(2,1)} %get-tuple-element.57.sel, f32[512,256]{1,0:T(8,128)} %fusion.4.base, f32[512,256]{1,0:T(8,128)} %get-tuple-element.58.act, ...), custom_call_target="tpu_custom_call" | custom-call | flops 400000000 | bytes 8388608 | tf_op jit(solution)/shard_map/scanned/pallas_call | solution.py:524
  218.7 9.1 %all-to-all-start.4 = ((f32[32,2,256]{2,1,0:T(2,128)}), f32[32,2,256]{2,1,0:T(2,128)S(1)}, u32[]{:S(2)}, u32[]{:S(2)}) async-start(f32[32,2,256]{2,1,0:T(2,128)} %get-tuple-element.63), calls=%async_computation.4 | async-start | bytes 131072 | tf_op jit(solution)/shard_map/all_to_all | solution.py:678
  227.8 2.3 add_convert_fusion
  230.1 5.0 %all-to-all-done.4.pairs = f32[32,2,256]{2,1,0:T(2,128)S(1)} async-done(((f32[32,2,256]{2,1,0:T(2,128)}), f32[32,2,256]{2,1,0:T(2,128)S(1)}, u32[]{:S(2)}, u32[]{:S(2)}) %all-to-all-start.4) | async-done | bytes 65568 | tf_op jit(solution)/shard_map/all_to_all | solution.py:678
  235.1 3.6 %all-to-all-start.2 = ((bf16[16,64,256]{2,1,0:T(8,128)(2,1)}), bf16[16,64,256]{2,1,0:T(8,128)(2,1)S(1)}, u32[]{:S(2)}, u32[]{:S(2)}) async-start(bf16[16,64,256]{2,1,0:T(8,128)(2,1)} %add_convert_fusion), calls=%async_computation.2 | async-start | bytes 1048576 | tf_op jit(solution)/shard_map/all_to_all | solution.py:673
  238.7 12.0 %grads.1 = (f32[1,2048,256]{2,1,0:T(8,128)}, f32[1,2048,256]{2,1,0:T(8,128)}, f32[1,256,2048]{2,1,0:T(8,128)}) custom-call(s32[3]{0:T(128)S(1)} %pad_add_fusion.where_ref, bf16[1280,1792]{1,0:T(8,128)(2,1)} %bitcast.8.got_rows.got_cot, bf16[1280,1792]{1,0:T(8,128)(2,1)} %bitcast.8.got_rows.got_cot, bf16[640,640]{1,0:T(8,128)(2,1)} %bitcast.34, ...), custom_call_target="tpu_custom_call" | custom-call | flops 4000000000 | bytes 17825792 | tf_op jit(solution)/shard_map/grads/pallas_call | solution.py:398
  250.6 2.9 %final.1 = bf16[512,256]{1,0:T(8,128)(2,1)} custom-call(s32[3]{0:T(128)S(1)} %pad_add_fusion.where_ref, f32[32,2,256]{2,1,0:T(2,128)S(1)} %all-to-all-done.4.pairs, f32[512,256]{1,0:T(8,128)} %get-tuple-element.64.local, f32[512,256]{1,0:T(8,128)} %get-tuple-element.65.exp, f32[512,256]{1,0:T(8,128)} %get-tuple-element.66.ca, ...), custom_call_target="tpu_custom_call" | custom-call | flops 100000000 | bytes 4194304 | tf_op jit(solution)/shard_map/final/pallas_call | solution.py:559
  253.5 0.7 convert_reduce_fusion
  (79 shorter events, 4.8 us)
Async XLA Ops:
  5.4 9.8 %copy-start.23 = (s32[512,2]{0,1:T(2,128)S(1)}, s32[512,2]{0,1:T(2,128)}, u32[]{:S(2)}) copy-start(s32[512,2]{0,1:T(2,128)} %param.17) | copy-start | bytes 12292
  5.4 10.6 %copy-start.24 = (f32[2,512]{1,0:T(2,128)S(1)}, f32[2,512]{1,0:T(2,128)}, u32[]{:S(2)}) copy-start(f32[2,512]{1,0:T(2,128)} %param.27) | copy-start | bytes 12292
  5.4 11.5 %copy-start.25 = (f32[1024]{0:T(1024)S(1)}, f32[1024]{0:T(1024)}, u32[]{:S(2)}) copy-start(f32[1024]{0:T(1024)} %param.26) | copy-start | bytes 12292
  5.4 33.3 %all-to-all-start.1 = ((bf16[32,40,640]{2,1,0:T(8,128)(2,1)}), bf16[32,40,640]{2,1,0:T(8,128)(2,1)S(1)}, u32[]{:S(2)}, u32[]{:S(2)}) async-start(bf16[32,40,640]{2,1,0:T(8,128)(2,1)} %bitcast.35), calls=%async_computation.1 | async-start | bytes 3276800 | tf_op jit(solution)/shard_map/all_to_all | solution.py:611
  38.8 1.2 copy-start.18
  38.8 7.0 %copy-start.21 = (bf16[2048,256]{1,0:T(8,128)(2,1)S(1)}, bf16[2048,256]{1,0:T(8,128)(2,1)}, u32[]{:S(2)}) copy-start(bf16[2048,256]{1,0:T(8,128)(2,1)} %whole_own.1) | copy-start | bytes 3145732
  39.9 60.5 %all-to-all-start = ((bf16[32,40,1792]{2,1,0:T(8,128)(2,1)}), bf16[32,40,1792]{2,1,0:T(8,128)(2,1)}, u32[]{:S(2)}, u32[]{:S(2)}) async-start(bf16[32,40,1792]{2,1,0:T(8,128)(2,1)} %bitcast.36), calls=%async_computation | async-start | bytes 9175040 | tf_op jit(solution)/shard_map/all_to_all | solution.py:611
  45.8 48.6 %copy-start.16 = (bf16[512,2048]{1,0:T(8,128)(2,1)S(1)}, bf16[512,2048]{1,0:T(8,128)(2,1)}, u32[]{:S(2)}) copy-start(bf16[512,2048]{1,0:T(8,128)(2,1)} %refs_1_.3) | copy-start | bytes 6291460
  45.8 48.6 %copy-start.20 = (bf16[512,256]{1,0:T(8,128)(2,1)S(1)}, bf16[512,256]{1,0:T(8,128)(2,1)}, u32[]{:S(2)}) copy-start(bf16[512,256]{1,0:T(8,128)(2,1)} %get-tuple-element.38.refs_2_) | copy-start | bytes 786436
  45.8 14.5 %collective-permute-start.6 = (bf16[1024,256]{1,0:T(8,128)(2,1)S(1)}, bf16[1024,256]{1,0:T(8,128)(2,1)S(1)}, u32[]{:S(2)}, u32[]{:S(2)}) collective-permute-start(bf16[1024,256]{1,0:T(8,128)(2,1)S(1)} %constant_dynamic-slice_fusion), channel_id=1, source_target_pairs={{0,1},{1,2},{2,3},{3,0},{4,5},{5,6},{6,7},{7,4},{8,9},{9,10},{10,1... | collective-permute-start | bytes 1572872 | tf_op jit(solution)/shard_map/ppermute | solution.py:571
  47.1 13.3 %collective-permute-start.7 = (bf16[1024,256]{1,0:T(8,128)(2,1)S(1)}, bf16[1024,256]{1,0:T(8,128)(2,1)}, u32[]{:S(2)}, u32[]{:S(2)}) collective-permute-start(bf16[1024,256]{1,0:T(8,128)(2,1)S(1)} %constant_dynamic-slice_fusion), channel_id=1, source_target_pairs={{0,3},{1,0},{2,1},{3,2},{4,7},{5,4},{6,5},{7,6},{8,11},{9,8},{10,9... | collective-permute-start | bytes 1572872 | tf_op jit(solution)/shard_map/ppermute | solution.py:571
  50.1 71.5 %copy-start = (bf16[16,40,640]{2,1,0:T(8,128)(2,1)}, bf16[16,40,640]{2,1,0:T(8,128)(2,1)S(1)}, u32[]{:S(2)}) copy-start(bf16[16,40,640]{2,1,0:T(8,128)(2,1)S(1)} %get-tuple-element.72) | copy-start | bytes 2457604
  50.1 71.5 %copy-start.1 = (bf16[16,40,640]{2,1,0:T(8,128)(2,1)}, bf16[16,40,640]{2,1,0:T(8,128)(2,1)S(1)}, u32[]{:S(2)}) copy-start(bf16[16,40,640]{2,1,0:T(8,128)(2,1)S(1)} %get-tuple-element.73) | copy-start | bytes 2457604
  50.1 41.6 %collective-permute-start = (bf16[640,640]{1,0:T(8,128)(2,1)S(1)}, bf16[640,640]{1,0:T(8,128)(2,1)S(1)}, u32[]{:S(2)}, u32[]{:S(2)}) collective-permute-start(bf16[640,640]{1,0:T(8,128)(2,1)S(1)} %bitcast.31), channel_id=1, source_target_pairs={{0,1},{1,2},{2,3},{3,0},{4,5},{5,6},{6,7},{7,4},{8,9},{9,10},{10,1... | collective-permute-start | bytes 2457608 | tf_op jit(solution)/shard_map/ppermute | solution.py:571
  50.2 41.5 %collective-permute-start.3 = (bf16[640,640]{1,0:T(8,128)(2,1)S(1)}, bf16[640,640]{1,0:T(8,128)(2,1)S(1)}, u32[]{:S(2)}, u32[]{:S(2)}) collective-permute-start(bf16[640,640]{1,0:T(8,128)(2,1)S(1)} %bitcast.27), channel_id=1, source_target_pairs={{0,3},{1,0},{2,1},{3,2},{4,7},{5,4},{6,5},{7,6},{8,11},{9,8},{10,9... | collective-permute-start | bytes 2457608 | tf_op jit(solution)/shard_map/ppermute | solution.py:571
  60.3 23.2 %collective-permute-start.8 = (bf16[512,256]{1,0:T(8,128)(2,1)S(1)}, bf16[512,256]{1,0:T(8,128)(2,1)S(1)}, u32[]{:S(2)}, u32[]{:S(2)}) collective-permute-start(bf16[512,256]{1,0:T(8,128)(2,1)S(1)} %slice.38), channel_id=1, source_target_pairs={{0,1},{1,2},{2,3},{3,0},{4,5},{5,6},{6,7},{7,4},{8,9},{9,10},{10,1... | collective-permute-start | bytes 786440 | tf_op jit(solution)/shard_map/ppermute | solution.py:571
  61.3 24.0 %collective-permute-start.9 = (bf16[512,256]{1,0:T(8,128)(2,1)S(1)}, bf16[512,256]{1,0:T(8,128)(2,1)S(1)}, u32[]{:S(2)}, u32[]{:S(2)}) collective-permute-start(bf16[512,256]{1,0:T(8,128)(2,1)S(1)} %slice.39), channel_id=1, source_target_pairs={{0,3},{1,0},{2,1},{3,2},{4,7},{5,4},{6,5},{7,6},{8,11},{9,8},{10,9... | collective-permute-start | bytes 786440 | tf_op jit(solution)/shard_map/ppermute | solution.py:571
  64.1 24.2 %collective-permute-start.10 = (bf16[1024,256]{1,0:T(8,128)(2,1)S(1)}, bf16[1024,256]{1,0:T(8,128)(2,1)S(1)}, u32[]{:S(2)}, u32[]{:S(2)}) collective-permute-start(bf16[1024,256]{1,0:T(8,128)(2,1)S(1)} %collective-permute-done.6.refs_0_), channel_id=1, source_target_pairs={{0,4},{4,0},{1,5},{5,1},{2,6},{6,2},{3,7},{7,3},{8,12},{12,8},{9,1... | collective-permute-start | bytes 1572872 | tf_op jit(solution)/shard_map/ppermute | solution.py:588
  66.7 0.8 copy-start.4
  83.4 2.6 %collective-permute-start.12 = (bf16[512,256]{1,0:T(8,128)(2,1)S(1)}, bf16[512,256]{1,0:T(8,128)(2,1)S(1)}, u32[]{:S(2)}, u32[]{:S(2)}) collective-permute-start(bf16[512,256]{1,0:T(8,128)(2,1)S(1)} %collective-permute-done.8.refs_2_), channel_id=1, source_target_pairs={{0,4},{4,0},{1,5},{5,1},{2,6},{6,2},{3,7},{7,3},{8,12},{12,8},{9,1... | collective-permute-start | bytes 786440 | tf_op jit(solution)/shard_map/ppermute | solution.py:588
  84.6 0.7 copy-start.8
  85.3 1.9 collective-permute-start.13
  85.3 0.7 copy-start.10
  86.0 0.7 copy-start.12
  86.7 20.6 %collective-permute-start.1 = (bf16[640,640]{1,0:T(8,128)(2,1)S(1)}, bf16[640,640]{1,0:T(8,128)(2,1)}, u32[]{:S(2)}, u32[]{:S(2)}) collective-permute-start(bf16[640,640]{1,0:T(8,128)(2,1)S(1)} %bitcast.28), channel_id=1, source_target_pairs={{0,1},{1,2},{2,3},{3,0},{4,5},{5,6},{6,7},{7,4},{8,9},{9,10},{10,1... | collective-permute-start | bytes 2457608 | tf_op jit(solution)/shard_map/ppermute | solution.py:571
  87.2 0.7 copy-start.14
  87.9 13.7 %collective-permute-start.11 = (bf16[1024,256]{1,0:T(8,128)(2,1)}, bf16[1024,256]{1,0:T(8,128)(2,1)}, u32[]{:S(2)}, u32[]{:S(2)}) collective-permute-start(bf16[1024,256]{1,0:T(8,128)(2,1)} %collective-permute-done.7.refs_1_), channel_id=1, source_target_pairs={{0,4},{4,0},{1,5},{5,1},{2,6},{6,2},{3,7},{7,3},{8,12},{12,8},{9,1... | collective-permute-start | bytes 1572872 | tf_op jit(solution)/shard_map/ppermute | solution.py:588
  88.2 0.8 copy-start.6
  89.0 32.5 %collective-permute-start.2 = (bf16[640,640]{1,0:T(8,128)(2,1)S(1)}, bf16[640,640]{1,0:T(8,128)(2,1)}, u32[]{:S(2)}, u32[]{:S(2)}) collective-permute-start(bf16[640,640]{1,0:T(8,128)(2,1)S(1)} %bitcast.32), channel_id=1, source_target_pairs={{0,3},{1,0},{2,1},{3,2},{4,7},{5,4},{6,5},{7,6},{8,11},{9,8},{10,9... | collective-permute-start | bytes 2457608 | tf_op jit(solution)/shard_map/ppermute | solution.py:571
  91.7 29.9 %copy-start.2 = (bf16[640,640]{1,0:T(8,128)(2,1)}, bf16[640,640]{1,0:T(8,128)(2,1)S(1)}, u32[]{:S(2)}) copy-start(bf16[640,640]{1,0:T(8,128)(2,1)S(1)} %collective-permute-done.refs_2_) | copy-start | bytes 2457604
  91.7 36.5 %collective-permute-start.4 = (bf16[640,640]{1,0:T(8,128)(2,1)S(1)}, bf16[640,640]{1,0:T(8,128)(2,1)}, u32[]{:S(2)}, u32[]{:S(2)}) collective-permute-start(bf16[640,640]{1,0:T(8,128)(2,1)S(1)} %collective-permute-done.refs_2_), channel_id=1, source_target_pairs={{0,1},{1,2},{2,3},{3,0},{4,5},{5,6},{6,7},{7,4},{8,9},{9,10},{10,1... | collective-permute-start | bytes 2457608 | tf_op jit(solution)/shard_map/ppermute | solution.py:571
  91.7 29.9 %copy-start.3 = (bf16[640,640]{1,0:T(8,128)(2,1)}, bf16[640,640]{1,0:T(8,128)(2,1)S(1)}, u32[]{:S(2)}) copy-start(bf16[640,640]{1,0:T(8,128)(2,1)S(1)} %collective-permute-done.3.refs_5_) | copy-start | bytes 2457604
  91.7 45.6 %collective-permute-start.5 = (bf16[640,640]{1,0:T(8,128)(2,1)S(1)}, bf16[640,640]{1,0:T(8,128)(2,1)}, u32[]{:S(2)}, u32[]{:S(2)}) collective-permute-start(bf16[640,640]{1,0:T(8,128)(2,1)S(1)} %collective-permute-done.3.refs_5_), channel_id=1, source_target_pairs={{0,3},{1,0},{2,1},{3,2},{4,7},{5,4},{6,5},{7,6},{8,11},{9,8},{10,9... | collective-permute-start | bytes 2457608 | tf_op jit(solution)/shard_map/ppermute | solution.py:571
  101.6 30.2 %collective-permute-start.14 = (bf16[640,256]{1,0:T(8,128)(2,1)S(1)}, bf16[640,256]{1,0:T(8,128)(2,1)S(1)}, u32[]{:S(2)}, u32[]{:S(2)}) collective-permute-start(bf16[640,256]{1,0:T(8,128)(2,1)S(1)} %get-tuple-element.71.refs_0_), channel_id=1, source_target_pairs={{0,1},{1,2},{2,3},{3,0},{4,5},{5,6},{6,7},{7,4},{8,9},{9,10},{10,1... | collective-permute-start | bytes 983048 | tf_op jit(solution)/shard_map/ppermute | solution.py:571
  107.4 26.5 %collective-permute-start.17 = (bf16[640,256]{1,0:T(8,128)(2,1)S(1)}, bf16[640,256]{1,0:T(8,128)(2,1)S(1)}, u32[]{:S(2)}, u32[]{:S(2)}) collective-permute-start(bf16[640,256]{1,0:T(8,128)(2,1)S(1)} %get-tuple-element.70.refs_1_), channel_id=1, source_target_pairs={{0,3},{1,0},{2,1},{3,2},{4,7},{5,4},{6,5},{7,6},{8,11},{9,8},{10,9... | collective-permute-start | bytes 983048 | tf_op jit(solution)/shard_map/ppermute | solution.py:571
  108.6 1.0 copy-start.5
  109.7 1.0 copy-start.7
  110.7 0.9 copy-start.9
  111.6 0.9 copy-start.11
  112.6 0.9 copy-start.13
  113.5 0.9 copy-start.15
  128.0 19.5 %collective-permute-start.15 = (bf16[640,256]{1,0:T(8,128)(2,1)S(1)}, bf16[640,256]{1,0:T(8,128)(2,1)S(1)}, u32[]{:S(2)}, u32[]{:S(2)}) collective-permute-start(bf16[640,256]{1,0:T(8,128)(2,1)S(1)} %get-tuple-element.70.refs_1_), channel_id=1, source_target_pairs={{0,1},{1,2},{2,3},{3,0},{4,5},{5,6},{6,7},{7,4},{8,9},{9,10},{10,1... | collective-permute-start | bytes 983048 | tf_op jit(solution)/shard_map/ppermute | solution.py:571
  128.2 19.3 %collective-permute-start.16 = (bf16[640,256]{1,0:T(8,128)(2,1)S(1)}, bf16[640,256]{1,0:T(8,128)(2,1)S(1)}, u32[]{:S(2)}, u32[]{:S(2)}) collective-permute-start(bf16[640,256]{1,0:T(8,128)(2,1)S(1)} %get-tuple-element.71.refs_0_), channel_id=1, source_target_pairs={{0,3},{1,0},{2,1},{3,2},{4,7},{5,4},{6,5},{7,6},{8,11},{9,8},{10,9... | collective-permute-start | bytes 983048 | tf_op jit(solution)/shard_map/ppermute | solution.py:571
  131.8 15.7 %collective-permute-start.18 = (bf16[640,256]{1,0:T(8,128)(2,1)S(1)}, bf16[640,256]{1,0:T(8,128)(2,1)S(1)}, u32[]{:S(2)}, u32[]{:S(2)}) collective-permute-start(bf16[640,256]{1,0:T(8,128)(2,1)S(1)} %collective-permute-done.14.refs_2_), channel_id=1, source_target_pairs={{0,1},{1,2},{2,3},{3,0},{4,5},{5,6},{6,7},{7,4},{8,9},{9,10},{10,1... | collective-permute-start | bytes 983048 | tf_op jit(solution)/shard_map/ppermute | solution.py:571
  133.9 14.0 %collective-permute-start.19 = (bf16[640,256]{1,0:T(8,128)(2,1)S(1)}, bf16[640,256]{1,0:T(8,128)(2,1)S(1)}, u32[]{:S(2)}, u32[]{:S(2)}) collective-permute-start(bf16[640,256]{1,0:T(8,128)(2,1)S(1)} %collective-permute-done.17.refs_5_), channel_id=1, source_target_pairs={{0,3},{1,0},{2,1},{3,2},{4,7},{5,4},{6,5},{7,6},{8,11},{9,8},{10,9... | collective-permute-start | bytes 983048 | tf_op jit(solution)/shard_map/ppermute | solution.py:571
  160.0 10.7 %collective-permute-start.20 = (bf16[4,16,64,256]{3,2,1,0:T(8,128)(2,1)}, bf16[4,16,64,256]{3,2,1,0:T(8,128)(2,1)}, u32[]{:S(2)}, u32[]{:S(2)}) collective-permute-start(bf16[4,16,64,256]{3,2,1,0:T(8,128)(2,1)} %slice_bitcast_fusion), channel_id=1, source_target_pairs={{0,4},{4,0},{1,5},{5,1},{2,6},{6,2},{3,7},{7,3},{8,12},{12,8},{9,1... | collective-permute-start | bytes 6291464 | tf_op jit(solution)/shard_map/ppermute | solution.py:659
  161.2 52.9 %all-to-all-start.3 = ((bf16[128,40,256]{2,1,0:T(8,128)(2,1)}), bf16[128,40,256]{2,1,0:T(8,128)(2,1)S(1)}, u32[]{:S(2)}, u32[]{:S(2)}) async-start(bf16[128,40,256]{2,1,0:T(8,128)(2,1)} %bitcast.37), calls=%async_computation.3 | async-start | bytes 5242880 | tf_op jit(solution)/shard_map/all_to_all | solution.py:649
  170.7 41.9 %copy-start.17 = (bf16[512,2048]{1,0:T(8,128)(2,1)S(1)}, bf16[512,2048]{1,0:T(8,128)(2,1)}, u32[]{:S(2)}) copy-start(bf16[512,2048]{1,0:T(8,128)(2,1)} %refs_1_.3) | copy-start | bytes 6291460
  170.7 41.9 %copy-start.22 = (bf16[2048,256]{1,0:T(8,128)(2,1)S(1)}, bf16[2048,256]{1,0:T(8,128)(2,1)}, u32[]{:S(2)}) copy-start(bf16[2048,256]{1,0:T(8,128)(2,1)} %whole_own.1) | copy-start | bytes 3145732
  174.4 32.7 %collective-permute-start.21 = (bf16[8,64,256]{2,1,0:T(8,128)(2,1)}, bf16[8,64,256]{2,1,0:T(8,128)(2,1)S(1)}, u32[]{:S(2)}, u32[]{:S(2)}) collective-permute-start(bf16[8,64,256]{2,1,0:T(8,128)(2,1)} %get-tuple-element.50), channel_id=1, source_target_pairs={{0,1},{1,2},{2,3},{3,0},{4,5},{5,6},{6,7},{7,4},{8,9},{9,10},{10,1... | collective-permute-start | bytes 786440 | tf_op jit(solution)/shard_map/ppermute | solution.py:571
  175.8 32.4 %collective-permute-start.23 = (bf16[8,64,256]{2,1,0:T(8,128)(2,1)}, bf16[8,64,256]{2,1,0:T(8,128)(2,1)S(1)}, u32[]{:S(2)}, u32[]{:S(2)}) collective-permute-start(bf16[8,64,256]{2,1,0:T(8,128)(2,1)} %get-tuple-element.52), channel_id=1, source_target_pairs={{0,3},{1,0},{2,1},{3,2},{4,7},{5,4},{6,5},{7,6},{8,11},{9,8},{10,9... | collective-permute-start | bytes 786440 | tf_op jit(solution)/shard_map/ppermute | solution.py:571
  177.1 50.7 %collective-permute-start.25 = (bf16[8,64,256]{2,1,0:T(8,128)(2,1)}, bf16[8,64,256]{2,1,0:T(8,128)(2,1)}, u32[]{:S(2)}, u32[]{:S(2)}) collective-permute-start(bf16[8,64,256]{2,1,0:T(8,128)(2,1)} %get-tuple-element.53), channel_id=1, source_target_pairs={{0,3},{1,0},{2,1},{3,2},{4,7},{5,4},{6,5},{7,6},{8,11},{9,8},{10,9... | collective-permute-start | bytes 786440 | tf_op jit(solution)/shard_map/ppermute | solution.py:571
  178.5 49.3 %collective-permute-start.26 = (bf16[8,64,256]{2,1,0:T(8,128)(2,1)}, bf16[8,64,256]{2,1,0:T(8,128)(2,1)}, u32[]{:S(2)}, u32[]{:S(2)}) collective-permute-start(bf16[8,64,256]{2,1,0:T(8,128)(2,1)} %get-tuple-element.54), channel_id=1, source_target_pairs={{0,1},{1,2},{2,3},{3,0},{4,5},{5,6},{6,7},{7,4},{8,9},{9,10},{10,1... | collective-permute-start | bytes 786440 | tf_op jit(solution)/shard_map/ppermute | solution.py:571
  208.1 19.7 %collective-permute-start.22 = (bf16[8,64,256]{2,1,0:T(8,128)(2,1)S(1)}, bf16[8,64,256]{2,1,0:T(8,128)(2,1)}, u32[]{:S(2)}, u32[]{:S(2)}) collective-permute-start(bf16[8,64,256]{2,1,0:T(8,128)(2,1)S(1)} %add_convert_fusion.2), channel_id=1, source_target_pairs={{0,1},{1,2},{2,3},{3,0},{4,5},{5,6},{6,7},{7,4},{8,9},{9,10},{10,1... | collective-permute-start | bytes 786440 | tf_op jit(solution)/shard_map/ppermute | solution.py:571
  209.9 17.9 %collective-permute-start.24 = (bf16[8,64,256]{2,1,0:T(8,128)(2,1)}, bf16[8,64,256]{2,1,0:T(8,128)(2,1)}, u32[]{:S(2)}, u32[]{:S(2)}) collective-permute-start(bf16[8,64,256]{2,1,0:T(8,128)(2,1)} %add_convert_fusion.1), channel_id=1, source_target_pairs={{0,3},{1,0},{2,1},{3,2},{4,7},{5,4},{6,5},{7,6},{8,11},{9,8},{10,9... | collective-permute-start | bytes 786440 | tf_op jit(solution)/shard_map/ppermute | solution.py:571
  214.1 13.7 %copy-start.19 = (bf16[16,64,256]{2,1,0:T(8,128)(2,1)S(1)}, bf16[16,64,256]{2,1,0:T(8,128)(2,1)}, u32[]{:S(2)}) copy-start(bf16[16,64,256]{2,1,0:T(8,128)(2,1)} %get-tuple-element.55) | copy-start | bytes 1572868
  218.7 16.4 %all-to-all-start.4 = ((f32[32,2,256]{2,1,0:T(2,128)}), f32[32,2,256]{2,1,0:T(2,128)S(1)}, u32[]{:S(2)}, u32[]{:S(2)}) async-start(f32[32,2,256]{2,1,0:T(2,128)} %get-tuple-element.63), calls=%async_computation.4 | async-start | bytes 131072 | tf_op jit(solution)/shard_map/all_to_all | solution.py:678
  235.1 18.4 %all-to-all-start.2 = ((bf16[16,64,256]{2,1,0:T(8,128)(2,1)}), bf16[16,64,256]{2,1,0:T(8,128)(2,1)S(1)}, u32[]{:S(2)}, u32[]{:S(2)}) async-start(bf16[16,64,256]{2,1,0:T(8,128)(2,1)} %add_convert_fusion), calls=%async_computation.2 | async-start | bytes 1048576 | tf_op jit(solution)/shard_map/all_to_all | solution.py:673

commit v5 on v4

--- a/solution.py
+++ b/solution.py
@@ -482,6 +482,46 @@
     )(*kept([parts]), other)
 
 
+def pair_sum_kernel(one, two, three, four, out_top, out_bottom):
+    out_top[...] = (one[...].astype(F32) + two[...].astype(F32)).astype(BF16)
+    out_bottom[...] = (three[...].astype(F32) + four[...].astype(F32)).astype(BF16)
+
+
+def pair_sum(*args):
+    out = made(args[0].shape, BF16)
+    return pl.pallas_call(
+        pair_sum_kernel,
+        out_shape=(out, out),
+        in_specs=[whole(a.shape) for a in args],
+        out_specs=[whole(out.shape)] * 2,
+        compiler_params=params(6),
+        cost_estimate=cost(10**6, 2**20),
+        name="pairsum",
+    )(*args)
+
+
+def arrive_kernel(own, last_top, last_bottom, from_right, from_left, out):
+    half = last_top.shape[0]
+    for at, far, near in ((0, last_top, from_right), (half, last_bottom, from_left)):
+        lines = slice(at, at + half)
+        out[lines] = (
+            own[lines].astype(F32) + far[...].astype(F32) + near[...].astype(F32)
+        ).astype(BF16)
+
+
+def arrive(*args):
+    out = made(args[0].shape, BF16)
+    return pl.pallas_call(
+        arrive_kernel,
+        out_shape=out,
+        in_specs=[whole(a.shape) for a in args],
+        out_specs=whole(out.shape),
+        compiler_params=params(6),
+        cost_estimate=cost(10**6, 2**20),
+        name="arrive",
+    )(*args)
+
+
 def scan_kernel(back, sel, base, act, b, decay, seg, block, out_grad, out_local, out_pair, drive, part):
     tokens, channels = base.shape
     length = tokens // 8
@@ -490,17 +530,21 @@
     mix = mix + dot(sel[...], total.astype(BF16))
     out_grad[...] = (mix * b[...]).astype(BF16)
     push = mix * act[...]
-    for h in range(channels // 128):
+    heads = channels // 128
+    for h in range(heads):
+        drive[h] = push[:, h * 128 : (h + 1) * 128]
+    last = pl.ds(length - 1, 8, stride=length)
+    values = [drive[h, last, :] for h in range(heads)]
+    for h in range(heads):
+        part[h, last, :] = values[h]
+    for i in range(length - 2, -1, -1):
+        here, after = pl.ds(i, 8, stride=length), pl.ds(i + 1, 8, stride=length)
+        for h in range(heads):
+            values[h] = drive[h, here, :] + decay[h, after, :] * values[h]
+            part[h, here, :] = values[h]
+    for h in range(heads):
         cols = slice(h * 128, (h + 1) * 128)
-        drive[h] = push[:, cols]
-        value = drive[h, pl.ds(length - 1, 8, stride=length), :]
-        part[h, pl.ds(length - 1, 8, stride=length), :] = value
-        for i in range(length - 2, -1, -1):
-            value = (
-                drive[h, pl.ds(i, 8, stride=length), :]
-                + decay[h, pl.ds(i + 1, 8, stride=length), :] * value
-            )
-            part[h, pl.ds(i, 8, stride=length), :] = value
+        value = values[h]
         lead = decay[h, pl.ds(0, 8, stride=length), :]
         inner = seg[h, pl.ds(0, 8, stride=length), :]
         carry = jnp.zeros((1, 128), F32)
@@ -662,14 +706,9 @@
     )
     through_top, through_bottom = shifted(far_top, 1), shifted(far_bottom, -1)
     from_left, from_right = shifted(right_bottom, 1), shifted(left_top, -1)
-    both_top = (right_top.astype(F32) + through_top.astype(F32)).astype(BF16)
-    both_bottom = (left_bottom.astype(F32) + through_bottom.astype(F32)).astype(BF16)
+    both_top, both_bottom = pair_sum(right_top, through_top, left_bottom, through_bottom)
     last_top, last_bottom = shifted(both_top, 1), shifted(both_bottom, -1)
-    arriving = (
-        jnp.concatenate([last_top, last_bottom], axis=0).astype(F32)
-        + jnp.concatenate([from_right, from_left], axis=0).astype(F32)
-        + own.astype(F32)
-    ).astype(BF16)
+    arriving = arrive(own, last_top, last_bottom, from_right, from_left)
     arrived = lax.all_to_all(arriving, "sq", 0, 0, tiled=True)
     grad_out_proj = arrived.astype(F32).sum(axis=0)
     gate_input_grad, local, pair = scanned(

time: 255 us -> 255 us (level)
  other arithmetic: 6.37 us -> 1.39 us
  Pallas kernels: 75.6 us -> 78.4 us
    convert_element_type x3 -> x0, other arithmetic: 4.98 us -> none  [the longest x1 2.25 us: per_device(): arriving = (jnp.concatenate([last_top, last_bottom], axis=0).astype(F32)...]
    pallas_call x0 -> x2, Pallas kernels: none -> 3 us  [the longest x1 2.13 us: arrive(): pl.pallas_call(arrive_kernel, out_shape=out, in_specs=[whole(a.shape) for...]
    unnamed x54 -> x58, local copies, waits for them, and re-layouts: 13.2 us -> 15.1 us
  transfers between devices with their start and end apart: 32 -> 32, of which waited for: 10 -> 10; matrix products, arithmetic and copies ran while one was open for 6% -> 4% of each run, Pallas kernels for 24% -> 26%
where the time goes in v5:
time: 255 us; the launch traced here: 254 us
  Pallas kernels  78.4 us (31%)
  waiting for transfers between devices  75.1 us (29%)
  starting transfers between devices  72.5 us (28%)
  local copies, waits for them, and re-layouts  22 us (9%)
  matrix products  3.76 us (1%)
    ppermute x22, waiting for transfers between devices, shifted(): return lax.ppermute(piece, 'tp', [(i, (i + by) % 4) for i in range(4)])  60.1 us
    ppermute x22, starting transfers between devices, shifted(): return lax.ppermute(piece, 'tp', [(i, (i + by) % 4) for i in range(4)])  29.6 us
    all_to_all x2, starting transfers between devices, exchanged(): lax.all_to_all(rows.reshape(sources, capacity, -1), sp_axes, 0, 0, tiled=...  15.5 us
    unnamed x58, local copies, waits for them, and re-layouts  15.1 us
    pallas_call x1, Pallas kernels, grads(): pl.pallas_call(functools.partial(grads_kernel, row_part=row_part, cot_par...  11.9 us
    pallas_call x2, Pallas kernels, build(): pl.pallas_call(functools.partial(build_kernel, capacity=capacity, group=g...  11.5 us
    pallas_call x1, Pallas kernels, expert(): pl.pallas_call(functools.partial(expert_kernel, row_part=row_part), out_s...  10.2 us
    all_to_all x2, waiting for transfers between devices, exchanged(): lax.all_to_all(rows.reshape(sources, capacity, -1), sp_axes, 0, 0, tiled=...  9.86 us
  transfers between devices with their start and end apart: 32, of which 10 were waited for; matrix products, arithmetic and copies ran while one was open for 4% of the time, Pallas kernels for 26%

profile of v5, /device:TPU:1, one launch (start us, length us, event | category | flops | bytes accessed | tf_op | source)
XLA Modules:
  0.0 254.1 jit_solution(11223266948228649334)
XLA Ops:
  0.7 4.7 %shard_map.191 = bf16[1280,640]{1,0:T(8,128)(2,1)} custom-call(s32[3]{0:T(128)S(1)} %pad_add_fusion.where_ref, s32[2,512]{1,0:T(2,128)} %bitcast.39, f32[2,512]{1,0:T(2,128)} %bitcast.41, bf16[512,2048]{1,0:T(8,128)(2,1)} %refs_0_.3, bf16[512,2048]{1,0:T(8,128)(2,1)} %refs_1_.3), custom_call_target="tpu_custom_call" | custom-call | flops 896000000 | bytes 3200000 | tf_op jit(solution)/shard_map/pallas_call | solution.py:196
  5.4 9.7 %all-to-all-start.1 = ((bf16[32,40,640]{2,1,0:T(8,128)(2,1)}), bf16[32,40,640]{2,1,0:T(8,128)(2,1)S(1)}, u32[]{:S(2)}, u32[]{:S(2)}) async-start(bf16[32,40,640]{2,1,0:T(8,128)(2,1)} %bitcast.35), calls=%async_computation.1 | async-start | bytes 3276800 | tf_op jit(solution)/shard_map/all_to_all | solution.py:655
  15.2 0.9 copy.22.ids
  16.0 0.9 copy.21
  17.5 8.4 %early.1 = (bf16[512,256]{1,0:T(8,128)(2,1)}, f32[512,256]{1,0:T(8,128)}, f32[512,256]{1,0:T(8,128)}, f32[512,256]{1,0:T(8,128)}, f32[512,256]{1,0:T(8,128)}, /*...) custom-call(s32[3]{0:T(128)S(1)} %pad_add_fusion.where_ref, ...), custom_call_target="tpu_custom_call" | custom-call | flops 3000000000 | bytes 8388608 | tf_op jit(solution)/shard_map/early/pallas_call | solution.py:142
  25.9 6.8 %shard_map.190 = bf16[1280,1792]{1,0:T(8,128)(2,1)} custom-call(s32[3]{0:T(128)S(1)} %pad_add_fusion.where_ref, s32[2,512]{1,0:T(2,128)} %bitcast.40, f32[2,512]{1,0:T(2,128)} %bitcast.42, bf16[512,2048]{1,0:T(8,128)(2,1)} %refs_0_.3, bf16[512,2048]{1,0:T(8,128)(2,1)} %refs_1_.3, bf16[512,256]{1,0:T(8,128)(2,1)} %get-tuple-element.40.refs_2_), custom_call_target="tpu_custom_call" | custom-call | flops 2508800000 | bytes 8960000 | tf_op jit(solution)/shard_map/pallas_call | solution.py:196
  32.7 6.1 %all-to-all-done.1 = bf16[32,40,640]{2,1,0:T(8,128)(2,1)S(1)} async-done(((bf16[32,40,640]{2,1,0:T(8,128)(2,1)}), bf16[32,40,640]{2,1,0:T(8,128)(2,1)S(1)}, u32[]{:S(2)}, u32[]{:S(2)}) %all-to-all-start.1) | async-done | bytes 1638432 | tf_op jit(solution)/shard_map/all_to_all | solution.py:655
  38.8 1.2 copy-done.21
  39.9 5.8 %all-to-all-start = ((bf16[32,40,1792]{2,1,0:T(8,128)(2,1)}), bf16[32,40,1792]{2,1,0:T(8,128)(2,1)}, u32[]{:S(2)}, u32[]{:S(2)}) async-start(bf16[32,40,1792]{2,1,0:T(8,128)(2,1)} %bitcast.36), calls=%async_computation | async-start | bytes 9175040 | tf_op jit(solution)/shard_map/all_to_all | solution.py:655
  45.8 1.3 collective-permute-start.6
  47.1 1.5 collective-permute-start.7
  48.6 1.5 fusion.3
  50.2 2.7 %collective-permute-start.3 = (bf16[640,640]{1,0:T(8,128)(2,1)S(1)}, bf16[640,640]{1,0:T(8,128)(2,1)S(1)}, u32[]{:S(2)}, u32[]{:S(2)}) collective-permute-start(bf16[640,640]{1,0:T(8,128)(2,1)S(1)} %bitcast.27), channel_id=1, source_target_pairs={{0,3},{1,0},{2,1},{3,2},{4,7},{5,4},{6,5},{7,6},{8,11},{9,8},{10,9... | collective-permute-start | bytes 2457608 | tf_op jit(solution)/shard_map/ppermute | solution.py:615
  52.9 7.4 %collective-permute-done.6.refs_0_ = bf16[1024,256]{1,0:T(8,128)(2,1)S(1)} collective-permute-done((bf16[1024,256]{1,0:T(8,128)(2,1)S(1)}, bf16[1024,256]{1,0:T(8,128)(2,1)S(1)}, u32[]{:S(2)}, u32[]{:S(2)}) %collective-permute-start.6) | collective-permute-done | bytes 524320 | tf_op jit(solution)/shard_map/ppermute | solution.py:615
  60.4 1.0 slice.39
  61.4 2.7 %collective-permute-start.9 = (bf16[512,256]{1,0:T(8,128)(2,1)S(1)}, bf16[512,256]{1,0:T(8,128)(2,1)S(1)}, u32[]{:S(2)}, u32[]{:S(2)}) collective-permute-start(bf16[512,256]{1,0:T(8,128)(2,1)S(1)} %slice.39), channel_id=1, source_target_pairs={{0,3},{1,0},{2,1},{3,2},{4,7},{5,4},{6,5},{7,6},{8,11},{9,8},{10,9... | collective-permute-start | bytes 786440 | tf_op jit(solution)/shard_map/ppermute | solution.py:615
  64.1 2.6 %collective-permute-start.10 = (bf16[1024,256]{1,0:T(8,128)(2,1)S(1)}, bf16[1024,256]{1,0:T(8,128)(2,1)S(1)}, u32[]{:S(2)}, u32[]{:S(2)}) collective-permute-start(bf16[1024,256]{1,0:T(8,128)(2,1)S(1)} %collective-permute-done.6.refs_0_), channel_id=1, source_target_pairs={{0,4},{4,0},{1,5},{5,1},{2,6},{6,2},{3,7},{7,3},{8,12},{12,8},{9,1... | collective-permute-start | bytes 1572872 | tf_op jit(solution)/shard_map/ppermute | solution.py:632
  66.7 0.8 copy-done.7
  67.5 16.0 %collective-permute-done.8.refs_2_ = bf16[512,256]{1,0:T(8,128)(2,1)S(1)} collective-permute-done((bf16[512,256]{1,0:T(8,128)(2,1)S(1)}, bf16[512,256]{1,0:T(8,128)(2,1)S(1)}, u32[]{:S(2)}, u32[]{:S(2)}) %collective-permute-start.8) | collective-permute-done | bytes 262176 | tf_op jit(solution)/shard_map/ppermute | solution.py:615
  83.4 1.2 collective-permute-start.12
  86.0 0.7 copy-done.15
  88.3 0.8 copy-done.9
  89.1 2.7 %collective-permute-start.2 = (bf16[640,640]{1,0:T(8,128)(2,1)S(1)}, bf16[640,640]{1,0:T(8,128)(2,1)}, u32[]{:S(2)}, u32[]{:S(2)}) collective-permute-start(bf16[640,640]{1,0:T(8,128)(2,1)S(1)} %bitcast.32), channel_id=1, source_target_pairs={{0,3},{1,0},{2,1},{3,2},{4,7},{5,4},{6,5},{7,6},{8,11},{9,8},{10,9... | collective-permute-start | bytes 2457608 | tf_op jit(solution)/shard_map/ppermute | solution.py:615
  91.8 2.7 %collective-permute-start.5 = (bf16[640,640]{1,0:T(8,128)(2,1)S(1)}, bf16[640,640]{1,0:T(8,128)(2,1)}, u32[]{:S(2)}, u32[]{:S(2)}) collective-permute-start(bf16[640,640]{1,0:T(8,128)(2,1)S(1)} %collective-permute-done.3.refs_5_), channel_id=1, source_target_pairs={{0,3},{1,0},{2,1},{3,2},{4,7},{5,4},{6,5},{7,6},{8,11},{9,8},{10,9... | collective-permute-start | bytes 2457608 | tf_op jit(solution)/shard_map/ppermute | solution.py:615
  94.4 2.3 convolution_bitcast_fusion.local
  96.7 3.8 %all-to-all-done = bf16[32,40,1792]{2,1,0:T(8,128)(2,1)} async-done(((bf16[32,40,1792]{2,1,0:T(8,128)(2,1)}), bf16[32,40,1792]{2,1,0:T(8,128)(2,1)}, u32[]{:S(2)}, u32[]{:S(2)}) %all-to-all-start) | async-done | bytes 4587552 | tf_op jit(solution)/shard_map/all_to_all | solution.py:655
  100.5 1.1 fusion.2
  101.6 1.3 collective-permute-start.14
  102.9 4.5 %collective-permute-done.1.refs_3_ = bf16[640,640]{1,0:T(8,128)(2,1)} collective-permute-done((bf16[640,640]{1,0:T(8,128)(2,1)S(1)}, bf16[640,640]{1,0:T(8,128)(2,1)}, u32[]{:S(2)}, u32[]{:S(2)}) %collective-permute-start.1) | collective-permute-done | bytes 819232 | tf_op jit(solution)/shard_map/ppermute | solution.py:615
  107.4 1.3 collective-permute-start.17
  108.6 1.0 copy-done.8
  109.7 1.0 copy-done.10
  110.7 0.9 copy-done.12
  111.7 0.9 copy-done.14
  112.6 0.9 copy-done.16
  113.6 0.9 copy-done.18
  114.5 7.1 %folded.1 = (bf16[2048,512]{1,0:T(8,128)(2,1)}, bf16[2048,256]{1,0:T(8,128)(2,1)}, bf16[4,256,256]{2,1,0:T(8,128)(2,1)}, bf16[4,256,256]{2,1,0:T(8,128)(2,1)}) custom-call(s32[3]{0:T(128)S(1)} %pad_add_fusion.where_ref, bf16[2048,256]{1,0:T(8,128)(2,1)} %bitcast.44, bf16[2048,256]{1,0:T(8,128)(2,1)} %bitcast.46, bf16[256,2048]{1,0:T(8,128)(2,1)} %bitcast.43, ...), custom_call_target="tpu_custom_call" | custom-call | flops 4000000000 | bytes 7340032 | tf_op jit(solution)/shard_map/folded/pallas_call | solution.py:262
  121.6 6.4 %ahead.1.before = f32[1280,768]{1,0:T(8,128)} custom-call(bf16[2048,512]{1,0:T(8,128)(2,1)} %get-tuple-element.41.gate_up, bf16[2048,256]{1,0:T(8,128)(2,1)} %get-tuple-element.42.down, bf16[640,640]{1,0:T(8,128)(2,1)S(1)} %bitcast.33, bf16[640,640]{1,0:T(8,128)(2,1)S(1)} %bitcast.29, bf16[640,640]{1,0:T(8,128)(2,1)S(1)} %collective-permute-done.refs_2_, ...), custom_call_target="tpu_custom_call" | custom-call | flops 2000000000 | bytes 12582912 | tf_op jit(solution)/shard_map/ahead/pallas_call | solution.py:289
  128.2 2.5 collective-permute-start.16
  130.7 1.2 collective-permute-done.14.refs_2_
  131.8 2.1 collective-permute-done.17.refs_5_
  133.9 3.4 %collective-permute-start.19 = (bf16[640,256]{1,0:T(8,128)(2,1)S(1)}, bf16[640,256]{1,0:T(8,128)(2,1)S(1)}, u32[]{:S(2)}, u32[]{:S(2)}) collective-permute-start(bf16[640,256]{1,0:T(8,128)(2,1)S(1)} %collective-permute-done.17.refs_5_), channel_id=1, source_target_pairs={{0,3},{1,0},{2,1},{3,2},{4,7},{5,4},{6,5},{7,6},{8,11},{9,8},{10,9... | collective-permute-start | bytes 983048 | tf_op jit(solution)/shard_map/ppermute | solution.py:615
  137.3 10.2 %expert.1 = (bf16[1280,256]{1,0:T(8,128)(2,1)}, bf16[1280,256]{1,0:T(8,128)(2,1)}, bf16[1280,256]{1,0:T(8,128)(2,1)}, bf16[4,1280,256]{2,1,0:T(8,128)(2,1)}) custom-call(bf16[1280,1792]{1,0:T(8,128)(2,1)} %bitcast.8.got_rows.got_cot, bf16[1280,1792]{1,0:T(8,128)(2,1)} %bitcast.8.got_rows.got_cot, bf16[640,640]{1,0:T(8,128)(2,1)} %collective-permute-done.4.far_top.refs_6_, ...), custom_call_target="tpu_custom_call" | custom-call | flops 5000000000 | bytes 16777216 | tf_op jit(solution)/shard_map/expert/pallas_call | solution.py:343
  147.9 8.9 %proj.1.kept_ref = bf16[2,4,16,64,256]{4,3,2,1,0:T(8,128)(2,1)} custom-call(s32[3]{0:T(128)S(1)} %pad_add_fusion.where_ref, bf16[1280,256]{1,0:T(8,128)(2,1)} %get-tuple-element.46.refs_9_.gate_cot, bf16[1280,256]{1,0:T(8,128)(2,1)} %get-tuple-element.47.refs_10_.up_cot, bf16[2048,256]{1,0:T(8,128)(2,1)} %bitcast.45, bf16[2048,256]{1,0:T(8,128)(2,1)} %bitcast.47, ...), custom_call_target="tpu_custom_call" | custom-call | flops 4000000000 | bytes 14680064 | tf_op jit(solution)/shard_map/proj/pallas_call | solution.py:442
  156.9 3.2 %slice_bitcast_fusion = bf16[4,16,64,256]{3,2,1,0:T(8,128)(2,1)} fusion(bf16[2,4,16,64,256]{4,3,2,1,0:T(8,128)(2,1)} %proj.1.kept_ref), kind=kLoop, calls=%fused_computation.1 | loop fusion | bytes 4194304 | tf_op jit(solution)/shard_map/squeeze | solution.py:703
  160.0 1.2 collective-permute-start.20
  161.2 9.5 %all-to-all-start.3 = ((bf16[128,40,256]{2,1,0:T(8,128)(2,1)}), bf16[128,40,256]{2,1,0:T(8,128)(2,1)S(1)}, u32[]{:S(2)}, u32[]{:S(2)}) async-start(bf16[128,40,256]{2,1,0:T(8,128)(2,1)} %bitcast.37), calls=%async_computation.3 | async-start | bytes 5242880 | tf_op jit(solution)/shard_map/all_to_all | solution.py:693
  170.7 3.7 %chipsum.1 = (bf16[16,64,256]{2,1,0:T(8,128)(2,1)}, bf16[8,64,256]{2,1,0:T(8,128)(2,1)}, bf16[8,64,256]{2,1,0:T(8,128)(2,1)}, bf16[8,64,256]{2,1,0:T(8,128)(2,1)...) custom-call(bf16[2,4,16,64,256]{4,3,2,1,0:T(8,128)(2,1)} %proj.1.kept_ref, ...), custom_call_target="tpu_custom_call" | custom-call | flops 10000000 | bytes 6291456 | tf_op jit(solution)/shard_map/chipsum/pallas_call | solution.py:468
  174.5 1.4 collective-permute-start.21
  175.8 1.3 collective-permute-start.22
  177.1 1.4 collective-permute-start.25
  178.6 28.5 %collective-permute-done.21.two = bf16[8,64,256]{2,1,0:T(8,128)(2,1)S(1)} collective-permute-done((bf16[8,64,256]{2,1,0:T(8,128)(2,1)}, bf16[8,64,256]{2,1,0:T(8,128)(2,1)S(1)}, u32[]{:S(2)}, u32[]{:S(2)}) %collective-permute-start.21) | collective-permute-done | bytes 262176 | tf_op jit(solution)/shard_map/ppermute | solution.py:615
  207.1 0.9 copy-done.5
  208.1 0.9 copy-done.6
  209.0 0.9 pairsum.1
  209.9 2.7 %collective-permute-start.24 = (bf16[8,64,256]{2,1,0:T(8,128)(2,1)}, bf16[8,64,256]{2,1,0:T(8,128)(2,1)}, u32[]{:S(2)}, u32[]{:S(2)}) collective-permute-start(bf16[8,64,256]{2,1,0:T(8,128)(2,1)} %get-tuple-element.57), channel_id=1, source_target_pairs={{0,3},{1,0},{2,1},{3,2},{4,7},{5,4},{6,5},{7,6},{8,11},{9,8},{10,9... | collective-permute-start | bytes 786440 | tf_op jit(solution)/shard_map/ppermute | solution.py:615
  212.6 1.5 fusion.4.base
  214.1 4.5 %scanned.1 = (bf16[512,256]{1,0:T(8,128)(2,1)}, f32[512,256]{1,0:T(8,128)}, f32[32,2,256]{2,1,0:T(2,128)}) custom-call(bf16[4,1280,256]{2,1,0:T(8,128)(2,1)S(1)} %bitcast.26, bf16[512,1280]{1,0:T(8,128)(2,1)} %get-tuple-element.61.sel, f32[512,256]{1,0:T(8,128)} %fusion.4.base, f32[512,256]{1,0:T(8,128)} %get-tuple-element.62.act, ...), custom_call_target="tpu_custom_call" | custom-call | flops 400000000 | bytes 8388608 | tf_op jit(solution)/shard_map/scanned/pallas_call | solution.py:568
  218.6 9.1 %all-to-all-start.4 = ((f32[32,2,256]{2,1,0:T(2,128)}), f32[32,2,256]{2,1,0:T(2,128)S(1)}, u32[]{:S(2)}, u32[]{:S(2)}) async-start(f32[32,2,256]{2,1,0:T(2,128)} %get-tuple-element.67), calls=%async_computation.4 | async-start | bytes 131072 | tf_op jit(solution)/shard_map/all_to_all | solution.py:717
  227.8 2.1 arrive.1
  229.9 5.1 %all-to-all-done.4.pairs = f32[32,2,256]{2,1,0:T(2,128)S(1)} async-done(((f32[32,2,256]{2,1,0:T(2,128)}), f32[32,2,256]{2,1,0:T(2,128)S(1)}, u32[]{:S(2)}, u32[]{:S(2)}) %all-to-all-start.4) | async-done | bytes 65568 | tf_op jit(solution)/shard_map/all_to_all | solution.py:717
  235.1 3.6 %all-to-all-start.2 = ((bf16[16,64,256]{2,1,0:T(8,128)(2,1)}), bf16[16,64,256]{2,1,0:T(8,128)(2,1)S(1)}, u32[]{:S(2)}, u32[]{:S(2)}) async-start(bf16[16,64,256]{2,1,0:T(8,128)(2,1)} %arrive.1), calls=%async_computation.2 | async-start | bytes 1048576 | tf_op jit(solution)/shard_map/all_to_all | solution.py:712
  238.7 11.9 %grads.1 = (f32[1,2048,256]{2,1,0:T(8,128)}, f32[1,2048,256]{2,1,0:T(8,128)}, f32[1,256,2048]{2,1,0:T(8,128)}) custom-call(s32[3]{0:T(128)S(1)} %pad_add_fusion.where_ref, bf16[1280,1792]{1,0:T(8,128)(2,1)} %bitcast.8.got_rows.got_cot, bf16[1280,1792]{1,0:T(8,128)(2,1)} %bitcast.8.got_rows.got_cot, bf16[640,640]{1,0:T(8,128)(2,1)} %bitcast.34, ...), custom_call_target="tpu_custom_call" | custom-call | flops 4000000000 | bytes 17825792 | tf_op jit(solution)/shard_map/grads/pallas_call | solution.py:398
  250.5 2.9 %final.1 = bf16[512,256]{1,0:T(8,128)(2,1)} custom-call(s32[3]{0:T(128)S(1)} %pad_add_fusion.where_ref, f32[32,2,256]{2,1,0:T(2,128)S(1)} %all-to-all-done.4.pairs, f32[512,256]{1,0:T(8,128)} %get-tuple-element.68.local, f32[512,256]{1,0:T(8,128)} %get-tuple-element.69.exp, f32[512,256]{1,0:T(8,128)} %get-tuple-element.70.ca, ...), custom_call_target="tpu_custom_call" | custom-call | flops 100000000 | bytes 4194304 | tf_op jit(solution)/shard_map/final/pallas_call | solution.py:603
  (82 shorter events, 5.4 us)
Async XLA Ops:
  5.4 9.8 %copy-start.25 = (s32[512,2]{0,1:T(2,128)S(1)}, s32[512,2]{0,1:T(2,128)}, u32[]{:S(2)}) copy-start(s32[512,2]{0,1:T(2,128)} %param.17) | copy-start | bytes 12292
  5.4 10.6 %copy-start.26 = (f32[2,512]{1,0:T(2,128)S(1)}, f32[2,512]{1,0:T(2,128)}, u32[]{:S(2)}) copy-start(f32[2,512]{1,0:T(2,128)} %param.27) | copy-start | bytes 12292
  5.4 11.5 %copy-start.27 = (f32[1024]{0:T(1024)S(1)}, f32[1024]{0:T(1024)}, u32[]{:S(2)}) copy-start(f32[1024]{0:T(1024)} %param.26) | copy-start | bytes 12292
  5.4 33.3 %all-to-all-start.1 = ((bf16[32,40,640]{2,1,0:T(8,128)(2,1)}), bf16[32,40,640]{2,1,0:T(8,128)(2,1)S(1)}, u32[]{:S(2)}, u32[]{:S(2)}) async-start(bf16[32,40,640]{2,1,0:T(8,128)(2,1)} %bitcast.35), calls=%async_computation.1 | async-start | bytes 3276800 | tf_op jit(solution)/shard_map/all_to_all | solution.py:655
  38.8 1.2 copy-start.21
  38.8 7.0 %copy-start.23 = (bf16[2048,256]{1,0:T(8,128)(2,1)S(1)}, bf16[2048,256]{1,0:T(8,128)(2,1)}, u32[]{:S(2)}) copy-start(bf16[2048,256]{1,0:T(8,128)(2,1)} %whole_own.1) | copy-start | bytes 3145732
  39.9 60.6 %all-to-all-start = ((bf16[32,40,1792]{2,1,0:T(8,128)(2,1)}), bf16[32,40,1792]{2,1,0:T(8,128)(2,1)}, u32[]{:S(2)}, u32[]{:S(2)}) async-start(bf16[32,40,1792]{2,1,0:T(8,128)(2,1)} %bitcast.36), calls=%async_computation | async-start | bytes 9175040 | tf_op jit(solution)/shard_map/all_to_all | solution.py:655
  45.8 48.6 %copy-start.19 = (bf16[512,2048]{1,0:T(8,128)(2,1)S(1)}, bf16[512,2048]{1,0:T(8,128)(2,1)}, u32[]{:S(2)}) copy-start(bf16[512,2048]{1,0:T(8,128)(2,1)} %refs_1_.3) | copy-start | bytes 6291460
  45.8 48.6 %copy-start.22 = (bf16[512,256]{1,0:T(8,128)(2,1)S(1)}, bf16[512,256]{1,0:T(8,128)(2,1)}, u32[]{:S(2)}) copy-start(bf16[512,256]{1,0:T(8,128)(2,1)} %get-tuple-element.40.refs_2_) | copy-start | bytes 786436
  45.8 14.5 %collective-permute-start.6 = (bf16[1024,256]{1,0:T(8,128)(2,1)S(1)}, bf16[1024,256]{1,0:T(8,128)(2,1)S(1)}, u32[]{:S(2)}, u32[]{:S(2)}) collective-permute-start(bf16[1024,256]{1,0:T(8,128)(2,1)S(1)} %constant_dynamic-slice_fusion), channel_id=1, source_target_pairs={{0,1},{1,2},{2,3},{3,0},{4,5},{5,6},{6,7},{7,4},{8,9},{9,10},{10,1... | collective-permute-start | bytes 1572872 | tf_op jit(solution)/shard_map/ppermute | solution.py:615
  47.1 13.3 %collective-permute-start.7 = (bf16[1024,256]{1,0:T(8,128)(2,1)S(1)}, bf16[1024,256]{1,0:T(8,128)(2,1)}, u32[]{:S(2)}, u32[]{:S(2)}) collective-permute-start(bf16[1024,256]{1,0:T(8,128)(2,1)S(1)} %constant_dynamic-slice_fusion), channel_id=1, source_target_pairs={{0,3},{1,0},{2,1},{3,2},{4,7},{5,4},{6,5},{7,6},{8,11},{9,8},{10,9... | collective-permute-start | bytes 1572872 | tf_op jit(solution)/shard_map/ppermute | solution.py:615
  50.1 71.5 %copy-start = (bf16[16,40,640]{2,1,0:T(8,128)(2,1)}, bf16[16,40,640]{2,1,0:T(8,128)(2,1)S(1)}, u32[]{:S(2)}) copy-start(bf16[16,40,640]{2,1,0:T(8,128)(2,1)S(1)} %get-tuple-element.76) | copy-start | bytes 2457604
  50.1 71.5 %copy-start.1 = (bf16[16,40,640]{2,1,0:T(8,128)(2,1)}, bf16[16,40,640]{2,1,0:T(8,128)(2,1)S(1)}, u32[]{:S(2)}) copy-start(bf16[16,40,640]{2,1,0:T(8,128)(2,1)S(1)} %get-tuple-element.77) | copy-start | bytes 2457604
  50.1 41.6 %collective-permute-start = (bf16[640,640]{1,0:T(8,128)(2,1)S(1)}, bf16[640,640]{1,0:T(8,128)(2,1)S(1)}, u32[]{:S(2)}, u32[]{:S(2)}) collective-permute-start(bf16[640,640]{1,0:T(8,128)(2,1)S(1)} %bitcast.31), channel_id=1, source_target_pairs={{0,1},{1,2},{2,3},{3,0},{4,5},{5,6},{6,7},{7,4},{8,9},{9,10},{10,1... | collective-permute-start | bytes 2457608 | tf_op jit(solution)/shard_map/ppermute | solution.py:615
  50.2 41.5 %collective-permute-start.3 = (bf16[640,640]{1,0:T(8,128)(2,1)S(1)}, bf16[640,640]{1,0:T(8,128)(2,1)S(1)}, u32[]{:S(2)}, u32[]{:S(2)}) collective-permute-start(bf16[640,640]{1,0:T(8,128)(2,1)S(1)} %bitcast.27), channel_id=1, source_target_pairs={{0,3},{1,0},{2,1},{3,2},{4,7},{5,4},{6,5},{7,6},{8,11},{9,8},{10,9... | collective-permute-start | bytes 2457608 | tf_op jit(solution)/shard_map/ppermute | solution.py:615
  60.3 23.2 %collective-permute-start.8 = (bf16[512,256]{1,0:T(8,128)(2,1)S(1)}, bf16[512,256]{1,0:T(8,128)(2,1)S(1)}, u32[]{:S(2)}, u32[]{:S(2)}) collective-permute-start(bf16[512,256]{1,0:T(8,128)(2,1)S(1)} %slice.38), channel_id=1, source_target_pairs={{0,1},{1,2},{2,3},{3,0},{4,5},{5,6},{6,7},{7,4},{8,9},{9,10},{10,1... | collective-permute-start | bytes 786440 | tf_op jit(solution)/shard_map/ppermute | solution.py:615
  61.4 24.0 %collective-permute-start.9 = (bf16[512,256]{1,0:T(8,128)(2,1)S(1)}, bf16[512,256]{1,0:T(8,128)(2,1)S(1)}, u32[]{:S(2)}, u32[]{:S(2)}) collective-permute-start(bf16[512,256]{1,0:T(8,128)(2,1)S(1)} %slice.39), channel_id=1, source_target_pairs={{0,3},{1,0},{2,1},{3,2},{4,7},{5,4},{6,5},{7,6},{8,11},{9,8},{10,9... | collective-permute-start | bytes 786440 | tf_op jit(solution)/shard_map/ppermute | solution.py:615
  64.1 24.2 %collective-permute-start.10 = (bf16[1024,256]{1,0:T(8,128)(2,1)S(1)}, bf16[1024,256]{1,0:T(8,128)(2,1)S(1)}, u32[]{:S(2)}, u32[]{:S(2)}) collective-permute-start(bf16[1024,256]{1,0:T(8,128)(2,1)S(1)} %collective-permute-done.6.refs_0_), channel_id=1, source_target_pairs={{0,4},{4,0},{1,5},{5,1},{2,6},{6,2},{3,7},{7,3},{8,12},{12,8},{9,1... | collective-permute-start | bytes 1572872 | tf_op jit(solution)/shard_map/ppermute | solution.py:632
  66.7 0.8 copy-start.7
  83.4 2.6 %collective-permute-start.12 = (bf16[512,256]{1,0:T(8,128)(2,1)S(1)}, bf16[512,256]{1,0:T(8,128)(2,1)S(1)}, u32[]{:S(2)}, u32[]{:S(2)}) collective-permute-start(bf16[512,256]{1,0:T(8,128)(2,1)S(1)} %collective-permute-done.8.refs_2_), channel_id=1, source_target_pairs={{0,4},{4,0},{1,5},{5,1},{2,6},{6,2},{3,7},{7,3},{8,12},{12,8},{9,1... | collective-permute-start | bytes 786440 | tf_op jit(solution)/shard_map/ppermute | solution.py:632
  84.6 0.7 copy-start.11
  85.3 1.9 collective-permute-start.13
  85.3 0.7 copy-start.13
  86.0 0.7 copy-start.15
  86.8 20.6 %collective-permute-start.1 = (bf16[640,640]{1,0:T(8,128)(2,1)S(1)}, bf16[640,640]{1,0:T(8,128)(2,1)}, u32[]{:S(2)}, u32[]{:S(2)}) collective-permute-start(bf16[640,640]{1,0:T(8,128)(2,1)S(1)} %bitcast.28), channel_id=1, source_target_pairs={{0,1},{1,2},{2,3},{3,0},{4,5},{5,6},{6,7},{7,4},{8,9},{9,10},{10,1... | collective-permute-start | bytes 2457608 | tf_op jit(solution)/shard_map/ppermute | solution.py:615
  87.3 0.7 copy-start.17
  88.0 13.6 %collective-permute-start.11 = (bf16[1024,256]{1,0:T(8,128)(2,1)}, bf16[1024,256]{1,0:T(8,128)(2,1)}, u32[]{:S(2)}, u32[]{:S(2)}) collective-permute-start(bf16[1024,256]{1,0:T(8,128)(2,1)} %collective-permute-done.7.refs_1_), channel_id=1, source_target_pairs={{0,4},{4,0},{1,5},{5,1},{2,6},{6,2},{3,7},{7,3},{8,12},{12,8},{9,1... | collective-permute-start | bytes 1572872 | tf_op jit(solution)/shard_map/ppermute | solution.py:632
  88.3 0.8 copy-start.9
  89.1 32.5 %collective-permute-start.2 = (bf16[640,640]{1,0:T(8,128)(2,1)S(1)}, bf16[640,640]{1,0:T(8,128)(2,1)}, u32[]{:S(2)}, u32[]{:S(2)}) collective-permute-start(bf16[640,640]{1,0:T(8,128)(2,1)S(1)} %bitcast.32), channel_id=1, source_target_pairs={{0,3},{1,0},{2,1},{3,2},{4,7},{5,4},{6,5},{7,6},{8,11},{9,8},{10,9... | collective-permute-start | bytes 2457608 | tf_op jit(solution)/shard_map/ppermute | solution.py:615
  91.7 29.9 %copy-start.2 = (bf16[640,640]{1,0:T(8,128)(2,1)}, bf16[640,640]{1,0:T(8,128)(2,1)S(1)}, u32[]{:S(2)}) copy-start(bf16[640,640]{1,0:T(8,128)(2,1)S(1)} %collective-permute-done.refs_2_) | copy-start | bytes 2457604
  91.7 36.5 %collective-permute-start.4 = (bf16[640,640]{1,0:T(8,128)(2,1)S(1)}, bf16[640,640]{1,0:T(8,128)(2,1)}, u32[]{:S(2)}, u32[]{:S(2)}) collective-permute-start(bf16[640,640]{1,0:T(8,128)(2,1)S(1)} %collective-permute-done.refs_2_), channel_id=1, source_target_pairs={{0,1},{1,2},{2,3},{3,0},{4,5},{5,6},{6,7},{7,4},{8,9},{9,10},{10,1... | collective-permute-start | bytes 2457608 | tf_op jit(solution)/shard_map/ppermute | solution.py:615
  91.8 29.9 %copy-start.3 = (bf16[640,640]{1,0:T(8,128)(2,1)}, bf16[640,640]{1,0:T(8,128)(2,1)S(1)}, u32[]{:S(2)}) copy-start(bf16[640,640]{1,0:T(8,128)(2,1)S(1)} %collective-permute-done.3.refs_5_) | copy-start | bytes 2457604
  91.8 45.6 %collective-permute-start.5 = (bf16[640,640]{1,0:T(8,128)(2,1)S(1)}, bf16[640,640]{1,0:T(8,128)(2,1)}, u32[]{:S(2)}, u32[]{:S(2)}) collective-permute-start(bf16[640,640]{1,0:T(8,128)(2,1)S(1)} %collective-permute-done.3.refs_5_), channel_id=1, source_target_pairs={{0,3},{1,0},{2,1},{3,2},{4,7},{5,4},{6,5},{7,6},{8,11},{9,8},{10,9... | collective-permute-start | bytes 2457608 | tf_op jit(solution)/shard_map/ppermute | solution.py:615
  101.6 30.2 %collective-permute-start.14 = (bf16[640,256]{1,0:T(8,128)(2,1)S(1)}, bf16[640,256]{1,0:T(8,128)(2,1)S(1)}, u32[]{:S(2)}, u32[]{:S(2)}) collective-permute-start(bf16[640,256]{1,0:T(8,128)(2,1)S(1)} %get-tuple-element.75.refs_0_), channel_id=1, source_target_pairs={{0,1},{1,2},{2,3},{3,0},{4,5},{5,6},{6,7},{7,4},{8,9},{9,10},{10,1... | collective-permute-start | bytes 983048 | tf_op jit(solution)/shard_map/ppermute | solution.py:615
  107.4 26.5 %collective-permute-start.17 = (bf16[640,256]{1,0:T(8,128)(2,1)S(1)}, bf16[640,256]{1,0:T(8,128)(2,1)S(1)}, u32[]{:S(2)}, u32[]{:S(2)}) collective-permute-start(bf16[640,256]{1,0:T(8,128)(2,1)S(1)} %get-tuple-element.74.refs_1_), channel_id=1, source_target_pairs={{0,3},{1,0},{2,1},{3,2},{4,7},{5,4},{6,5},{7,6},{8,11},{9,8},{10,9... | collective-permute-start | bytes 983048 | tf_op jit(solution)/shard_map/ppermute | solution.py:615
  108.6 1.0 copy-start.8
  109.7 1.0 copy-start.10
  110.7 0.9 copy-start.12
  111.7 0.9 copy-start.14
  112.6 0.9 copy-start.16
  113.6 0.9 copy-start.18
  128.0 19.5 %collective-permute-start.15 = (bf16[640,256]{1,0:T(8,128)(2,1)S(1)}, bf16[640,256]{1,0:T(8,128)(2,1)S(1)}, u32[]{:S(2)}, u32[]{:S(2)}) collective-permute-start(bf16[640,256]{1,0:T(8,128)(2,1)S(1)} %get-tuple-element.74.refs_1_), channel_id=1, source_target_pairs={{0,1},{1,2},{2,3},{3,0},{4,5},{5,6},{6,7},{7,4},{8,9},{9,10},{10,1... | collective-permute-start | bytes 983048 | tf_op jit(solution)/shard_map/ppermute | solution.py:615
  128.2 19.3 %collective-permute-start.16 = (bf16[640,256]{1,0:T(8,128)(2,1)S(1)}, bf16[640,256]{1,0:T(8,128)(2,1)S(1)}, u32[]{:S(2)}, u32[]{:S(2)}) collective-permute-start(bf16[640,256]{1,0:T(8,128)(2,1)S(1)} %get-tuple-element.75.refs_0_), channel_id=1, source_target_pairs={{0,3},{1,0},{2,1},{3,2},{4,7},{5,4},{6,5},{7,6},{8,11},{9,8},{10,9... | collective-permute-start | bytes 983048 | tf_op jit(solution)/shard_map/ppermute | solution.py:615
  131.8 15.7 %collective-permute-start.18 = (bf16[640,256]{1,0:T(8,128)(2,1)S(1)}, bf16[640,256]{1,0:T(8,128)(2,1)S(1)}, u32[]{:S(2)}, u32[]{:S(2)}) collective-permute-start(bf16[640,256]{1,0:T(8,128)(2,1)S(1)} %collective-permute-done.14.refs_2_), channel_id=1, source_target_pairs={{0,1},{1,2},{2,3},{3,0},{4,5},{5,6},{6,7},{7,4},{8,9},{9,10},{10,1... | collective-permute-start | bytes 983048 | tf_op jit(solution)/shard_map/ppermute | solution.py:615
  133.9 14.0 %collective-permute-start.19 = (bf16[640,256]{1,0:T(8,128)(2,1)S(1)}, bf16[640,256]{1,0:T(8,128)(2,1)S(1)}, u32[]{:S(2)}, u32[]{:S(2)}) collective-permute-start(bf16[640,256]{1,0:T(8,128)(2,1)S(1)} %collective-permute-done.17.refs_5_), channel_id=1, source_target_pairs={{0,3},{1,0},{2,1},{3,2},{4,7},{5,4},{6,5},{7,6},{8,11},{9,8},{10,9... | collective-permute-start | bytes 983048 | tf_op jit(solution)/shard_map/ppermute | solution.py:615
  160.0 10.7 %collective-permute-start.20 = (bf16[4,16,64,256]{3,2,1,0:T(8,128)(2,1)}, bf16[4,16,64,256]{3,2,1,0:T(8,128)(2,1)}, u32[]{:S(2)}, u32[]{:S(2)}) collective-permute-start(bf16[4,16,64,256]{3,2,1,0:T(8,128)(2,1)} %slice_bitcast_fusion), channel_id=1, source_target_pairs={{0,4},{4,0},{1,5},{5,1},{2,6},{6,2},{3,7},{7,3},{8,12},{12,8},{9,1... | collective-permute-start | bytes 6291464 | tf_op jit(solution)/shard_map/ppermute | solution.py:703
  161.2 52.9 %all-to-all-start.3 = ((bf16[128,40,256]{2,1,0:T(8,128)(2,1)}), bf16[128,40,256]{2,1,0:T(8,128)(2,1)S(1)}, u32[]{:S(2)}, u32[]{:S(2)}) async-start(bf16[128,40,256]{2,1,0:T(8,128)(2,1)} %bitcast.37), calls=%async_computation.3 | async-start | bytes 5242880 | tf_op jit(solution)/shard_map/all_to_all | solution.py:693
  170.7 41.9 %copy-start.20 = (bf16[512,2048]{1,0:T(8,128)(2,1)S(1)}, bf16[512,2048]{1,0:T(8,128)(2,1)}, u32[]{:S(2)}) copy-start(bf16[512,2048]{1,0:T(8,128)(2,1)} %refs_1_.3) | copy-start | bytes 6291460
  170.7 41.9 %copy-start.24 = (bf16[2048,256]{1,0:T(8,128)(2,1)S(1)}, bf16[2048,256]{1,0:T(8,128)(2,1)}, u32[]{:S(2)}) copy-start(bf16[2048,256]{1,0:T(8,128)(2,1)} %whole_own.1) | copy-start | bytes 3145732
  174.5 32.7 %collective-permute-start.21 = (bf16[8,64,256]{2,1,0:T(8,128)(2,1)}, bf16[8,64,256]{2,1,0:T(8,128)(2,1)S(1)}, u32[]{:S(2)}, u32[]{:S(2)}) collective-permute-start(bf16[8,64,256]{2,1,0:T(8,128)(2,1)} %get-tuple-element.53), channel_id=1, source_target_pairs={{0,1},{1,2},{2,3},{3,0},{4,5},{5,6},{6,7},{7,4},{8,9},{9,10},{10,1... | collective-permute-start | bytes 786440 | tf_op jit(solution)/shard_map/ppermute | solution.py:615
  175.8 31.3 %collective-permute-start.22 = (bf16[8,64,256]{2,1,0:T(8,128)(2,1)}, bf16[8,64,256]{2,1,0:T(8,128)(2,1)S(1)}, u32[]{:S(2)}, u32[]{:S(2)}) collective-permute-start(bf16[8,64,256]{2,1,0:T(8,128)(2,1)} %get-tuple-element.55), channel_id=1, source_target_pairs={{0,3},{1,0},{2,1},{3,2},{4,7},{5,4},{6,5},{7,6},{8,11},{9,8},{10,9... | collective-permute-start | bytes 786440 | tf_op jit(solution)/shard_map/ppermute | solution.py:615
  177.1 50.6 %collective-permute-start.25 = (bf16[8,64,256]{2,1,0:T(8,128)(2,1)}, bf16[8,64,256]{2,1,0:T(8,128)(2,1)S(1)}, u32[]{:S(2)}, u32[]{:S(2)}) collective-permute-start(bf16[8,64,256]{2,1,0:T(8,128)(2,1)} %get-tuple-element.58), channel_id=1, source_target_pairs={{0,3},{1,0},{2,1},{3,2},{4,7},{5,4},{6,5},{7,6},{8,11},{9,8},{10,9... | collective-permute-start | bytes 786440 | tf_op jit(solution)/shard_map/ppermute | solution.py:615
  178.5 49.3 %collective-permute-start.26 = (bf16[8,64,256]{2,1,0:T(8,128)(2,1)}, bf16[8,64,256]{2,1,0:T(8,128)(2,1)}, u32[]{:S(2)}, u32[]{:S(2)}) collective-permute-start(bf16[8,64,256]{2,1,0:T(8,128)(2,1)} %get-tuple-element.59), channel_id=1, source_target_pairs={{0,1},{1,2},{2,3},{3,0},{4,5},{5,6},{6,7},{7,4},{8,9},{9,10},{10,1... | collective-permute-start | bytes 786440 | tf_op jit(solution)/shard_map/ppermute | solution.py:615
  207.1 1.0 copy-start.5
  208.1 0.9 copy-start.6
  209.9 17.9 %collective-permute-start.23 = (bf16[8,64,256]{2,1,0:T(8,128)(2,1)}, bf16[8,64,256]{2,1,0:T(8,128)(2,1)}, u32[]{:S(2)}, u32[]{:S(2)}) collective-permute-start(bf16[8,64,256]{2,1,0:T(8,128)(2,1)} %get-tuple-element.56), channel_id=1, source_target_pairs={{0,1},{1,2},{2,3},{3,0},{4,5},{5,6},{6,7},{7,4},{8,9},{9,10},{10,1... | collective-permute-start | bytes 786440 | tf_op jit(solution)/shard_map/ppermute | solution.py:615
  209.9 17.9 %collective-permute-start.24 = (bf16[8,64,256]{2,1,0:T(8,128)(2,1)}, bf16[8,64,256]{2,1,0:T(8,128)(2,1)}, u32[]{:S(2)}, u32[]{:S(2)}) collective-permute-start(bf16[8,64,256]{2,1,0:T(8,128)(2,1)} %get-tuple-element.57), channel_id=1, source_target_pairs={{0,3},{1,0},{2,1},{3,2},{4,7},{5,4},{6,5},{7,6},{8,11},{9,8},{10,9... | collective-permute-start | bytes 786440 | tf_op jit(solution)/shard_map/ppermute | solution.py:615
  214.1 13.7 %copy-start.4 = (bf16[16,64,256]{2,1,0:T(8,128)(2,1)S(1)}, bf16[16,64,256]{2,1,0:T(8,128)(2,1)}, u32[]{:S(2)}) copy-start(bf16[16,64,256]{2,1,0:T(8,128)(2,1)} %get-tuple-element.51.own) | copy-start | bytes 1572868
  218.6 16.4 %all-to-all-start.4 = ((f32[32,2,256]{2,1,0:T(2,128)}), f32[32,2,256]{2,1,0:T(2,128)S(1)}, u32[]{:S(2)}, u32[]{:S(2)}) async-start(f32[32,2,256]{2,1,0:T(2,128)} %get-tuple-element.67), calls=%async_computation.4 | async-start | bytes 131072 | tf_op jit(solution)/shard_map/all_to_all | solution.py:717
  235.1 18.3 %all-to-all-start.2 = ((bf16[16,64,256]{2,1,0:T(8,128)(2,1)}), bf16[16,64,256]{2,1,0:T(8,128)(2,1)S(1)}, u32[]{:S(2)}, u32[]{:S(2)}) async-start(bf16[16,64,256]{2,1,0:T(8,128)(2,1)} %arrive.1), calls=%async_computation.2 | async-start | bytes 1048576 | tf_op jit(solution)/shard_map/all_to_all | solution.py:712
